TPU v7x, 128 devices: a whole 4x4x4 slice. The times are simulated.
128 devices in a mesh: fs: 16 (over z, y), tp: 8 (over x, core).
Axes of the slice: x: 4, y: 4, z: 4, core: 2. Of those that a mesh axis runs over, the one named last changes fastest.
Arguments:
- saved_input: bfloat16 [32768, 2048], P('fs'), may hold values from -6 to 6
- query_cotangent: bfloat16 [32768, 2048], P('fs', 'tp'), may hold values from -0.032958984 to 0.032958984
- forget_cotangent: bfloat16 [32768, 2048], P('fs', 'tp'), may hold values from -0.032958984 to 0.032958984
- mixed_output: bfloat16 [32768, 2048], P('fs', 'tp'), may hold values from -6 to 6
- out_cotangent: bfloat16 [32768, 2048], P('fs'), may hold values from -0.032958984 to 0.032958984
- query_basis: bfloat16 [2048, 256], replicated, may hold values from -0.125 to 0.125
- forget_basis: bfloat16 [2048, 256], replicated, may hold values from -0.125 to 0.125
- out_basis: bfloat16 [2048, 256], replicated, may hold values from -0.125 to 0.125
- query_weight: float32 [2048, 2048], P('fs', 'tp'), may hold values from -0.125 to 0.125
- forget_weight: float32 [2048, 2048], P('fs', 'tp'), may hold values from -0.125 to 0.125
- out_weight: float32 [2048, 2048], P('fs', 'tp'), may hold values from -0.125 to 0.125
- query_first: float32 [256, 2048], P('fs', 'tp'), may hold values from -25 to 25
- forget_first: float32 [256, 2048], P('fs', 'tp'), may hold values from -25 to 25
- out_first: float32 [256, 2048], P('fs', 'tp'), may hold values from -25 to 25
- query_second: float32 [256, 2048], P('fs', 'tp'), may hold values from 0.2 to 2
- forget_second: float32 [256, 2048], P('fs', 'tp'), may hold values from 0.2 to 2
- out_second: float32 [256, 2048], P('fs', 'tp'), may hold values from 0.2 to 2
Outputs:
- query_update: float32 [2048, 2048], P('fs', 'tp')
- forget_update: float32 [2048, 2048], P('fs', 'tp')
- out_update: float32 [2048, 2048], P('fs', 'tp')
- query_first_new: float32 [256, 2048], P('fs', 'tp')
- forget_first_new: float32 [256, 2048], P('fs', 'tp')
- out_first_new: float32 [256, 2048], P('fs', 'tp')
- query_second_new: float32 [256, 2048], P('fs', 'tp')
- forget_second_new: float32 [256, 2048], P('fs', 'tp')
- out_second_new: float32 [256, 2048], P('fs', 'tp')
- query_copy: bfloat16 [2048, 2048], P(None, 'tp')
- forget_copy: bfloat16 [2048, 2048], P(None, 'tp')
- out_copy: bfloat16 [2048, 2048], P(None, 'tp')
All inputs are finite; a program needn't handle non-finite values.
Results may differ from a plain program's by a relative error of at most 0.0065.
Values may be sent and summed in bfloat16 or wider, within the bound.
No kernel may reach another device: no remote copies, remote signals or barrier semaphores. Data moves between devices by JAX's collectives and lax.ppermute only.
A program may use at most 128 MiB of HBM per device.

v0:
```python
import jax
import jax.numpy as jnp
from jax import lax
from jax.sharding import Mesh
from jax.sharding import PartitionSpec as P

WIDTH = 2048
RANK = 256
FS = ("fs_0", "fs_1")
FS_TP = ("fs_0", "fs_1", "tp_0", "tp_1")
TP = ("tp_0", "tp_1")


def cut_along(shard, dim, size):
    before, after = (shard.shape[:dim], shard.shape[dim + 1 :])
    return jnp.moveaxis(shard.reshape(*before, size, -1, *after), dim, 0)


def sent_and_summed(shard, axis, dim):
    blocks = cut_along(shard, dim, lax.axis_size(axis))
    arrived = lax.all_to_all(blocks, axis, split_axis=0, concat_axis=0, tiled=True)
    return arrived.astype(jnp.float32).sum(axis=0)


def from_everyone(shard, axis):
    size = lax.axis_size(axis)
    return lax.all_to_all(
        jnp.broadcast_to(shard[None], (size, *shard.shape)), axis, 0, 0, tiled=True
    )


def laid_out(blocks, dim):
    blocks = jnp.moveaxis(blocks, 0, dim)
    dims = blocks.shape
    return blocks.reshape(*dims[:dim], dims[dim] * dims[dim + 1], *dims[dim + 2 :])


def gathered_copies(shard, axis, dim):
    blocks = from_everyone(shard, axis)
    return laid_out(blocks, dim)


def one_axis_at_a_time(shard, axes):
    for axis in axes:
        shard = lax.psum(shard, axis)
    return shard


def sent_together(arrays, axis, dim, along):
    both = jnp.concatenate(arrays, axis=along)
    result, at, gathered = (lax.all_gather(both, axis, axis=dim, tiled=True), 0, [])
    for a in arrays:
        gathered.append(lax.slice_in_dim(result, at, at + a.shape[along], axis=along))
        at += a.shape[along]
    return tuple(gathered)


def contract_rows(left, right):
    return lax.dot_general(
        left, right, (((0,), (0,)), ((), ())), precision=None, preferred_element_type=jnp.float32
    )


def moments(source, cotangent, basis, weight, first, second):
    row_count = weight.shape[0]
    basis_rows = lax.dynamic_slice_in_dim(
        basis, lax.axis_index(FS) * row_count, row_count, 0
    ).astype(jnp.float32)
    reduced = jnp.dot(source, basis, preferred_element_type=jnp.float32)
    reduced_high = reduced.astype(jnp.bfloat16)
    reduced_low = (reduced - reduced_high.astype(jnp.float32)).astype(jnp.bfloat16)
    projected = sent_and_summed(
        (contract_rows(reduced_high, cotangent) + contract_rows(reduced_low, cotangent)).astype(
            jnp.bfloat16
        ),
        FS,
        0,
    )
    first_new = 0.8 * first + 0.2 * projected
    second_new = 0.95 * second + 0.05 * projected * projected
    direction = first_new / (jnp.sqrt(second_new) + 1e-08)
    return (direction, first_new, second_new, jnp.sum(direction * direction), basis_rows)


def expand(direction, basis_rows, total, weight):
    stepped = jnp.dot(basis_rows, gathered_copies(direction, FS, 0))
    update = stepped * lax.rsqrt(total / (RANK * WIDTH) + 1e-06)
    return (update, (weight - 0.05 * update).astype(jnp.bfloat16))


def local(
    saved_input,
    query_cotangent,
    forget_cotangent,
    mixed_output,
    out_cotangent,
    query_basis,
    forget_basis,
    out_basis,
    query_weight,
    forget_weight,
    out_weight,
    query_first,
    forget_first,
    out_first,
    query_second,
    forget_second,
    out_second,
):
    query_dir, query_one, query_two, query_sq, query_rows = moments(
        saved_input, query_cotangent, query_basis, query_weight, query_first, query_second
    )
    forget_dir, forget_one, forget_two, forget_sq, forget_rows = moments(
        saved_input, forget_cotangent, forget_basis, forget_weight, forget_first, forget_second
    )
    out_dir, out_one, out_two, out_sq, out_rows = moments(
        out_cotangent, mixed_output, out_basis, out_weight, out_first, out_second
    )
    totals = (
        one_axis_at_a_time(query_sq, FS_TP),
        one_axis_at_a_time(forget_sq, FS_TP),
        one_axis_at_a_time(out_sq, FS_TP),
    )
    query_step, query_new = expand(query_dir, query_rows, totals[0], query_weight)
    forget_step, forget_new = expand(forget_dir, forget_rows, totals[1], forget_weight)
    out_step, out_new = expand(out_dir, out_rows, totals[2], out_weight)
    query_copy, forget_copy, out_copy = sent_together((query_new, forget_new, out_new), FS, 0, 1)
    return (
        query_step,
        forget_step,
        out_step,
        query_one,
        forget_one,
        out_one,
        query_two,
        forget_two,
        out_two,
        query_copy,
        forget_copy,
        out_copy,
    )


def solution(mesh):
    split = Mesh(mesh.devices.reshape(4, 4, 4, 2), ("fs_0", "fs_1", "tp_0", "tp_1"))
    in_specs = (
        P(FS, None),
        P(FS, TP),
        P(FS, TP),
        P(FS, TP),
        P(FS, None),
        P(),
        P(),
        P(),
        P(FS, TP),
        P(FS, TP),
        P(FS, TP),
        P(FS, TP),
        P(FS, TP),
        P(FS, TP),
        P(FS, TP),
        P(FS, TP),
        P(FS, TP),
    )
    out_specs = (
        P(FS, TP),
        P(FS, TP),
        P(FS, TP),
        P(FS, TP),
        P(FS, TP),
        P(FS, TP),
        P(FS, TP),
        P(FS, TP),
        P(FS, TP),
        P(None, TP),
        P(None, TP),
        P(None, TP),
    )
    return jax.shard_map(local, mesh=split, in_specs=in_specs, out_specs=out_specs, check_vma=False)
```

profile of v0, /device:TPU:1, one launch (start us, length us, event | category | flops | bytes accessed | tf_op | source)
XLA Modules:
  0.0 189.6 jit_solution(8904158954147823008)
XLA Ops:
  7.2 6.2 %fusion.27 = f32[2048,256]{1,0:T(8,128)S(1)} fusion(bf16[2048,2048]{1,0:T(8,128)(2,1)} %param.21, bf16[2048,256]{1,0:T(8,128)(2,1)} %param.24), kind=kOutput, calls=%fused_computation.52 | convolution fusion | flops 2147483648 | bytes 11534336 | tf_op jit(solution)/shard_map/dot_general | solution.py:69
  13.9 1.1 fusion.2
  15.1 8.6 %all-to-all-start.4 = ((bf16[16,16,256]{2,1,0:T(8,128)(2,1)}), bf16[16,16,256]{2,1,0:T(8,128)(2,1)S(1)}, u32[]{:S(2)}, u32[]{:S(2)}) async-start(bf16[16,16,256]{2,1,0:T(8,128)(2,1)} %bitcast.4), calls=%async_computation.4 | async-start | bytes 262144 | tf_op jit(solution)/shard_map/all_to_all | solution.py:21
  23.7 5.9 %fusion.26 = f32[2048,256]{1,0:T(8,128)S(1)} fusion(bf16[2048,2048]{1,0:T(8,128)(2,1)} %param.17, bf16[2048,256]{1,0:T(8,128)(2,1)S(1)} %copy-done), kind=kOutput, calls=%fused_computation.51 | convolution fusion | flops 2147483648 | bytes 11534336 | tf_op jit(solution)/shard_map/dot_general | solution.py:69
  31.4 5.9 %fusion.25 = f32[2048,256]{1,0:T(8,128)S(1)} fusion(bf16[2048,2048]{1,0:T(8,128)(2,1)} %param.17, bf16[2048,256]{1,0:T(8,128)(2,1)S(1)} %copy-done.13), kind=kOutput, calls=%fused_computation.50 | convolution fusion | flops 2147483648 | bytes 11534336 | tf_op jit(solution)/shard_map/dot_general | solution.py:69
  39.0 6.8 %all-to-all-start.2 = ((bf16[16,16,256]{2,1,0:T(8,128)(2,1)}), bf16[16,16,256]{2,1,0:T(8,128)(2,1)S(1)}, u32[]{:S(2)}, u32[]{:S(2)}) async-start(bf16[16,16,256]{2,1,0:T(8,128)(2,1)} %bitcast.2), calls=%async_computation.2 | async-start | bytes 262144 | tf_op jit(solution)/shard_map/all_to_all | solution.py:21
  45.9 1.2 multiply_reduce_fusion
  47.1 5.6 %all-to-all-done.2 = bf16[16,16,256]{2,1,0:T(8,128)(2,1)S(1)} async-done(((bf16[16,16,256]{2,1,0:T(8,128)(2,1)}), bf16[16,16,256]{2,1,0:T(8,128)(2,1)S(1)}, u32[]{:S(2)}, u32[]{:S(2)}) %all-to-all-start.2) | async-done | bytes 131104 | tf_op jit(solution)/shard_map/all_to_all | solution.py:21
  52.7 3.5 %all-to-all-start = ((bf16[16,16,256]{2,1,0:T(8,128)(2,1)}), bf16[16,16,256]{2,1,0:T(8,128)(2,1)S(1)}, u32[]{:S(2)}, u32[]{:S(2)}) async-start(bf16[16,16,256]{2,1,0:T(8,128)(2,1)} %bitcast), calls=%async_computation | async-start | bytes 262144 | tf_op jit(solution)/shard_map/all_to_all | solution.py:21
  56.2 1.2 multiply_reduce_fusion.1
  57.5 5.5 %all-to-all-done = bf16[16,16,256]{2,1,0:T(8,128)(2,1)S(1)} async-done(((bf16[16,16,256]{2,1,0:T(8,128)(2,1)}), bf16[16,16,256]{2,1,0:T(8,128)(2,1)S(1)}, u32[]{:S(2)}, u32[]{:S(2)}) %all-to-all-start) | async-done | bytes 131104 | tf_op jit(solution)/shard_map/all_to_all | solution.py:21
  63.7 3.5 %all-to-all-start.3 = ((bf16[16,16,256]{2,1,0:T(8,128)(2,1)}), bf16[16,16,256]{2,1,0:T(8,128)(2,1)S(1)}, u32[]{:S(2)}, u32[]{:S(2)}) async-start(bf16[16,16,256]{2,1,0:T(8,128)(2,1)} %broadcast_in_dim.7), calls=%async_computation.3 | async-start | bytes 262144 | tf_op jit(solution)/shard_map/all_to_all | solution.py:27
  67.2 1.2 multiply_reduce_fusion.2
  68.5 9.8 %all-reduce.2 = (f32[]{:T(128)}, f32[]{:T(128)}, f32[]{:T(128)}) all-reduce(f32[]{:T(128)} %get-tuple-element.32, f32[]{:T(128)} %get-tuple-element.28, f32[]{:T(128)} %get-tuple-element.24), channel_id=1, replica_groups=mesh['fs_0'=4,'fs_1'=4,'tp_0'=4,'tp_1'=2] {'fs_0'}, use_global_device_ids=true, to_apply=%region_2.0 | all-reduce | flops 3 | bytes 24 | tf_op jit(solution)/shard_map/psum | solution.py:45
  78.2 8.7 %all-reduce.1 = (f32[]{:T(128)}, f32[]{:T(128)}, f32[]{:T(128)}) all-reduce(f32[]{:T(128)} %get-tuple-element.18, f32[]{:T(128)} %get-tuple-element.19, f32[]{:T(128)} %get-tuple-element.20), channel_id=1, replica_groups=mesh['fs_0'=4,'fs_1'=4,'tp_0'=4,'tp_1'=2] {'fs_1'}, use_global_device_ids=true, to_apply=%region_3.0 | all-reduce | flops 3 | bytes 24 | tf_op jit(solution)/shard_map/psum | solution.py:45
  86.9 9.1 %all-reduce = (f32[]{:T(128)}, f32[]{:T(128)}, f32[]{:T(128)}) all-reduce(f32[]{:T(128)} %get-tuple-element.15, f32[]{:T(128)} %get-tuple-element.16, f32[]{:T(128)} %get-tuple-element.17), channel_id=1, replica_groups=mesh['fs_0'=4,'fs_1'=4,'tp_0'=4,'tp_1'=2] {'tp_0'}, use_global_device_ids=true, to_apply=%region_4.0 | all-reduce | flops 3 | bytes 24 | tf_op jit(solution)/shard_map/psum | solution.py:45
  96.0 12.6 %all-reduce.3 = (f32[]{:T(128)}, f32[]{:T(128)}, f32[]{:T(128)}) all-reduce(f32[]{:T(128)} %get-tuple-element.12, f32[]{:T(128)} %get-tuple-element.13, f32[]{:T(128)} %get-tuple-element.14), channel_id=1, replica_groups=mesh['fs_0'=4,'fs_1'=4,'tp_0'=4,'tp_1'=2] {'tp_1'}, use_global_device_ids=true, to_apply=%region_5.0 | all-reduce | flops 3 | bytes 24 | tf_op jit(solution)/shard_map/psum | solution.py:45
  111.3 3.5 %all-to-all-start.5 = ((bf16[16,16,256]{2,1,0:T(8,128)(2,1)}), bf16[16,16,256]{2,1,0:T(8,128)(2,1)S(1)}, u32[]{:S(2)}, u32[]{:S(2)}) async-start(bf16[16,16,256]{2,1,0:T(8,128)(2,1)} %broadcast_in_dim.8), calls=%async_computation.5 | async-start | bytes 262144 | tf_op jit(solution)/shard_map/all_to_all | solution.py:27
  115.7 6.0 %all-to-all-done.5 = bf16[16,16,256]{2,1,0:T(8,128)(2,1)S(1)} async-done(((bf16[16,16,256]{2,1,0:T(8,128)(2,1)}), bf16[16,16,256]{2,1,0:T(8,128)(2,1)S(1)}, u32[]{:S(2)}, u32[]{:S(2)}) %all-to-all-start.5) | async-done | bytes 131104 | tf_op jit(solution)/shard_map/all_to_all | solution.py:27
  122.3 3.5 %all-to-all-start.1 = ((bf16[16,16,256]{2,1,0:T(8,128)(2,1)}), bf16[16,16,256]{2,1,0:T(8,128)(2,1)S(1)}, u32[]{:S(2)}, u32[]{:S(2)}) async-start(bf16[16,16,256]{2,1,0:T(8,128)(2,1)} %broadcast_in_dim.6), calls=%async_computation.1 | async-start | bytes 262144 | tf_op jit(solution)/shard_map/all_to_all | solution.py:27
  125.9 1.7 subtract_convert_fusion.6
  127.6 5.1 %all-to-all-done.1 = bf16[16,16,256]{2,1,0:T(8,128)(2,1)S(1)} async-done(((bf16[16,16,256]{2,1,0:T(8,128)(2,1)}), bf16[16,16,256]{2,1,0:T(8,128)(2,1)S(1)}, u32[]{:S(2)}, u32[]{:S(2)}) %all-to-all-start.1) | async-done | bytes 131104 | tf_op jit(solution)/shard_map/all_to_all | solution.py:27
  134.2 44.9 %all-gather.2.cloned.1.call-done = bf16[2048,768]{1,0:T(8,128)(2,1)} async-done(((bf16[128,768]{1,0:T(8,128)(2,1)}), bf16[2048,768]{1,0:T(8,128)(2,1)}) %all-gather.2.cloned.1.call-update) | async-done | bytes 3145744 | tf_op jit(solution)/shard_map/all_gather | solution.py:51
  179.1 3.6 %fusion.24 = (bf16[2048,256]{1,0:T(8,128)(2,1)}, bf16[2048,256]{1,0:T(8,128)(2,1)}, bf16[2048,256]{1,0:T(8,128)(2,1)}) fusion(bf16[2048,768]{1,0:T(8,128)(2,1)} %all-gather.2.cloned.1.call-done), kind=kLoop, calls=%fused_computation.49 | loop fusion | bytes 6291456 | tf_op jit(solution)/shard_map/slice | solution.py:53
  (46 shorter events, 8.3 us)
Async XLA Ops:
  7.2 16.5 %copy-start = (bf16[2048,256]{1,0:T(8,128)(2,1)S(1)}, bf16[2048,256]{1,0:T(8,128)(2,1)}, u32[]{:S(2)}) copy-start(bf16[2048,256]{1,0:T(8,128)(2,1)} %param.23) | copy-start | bytes 3145732
  7.2 6.3 %copy-start.1 = (bf16[2048,256]{1,0:T(8,128)(2,1)S(1)}, bf16[2048,256]{1,0:T(8,128)(2,1)}, u32[]{:S(2)}) copy-start(bf16[2048,256]{1,0:T(8,128)(2,1)} %param.20) | copy-start | bytes 3145732
  15.1 24.0 %all-to-all-start.4 = ((bf16[16,16,256]{2,1,0:T(8,128)(2,1)}), bf16[16,16,256]{2,1,0:T(8,128)(2,1)S(1)}, u32[]{:S(2)}, u32[]{:S(2)}) async-start(bf16[16,16,256]{2,1,0:T(8,128)(2,1)} %bitcast.4), calls=%async_computation.4 | async-start | bytes 262144 | tf_op jit(solution)/shard_map/all_to_all | solution.py:21
  23.7 6.0 %copy-start.2 = (bf16[2048,256]{1,0:T(8,128)(2,1)S(1)}, bf16[2048,256]{1,0:T(8,128)(2,1)}, u32[]{:S(2)}) copy-start(bf16[2048,256]{1,0:T(8,128)(2,1)} %param.19) | copy-start | bytes 3145732
  30.1 1.2 copy-start.13
  31.4 6.0 %copy-start.3 = (bf16[2048,256]{1,0:T(8,128)(2,1)S(1)}, bf16[2048,256]{1,0:T(8,128)(2,1)}, u32[]{:S(2)}) copy-start(bf16[2048,256]{1,0:T(8,128)(2,1)} %param.18) | copy-start | bytes 3145732
  37.8 8.1 %copy-start.7 = (f32[16,256]{1,0:T(8,128)S(1)}, f32[16,256]{1,0:T(8,128)}, u32[]{:S(2)}) copy-start(f32[16,256]{1,0:T(8,128)} %param.33) | copy-start | bytes 49156
  37.8 8.1 %copy-start.8 = (f32[16,256]{1,0:T(8,128)S(1)}, f32[16,256]{1,0:T(8,128)}, u32[]{:S(2)}) copy-start(f32[16,256]{1,0:T(8,128)} %param.30) | copy-start | bytes 49156
  37.8 18.4 %copy-start.9 = (f32[16,256]{1,0:T(8,128)S(1)}, f32[16,256]{1,0:T(8,128)}, u32[]{:S(2)}) copy-start(f32[16,256]{1,0:T(8,128)} %param.32) | copy-start | bytes 49156
  37.8 18.4 %copy-start.10 = (f32[16,256]{1,0:T(8,128)S(1)}, f32[16,256]{1,0:T(8,128)}, u32[]{:S(2)}) copy-start(f32[16,256]{1,0:T(8,128)} %param.29) | copy-start | bytes 49156
  37.9 29.4 %copy-start.11 = (f32[16,256]{1,0:T(8,128)S(1)}, f32[16,256]{1,0:T(8,128)}, u32[]{:S(2)}) copy-start(f32[16,256]{1,0:T(8,128)} %param.31) | copy-start | bytes 49156
  37.9 29.4 %copy-start.12 = (f32[16,256]{1,0:T(8,128)S(1)}, f32[16,256]{1,0:T(8,128)}, u32[]{:S(2)}) copy-start(f32[16,256]{1,0:T(8,128)} %param.28) | copy-start | bytes 49156
  37.9 77.0 %copy-start.4 = (f32[128,256]{1,0:T(8,128)S(1)}, f32[128,256]{1,0:T(8,128)}, u32[]{:S(2)}) copy-start(f32[128,256]{1,0:T(8,128)} %param.26) | copy-start | bytes 393220
  39.0 86.9 %copy-start.5 = (f32[128,256]{1,0:T(8,128)S(1)}, f32[128,256]{1,0:T(8,128)}, u32[]{:S(2)}) copy-start(f32[128,256]{1,0:T(8,128)} %param.27) | copy-start | bytes 393220
  39.0 93.6 %copy-start.6 = (f32[128,256]{1,0:T(8,128)S(1)}, f32[128,256]{1,0:T(8,128)}, u32[]{:S(2)}) copy-start(f32[128,256]{1,0:T(8,128)} %param.25) | copy-start | bytes 393220
  39.0 13.6 %all-to-all-start.2 = ((bf16[16,16,256]{2,1,0:T(8,128)(2,1)}), bf16[16,16,256]{2,1,0:T(8,128)(2,1)S(1)}, u32[]{:S(2)}, u32[]{:S(2)}) async-start(bf16[16,16,256]{2,1,0:T(8,128)(2,1)} %bitcast.2), calls=%async_computation.2 | async-start | bytes 262144 | tf_op jit(solution)/shard_map/all_to_all | solution.py:21
  52.7 10.3 %all-to-all-start = ((bf16[16,16,256]{2,1,0:T(8,128)(2,1)}), bf16[16,16,256]{2,1,0:T(8,128)(2,1)S(1)}, u32[]{:S(2)}, u32[]{:S(2)}) async-start(bf16[16,16,256]{2,1,0:T(8,128)(2,1)} %bitcast), calls=%async_computation | async-start | bytes 262144 | tf_op jit(solution)/shard_map/all_to_all | solution.py:21
  63.7 47.0 %all-to-all-start.3 = ((bf16[16,16,256]{2,1,0:T(8,128)(2,1)}), bf16[16,16,256]{2,1,0:T(8,128)(2,1)S(1)}, u32[]{:S(2)}, u32[]{:S(2)}) async-start(bf16[16,16,256]{2,1,0:T(8,128)(2,1)} %broadcast_in_dim.7), calls=%async_computation.3 | async-start | bytes 262144 | tf_op jit(solution)/shard_map/all_to_all | solution.py:27
  111.3 10.3 %all-to-all-start.5 = ((bf16[16,16,256]{2,1,0:T(8,128)(2,1)}), bf16[16,16,256]{2,1,0:T(8,128)(2,1)S(1)}, u32[]{:S(2)}, u32[]{:S(2)}) async-start(bf16[16,16,256]{2,1,0:T(8,128)(2,1)} %broadcast_in_dim.8), calls=%async_computation.5 | async-start | bytes 262144 | tf_op jit(solution)/shard_map/all_to_all | solution.py:27
  122.3 10.3 %all-to-all-start.1 = ((bf16[16,16,256]{2,1,0:T(8,128)(2,1)}), bf16[16,16,256]{2,1,0:T(8,128)(2,1)S(1)}, u32[]{:S(2)}, u32[]{:S(2)}) async-start(bf16[16,16,256]{2,1,0:T(8,128)(2,1)} %broadcast_in_dim.6), calls=%async_computation.1 | async-start | bytes 262144 | tf_op jit(solution)/shard_map/all_to_all | solution.py:27
  125.8 53.3 %all-gather.2.cloned.1.call-start = ((), (), s32[]{:S(2)}) async-start(), calls=%async_computation.6 | async-start | bytes 3342336 | tf_op jit(solution)/shard_map/all_gather | solution.py:51
Sparse Core Ops, SparseCore 0:
  134.3 44.7 all-gather.1
where the time goes:
time: 190 us
  waiting for transfers between devices  67.1 us (35%)
  blocking collectives  40.1 us (21%)
  starting transfers between devices  29.5 us (16%)
  matrix products  26.3 us (14%)
  between operations  16.4 us (9%)
  local copies, waits for them, and re-layouts  5.76 us (3%)
  other arithmetic  4.41 us (2%)
    all_gather x1, waiting for transfers between devices, sent_together(): lax.all_gather(both, axis, axis=dim, tiled=True)  44.9 us
    psum x4, blocking collectives, one_axis_at_a_time(): shard = lax.psum(shard, axis)  40.1 us
    all_to_all x3, starting transfers between devices, sent_and_summed(): lax.all_to_all(blocks, axis, split_axis=0, concat_axis=0, tiled=True)  18.9 us
    dot_general x3, matrix products, moments(): reduced = jnp.dot(source, basis, preferred_element_type=jnp.float32)  18.1 us
    all_to_all x3, waiting for transfers between devices, sent_and_summed(): lax.all_to_all(blocks, axis, split_axis=0, concat_axis=0, tiled=True)  11.1 us
    all_to_all x3, waiting for transfers between devices, from_everyone(): lax.all_to_all(jnp.broadcast_to(shard[None], (size, *shard.shape)), axis,...  11 us
    all_to_all x3, starting transfers between devices, from_everyone(): lax.all_to_all(jnp.broadcast_to(shard[None], (size, *shard.shape)), axis,...  10.5 us
    dot_general x6, matrix products, contract_rows(): lax.dot_general(left, right, (((0,), (0,)), ((), ())), precision=None, pr...  4.85 us
  transfers between devices with their start and end apart: 7, of which 5 were waited for; matrix products, arithmetic and copies ran while one was open for 11% of the time, Pallas kernels for 0%

commit v1 on v0

v1 whole, which is shorter than its diff:
```python
import jax
import jax.numpy as jnp
from jax import lax
from jax.experimental import pallas as pl
from jax.experimental.pallas import tpu as pltpu
from jax.sharding import Mesh
from jax.sharding import PartitionSpec as P

WIDTH = 2048
RANK = 256
FS = ("fs_0", "fs_1")
TP = ("tp_0", "tp_1")
MATS = 3
TOKEN_BLOCK = 512
ROW_BLOCK = 256
VMEM_BYTES = 60 * 1024 * 1024

F32 = jnp.float32
BF16 = jnp.bfloat16


def whole(shape):
    return pl.BlockSpec(shape, lambda *_: (0,) * len(shape))


def cost(flops, moved):
    return pl.CostEstimate(flops=flops, bytes_accessed=moved, transcendentals=0)


def project_kernel(saved, grad, qb, fb, ob, qc, fc, mixed, out, *sums):
    step = pl.program_id(0)
    for total, source, basis, cotangent in zip(
        sums, (saved, saved, grad), (qb, fb, ob), (qc, fc, mixed)
    ):
        reduced = jnp.dot(source[...], basis[...], preferred_element_type=F32).astype(BF16)
        part = lax.dot_general(
            reduced, cotangent[...], (((0,), (0,)), ((), ())), preferred_element_type=F32
        )

        @pl.when(step == 0)
        def _():
            total[...] = part

        @pl.when(step > 0)
        def _():
            total[...] += part

    @pl.when(step == pl.num_programs(0) - 1)
    def _():
        groups, rows = out.shape[0], out.shape[1] // MATS
        for m, total in enumerate(sums):
            out[:, m * rows : (m + 1) * rows, :] = (
                total[...].astype(BF16).reshape(groups, rows, total.shape[1])
            )


def project(saved, grad, bases, cotangents, groups):
    tokens, width = saved.shape
    cols = cotangents[0].shape[1]
    rows = RANK // groups
    return pl.pallas_call(
        project_kernel,
        grid=(tokens // TOKEN_BLOCK,),
        in_specs=[
            pl.BlockSpec((TOKEN_BLOCK, width), lambda i: (i, 0)),
            pl.BlockSpec((TOKEN_BLOCK, width), lambda i: (i, 0)),
            *(whole((width, RANK)) for _ in bases),
            *(pl.BlockSpec((TOKEN_BLOCK, cols), lambda i: (i, 0)) for _ in cotangents),
        ],
        out_specs=whole((groups, MATS * rows, cols)),
        out_shape=jax.ShapeDtypeStruct((groups, MATS * rows, cols), BF16),
        scratch_shapes=[pltpu.VMEM((RANK, cols), F32) for _ in range(MATS)],
        compiler_params=pltpu.CompilerParams(vmem_limit_bytes=VMEM_BYTES),
        cost_estimate=cost(MATS * 2 * tokens * RANK * (width + cols), 22 << 20),
        name="project",
    )(saved, grad, *bases, *cotangents)


def moment_kernel(arrived, *refs):
    firsts, seconds = refs[:MATS], refs[MATS : 2 * MATS]
    firsts_new, seconds_new = refs[2 * MATS : 3 * MATS], refs[3 * MATS : 4 * MATS]
    directions = refs[4 * MATS]
    groups = arrived.shape[0]
    rows = arrived.shape[1] // MATS
    for m in range(MATS):
        at = slice(m * rows, (m + 1) * rows)
        projected = arrived[0, at, :].astype(F32)
        for g in range(1, groups):
            projected = projected + arrived[g, at, :].astype(F32)
        first_new = 0.8 * firsts[m][...] + 0.2 * projected
        second_new = 0.95 * seconds[m][...] + 0.05 * projected * projected
        firsts_new[m][...] = first_new
        seconds_new[m][...] = second_new
        direction = (first_new / (jnp.sqrt(second_new) + 1e-08)).astype(BF16)
        for g in range(groups):
            directions[g, at, :] = direction


def moments(arrived, firsts, seconds):
    state = [jax.ShapeDtypeStruct(a.shape, F32) for a in (*firsts, *seconds)]
    results = pl.pallas_call(
        moment_kernel,
        out_shape=(*state, jax.ShapeDtypeStruct(arrived.shape, BF16)),
        cost_estimate=cost(1 << 22, 1 << 20),
        name="moments",
    )(arrived, *firsts, *seconds)
    return results[:MATS], results[MATS : 2 * MATS], results[2 * MATS]


def square_kernel(gathered, out):
    rows = gathered.shape[1] // MATS
    out[...] = jnp.zeros_like(out)
    for m in range(MATS):
        values = gathered[:, m * rows : (m + 1) * rows, :].astype(F32)
        total = jnp.sum(values * values)
        out[m : m + 1, :] = jnp.full((1, out.shape[1]), total, F32)


def squares(gathered):
    return pl.pallas_call(
        square_kernel,
        out_shape=jax.ShapeDtypeStruct((8, 128), F32),
        cost_estimate=cost(1 << 22, 1 << 19),
        name="squares",
    )(gathered)


def expand_kernel(me, totals, gathered, qb, fb, ob, weights, *outs):
    updates, copies = outs[:MATS], outs[MATS:]
    step = pl.program_id(0)
    rows, cols = updates[0].shape
    rank_rows = gathered.shape[1] // MATS
    for m, basis in enumerate((qb, fb, ob)):
        direction = gathered[:, m * rank_rows : (m + 1) * rank_rows, :].reshape(RANK, cols)
        total = totals[m : m + 1, :1]
        scale = lax.rsqrt(total * (1.0 / (RANK * WIDTH)) + 1e-06)

        @pl.when(step == 0)
        def _():
            mine = basis[pl.ds(pl.multiple_of(me[0] * rows, rows), rows), :]
            updates[m][...] = jnp.dot(mine, direction, preferred_element_type=F32) * scale

        at = pl.ds(pl.multiple_of(step * ROW_BLOCK, ROW_BLOCK), ROW_BLOCK)
        stepped = jnp.dot(basis[at, :], direction, preferred_element_type=F32)
        weight = weights[:, m * cols : (m + 1) * cols].astype(F32)
        copies[m][...] = (weight - 0.05 * (stepped * scale)).astype(BF16)


def expand(me, totals, gathered, bases, weights, rows):
    width = bases[0].shape[0]
    cols = gathered.shape[2]
    return pl.pallas_call(
        expand_kernel,
        grid_spec=pltpu.PrefetchScalarGridSpec(
            num_scalar_prefetch=1,
            grid=(width // ROW_BLOCK,),
            in_specs=[
                whole(totals.shape),
                whole(gathered.shape),
                *(whole((width, RANK)) for _ in bases),
                pl.BlockSpec((ROW_BLOCK, MATS * cols), lambda i, *_: (i, 0)),
            ],
            out_specs=[
                *(whole((rows, cols)) for _ in range(MATS)),
                *(pl.BlockSpec((ROW_BLOCK, cols), lambda i, *_: (i, 0)) for _ in range(MATS)),
            ],
        ),
        out_shape=[
            *(jax.ShapeDtypeStruct((rows, cols), F32) for _ in range(MATS)),
            *(jax.ShapeDtypeStruct((width, cols), BF16) for _ in range(MATS)),
        ],
        compiler_params=pltpu.CompilerParams(vmem_limit_bytes=VMEM_BYTES),
        cost_estimate=cost(MATS * 2 * width * RANK * cols, 9 << 20),
        name="expand",
    )(me, totals, gathered, *bases, weights)


def summed_over_tp(value):
    for axis, far in (("tp_1", 1), ("tp_0", 1), ("tp_0", 2)):
        size = lax.axis_size(axis)
        value = value + lax.ppermute(value, axis, [(i, i ^ far) for i in range(size)])
    return value


def local(
    saved_input,
    query_cotangent,
    forget_cotangent,
    mixed_output,
    out_cotangent,
    query_basis,
    forget_basis,
    out_basis,
    query_weight,
    forget_weight,
    out_weight,
    *state,
):
    rows = query_weight.shape[0]
    groups = lax.axis_size(FS)
    bases = (query_basis, forget_basis, out_basis)
    weights = jnp.concatenate(
        [w.astype(BF16) for w in (query_weight, forget_weight, out_weight)], axis=1
    )
    all_weights = lax.all_gather(weights, FS, axis=0, tiled=True)
    blocks = project(
        saved_input,
        out_cotangent,
        bases,
        (query_cotangent, forget_cotangent, mixed_output),
        groups,
    )
    arrived = lax.all_to_all(blocks, FS, 0, 0, tiled=True)
    firsts, seconds, directions = moments(arrived, state[:MATS], state[MATS:])
    gathered = lax.all_to_all(directions, FS, 0, 0, tiled=True)
    totals = summed_over_tp(squares(gathered))
    me = lax.axis_index(FS).astype(jnp.int32).reshape(1)
    outs = expand(me, totals, gathered, bases, all_weights, rows)
    return (*outs[:MATS], *firsts, *seconds, *outs[MATS:])


def solution(mesh):
    split = Mesh(mesh.devices.reshape(4, 4, 4, 2), ("fs_0", "fs_1", "tp_0", "tp_1"))
    in_specs = (
        P(FS, None),
        P(FS, TP),
        P(FS, TP),
        P(FS, TP),
        P(FS, None),
        P(),
        P(),
        P(),
        *(P(FS, TP) for _ in range(9)),
    )
    out_specs = (*(P(FS, TP) for _ in range(9)), *(P(None, TP) for _ in range(3)))
    return jax.shard_map(local, mesh=split, in_specs=in_specs, out_specs=out_specs, check_vma=False)
```

time: 190 us -> 97 us (0.51)
  waiting for transfers between devices: 67.1 us -> 3.52 us
  Pallas kernels: 0 us -> 34.2 us
  matrix products: 26.3 us -> 0 us
  starting transfers between devices: 29.5 us -> 5.59 us
  blocking collectives: 40.1 us -> 33.1 us
  local copies, waits for them, and re-layouts: 5.76 us -> 0 us
  between operations: 16.4 us -> 14 us
    all_gather x1, waiting for transfers between devices: 44.9 us -> 0.01 us  [local(): all_weights = lax.all_gather(weights, FS, axis=0, tiled=True)]
    psum x4 -> x0, blocking collectives: 40.1 us -> none  [one_axis_at_a_time(): shard = lax.psum(shard, axis)]
    pallas_call x0 -> x4, Pallas kernels: none -> 34.2 us  [the longest x1 20.8 us: project(): pl.pallas_call(project_kernel, grid=(tokens // TOKEN_BLOCK,), in_specs=[p...]
    all_to_all x0 -> x2, blocking collectives: none -> 33.1 us  [the longest x1 17.9 us: local(): arrived = lax.all_to_all(blocks, FS, 0, 0, tiled=True)]
    all_to_all x6 -> x0, starting transfers between devices: 29.4 us -> none  [the longest x3 18.9 us: sent_and_summed(): lax.all_to_all(blocks, axis, split_axis=0, concat_axis=0, tiled=True)]
    dot_general x12 -> x0, matrix products: 26.3 us -> none  [the longest x3 18.1 us: moments(): reduced = jnp.dot(source, basis, preferred_element_type=jnp.float32)]
    all_to_all x6 -> x0, waiting for transfers between devices: 22.2 us -> none  [the longest x3 11.1 us: sent_and_summed(): lax.all_to_all(blocks, axis, split_axis=0, concat_axis=0, tiled=True)]
    ppermute x0 -> x3, starting transfers between devices: none -> 5.55 us  [summed_over_tp(): lax.ppermute(value, axis, [(i, i ^ far) for i in range(size)])]
  transfers between devices with their start and end apart: 7 -> 4, of which waited for: 5 -> 3; matrix products, arithmetic and copies ran while one was open for 11% -> 1% of each run, Pallas kernels for 0% -> 26%
where the time goes in v1:
time: 97 us; the launch traced here: 95.1 us
  Pallas kernels  34.2 us (35%)
  blocking collectives  33.1 us (34%)
  between operations  14 us (14%)
  starting transfers between devices  5.59 us (6%)
  other arithmetic  4.71 us (5%)
  waiting for transfers between devices  3.52 us (4%)
    pallas_call x1, Pallas kernels, project(): pl.pallas_call(project_kernel, grid=(tokens // TOKEN_BLOCK,), in_specs=[p...  20.8 us
    all_to_all x1, blocking collectives, local(): arrived = lax.all_to_all(blocks, FS, 0, 0, tiled=True)  17.9 us
    all_to_all x1, blocking collectives, local(): gathered = lax.all_to_all(directions, FS, 0, 0, tiled=True)  15.2 us
    pallas_call x1, Pallas kernels, expand(): pl.pallas_call(expand_kernel, grid_spec=pltpu.PrefetchScalarGridSpec(num_...  9.7 us
    ppermute x3, starting transfers between devices, summed_over_tp(): lax.ppermute(value, axis, [(i, i ^ far) for i in range(size)])  5.55 us
    ppermute x3, waiting for transfers between devices, summed_over_tp(): lax.ppermute(value, axis, [(i, i ^ far) for i in range(size)])  3.5 us
    convert_element_type x3, other arithmetic, local(): w.astype(BF16)  2.74 us
  transfers between devices with their start and end apart: 4, of which 3 were waited for; matrix products, arithmetic and copies ran while one was open for 1% of the time, Pallas kernels for 26%

profile of v1, /device:TPU:1, one launch (start us, length us, event | category | flops | bytes accessed | tf_op | source)
XLA Modules:
  0.0 95.1 jit_solution(492297342338174128)
XLA Ops:
  7.2 0.0 all-gather.2.cloned.1.call-start
  7.2 0.9 convert_element_type.9
  8.1 0.9 convert_element_type.10
  9.0 0.9 convert_element_type.11
  10.0 0.7 pad_maximum_fusion
  10.7 0.0 all-gather.2.cloned.1.call-update
  10.7 20.8 %project.1 = bf16[16,48,256]{2,1,0:T(8,128)(2,1)} custom-call(bf16[2048,2048]{1,0:T(8,128)(2,1)} %saved.1, bf16[2048,2048]{1,0:T(8,128)(2,1)} %grad.1, bf16[2048,256]{1,0:T(8,128)(2,1)} %qb.3, bf16[2048,256]{1,0:T(8,128)(2,1)} %fb.3, bf16[2048,256]{1,0:T(8,128)(2,1)} %ob.3, bf16[2048,256]{1,0:T(8,128)(2,1)} %qc.1, bf16[2048,256]{1,0:T(8,128)(2,1)} %fc.1, ...), custom_call_target="tpu_custom_call" | custom-call | flops 7247757312 | bytes 23068672 | tf_op jit(solution)/shard_map/project/pallas_call | solution.py:61
  31.5 17.9 %all_to_all.10.arrived = bf16[16,48,256]{2,1,0:T(8,128)(2,1)} all-to-all(bf16[16,48,256]{2,1,0:T(8,128)(2,1)} %project.1), channel_id=1, replica_groups=mesh['fs_0'=4,'fs_1'=4,'tp_0'=4,'tp_1'=2] {'fs_0','fs_1'}, dimensions={0} | all-to-all | bytes 786432 | tf_op jit(solution)/shard_map/all_to_all | solution.py:213
  49.4 1.9 %moments.1 = (f32[16,256]{1,0:T(8,128)}, f32[16,256]{1,0:T(8,128)}, f32[16,256]{1,0:T(8,128)}, f32[16,256]{1,0:T(8,128)}, f32[16,256]{1,0:T(8,128)}, /*index=5*/f32[16,256]{1,0:T(8,128)}, bf16[16,48,256]{2,1,0:T(8,128)(2,1)}) custom-call(bf16[16,48,256]{2,1,0:T(8,128)(2,1)} %all_to_all.10.arrived, f32[16,256]{1,0:T(8,128)} %refs_0_.1, f32[16,256]{1,0:T(8,128)} %refs_1_.1, ...), custom_call_target="tpu_custom_call" | custom-call | flops 4194304 | bytes 1048576 | tf_op jit(solution)/shard_map/moments/pallas_call | solution.py:101
  51.3 15.2 %all_to_all.11.gathered = bf16[16,48,256]{2,1,0:T(8,128)(2,1)} all-to-all(bf16[16,48,256]{2,1,0:T(8,128)(2,1)} %get-tuple-element.25), channel_id=1, replica_groups=mesh['fs_0'=4,'fs_1'=4,'tp_0'=4,'tp_1'=2] {'fs_0','fs_1'}, dimensions={0} | all-to-all | bytes 786432 | tf_op jit(solution)/shard_map/all_to_all | solution.py:215
  66.4 1.8 %squares.1 = f32[8,128]{1,0:T(8,128)} custom-call(bf16[16,48,256]{2,1,0:T(8,128)(2,1)} %all_to_all.11.gathered), custom_call_target="tpu_custom_call" | custom-call | flops 4194304 | bytes 524288 | tf_op jit(solution)/shard_map/squares/pallas_call | solution.py:120
  68.3 1.6 %collective-permute-start = (f32[8,128]{1,0:T(8,128)}, f32[8,128]{1,0:T(8,128)S(1)}, u32[]{:S(2)}, u32[]{:S(2)}) collective-permute-start(f32[8,128]{1,0:T(8,128)} %squares.1), channel_id=1, source_target_pairs={{0,1},{1,0},{2,3},{3,2},{4,5},{5,4},{6,7},{7,6},{8,9},{9,8},{10,11... | collective-permute-start | bytes 12296 | tf_op jit(solution)/shard_map/ppermute | solution.py:181
  69.9 1.0 %collective-permute-done = f32[8,128]{1,0:T(8,128)S(1)} collective-permute-done((f32[8,128]{1,0:T(8,128)}, f32[8,128]{1,0:T(8,128)S(1)}, u32[]{:S(2)}, u32[]{:S(2)}) %collective-permute-start) | collective-permute-done | bytes 4128 | tf_op jit(solution)/shard_map/ppermute | solution.py:181
  70.9 0.7 add.13
  71.6 1.2 %collective-permute-start.1 = (f32[8,128]{1,0:T(8,128)S(1)}, f32[8,128]{1,0:T(8,128)S(1)}, u32[]{:S(2)}, u32[]{:S(2)}) collective-permute-start(f32[8,128]{1,0:T(8,128)S(1)} %add.13), channel_id=1, source_target_pairs={{0,2},{2,0},{4,6},{6,4},{1,3},{3,1},{5,7},{7,5},{8,10},{10,8},{12,... | collective-permute-start | bytes 12296 | tf_op jit(solution)/shard_map/ppermute | solution.py:181
  72.8 1.2 %collective-permute-done.1 = f32[8,128]{1,0:T(8,128)S(1)} collective-permute-done((f32[8,128]{1,0:T(8,128)S(1)}, f32[8,128]{1,0:T(8,128)S(1)}, u32[]{:S(2)}, u32[]{:S(2)}) %collective-permute-start.1) | collective-permute-done | bytes 4128 | tf_op jit(solution)/shard_map/ppermute | solution.py:181
  74.0 2.7 %collective-permute-start.2 = (f32[8,128]{1,0:T(8,128)S(1)}, f32[8,128]{1,0:T(8,128)S(1)}, u32[]{:S(2)}, u32[]{:S(2)}) collective-permute-start(f32[8,128]{1,0:T(8,128)S(1)} %add.14), channel_id=1, source_target_pairs={{0,4},{2,6},{4,0},{6,2},{1,5},{3,7},{5,1},{7,3},{8,12},{10,14},{12... | collective-permute-start | bytes 12296 | tf_op jit(solution)/shard_map/ppermute | solution.py:181
  76.8 1.2 %collective-permute-done.2 = f32[8,128]{1,0:T(8,128)S(1)} collective-permute-done((f32[8,128]{1,0:T(8,128)S(1)}, f32[8,128]{1,0:T(8,128)S(1)}, u32[]{:S(2)}, u32[]{:S(2)}) %collective-permute-start.2) | collective-permute-done | bytes 4128 | tf_op jit(solution)/shard_map/ppermute | solution.py:181
  78.0 0.6 add.15.totals
  78.6 0.0 all-gather.2.cloned.1.call-done.weights
  78.6 9.7 %expand.1 = (f32[128,256]{1,0:T(8,128)}, f32[128,256]{1,0:T(8,128)}, f32[128,256]{1,0:T(8,128)}, bf16[2048,256]{1,0:T(8,128)(2,1)}, bf16[2048,256]{1,0:T(8,128)(2,1)}, /*index=5*/bf16[2048,256]{1,0:T(8,128)(2,1)}) custom-call(s32[1]{0:T(128)} %bitcast.me, f32[8,128]{1,0:T(8,128)} %add.15.totals, bf16[16,48,256]{2,1,0:T(8,128)(2,1)} %all_to_all.11.gathered, ...), custom_call_target="tpu_custom_call" | custom-call | flops 805306368 | bytes 9437184 | tf_op jit(solution)/shard_map/expand/pallas_call | solution.py:152
  (1 shorter events, 0.0 us)
Async XLA Ops:
  7.2 71.4 %all-gather.2.cloned.1.call-start = ((), (), s32[]{:S(2)}) async-start(), calls=%async_computation.2 | async-start | bytes 3342336 | tf_op jit(solution)/shard_map/all_gather | solution.py:205
  68.3 2.6 %collective-permute-start = (f32[8,128]{1,0:T(8,128)}, f32[8,128]{1,0:T(8,128)S(1)}, u32[]{:S(2)}, u32[]{:S(2)}) collective-permute-start(f32[8,128]{1,0:T(8,128)} %squares.1), channel_id=1, source_target_pairs={{0,1},{1,0},{2,3},{3,2},{4,5},{5,4},{6,7},{7,6},{8,9},{9,8},{10,11... | collective-permute-start | bytes 12296 | tf_op jit(solution)/shard_map/ppermute | solution.py:181
  71.6 2.5 %collective-permute-start.1 = (f32[8,128]{1,0:T(8,128)S(1)}, f32[8,128]{1,0:T(8,128)S(1)}, u32[]{:S(2)}, u32[]{:S(2)}) collective-permute-start(f32[8,128]{1,0:T(8,128)S(1)} %add.13), channel_id=1, source_target_pairs={{0,2},{2,0},{4,6},{6,4},{1,3},{3,1},{5,7},{7,5},{8,10},{10,8},{12,... | collective-permute-start | bytes 12296 | tf_op jit(solution)/shard_map/ppermute | solution.py:181
  74.0 4.0 %collective-permute-start.2 = (f32[8,128]{1,0:T(8,128)S(1)}, f32[8,128]{1,0:T(8,128)S(1)}, u32[]{:S(2)}, u32[]{:S(2)}) collective-permute-start(f32[8,128]{1,0:T(8,128)S(1)} %add.14), channel_id=1, source_target_pairs={{0,4},{2,6},{4,0},{6,2},{1,5},{3,7},{5,1},{7,3},{8,12},{10,14},{12... | collective-permute-start | bytes 12296 | tf_op jit(solution)/shard_map/ppermute | solution.py:181
Sparse Core Ops, SparseCore 0:
  10.8 54.1 all-gather.1

commit v2 on v1

v2 whole, which is shorter than its diff:
```python
import functools

import jax
import jax.numpy as jnp
from jax import lax
from jax.experimental import pallas as pl
from jax.experimental.pallas import tpu as pltpu
from jax.sharding import Mesh
from jax.sharding import PartitionSpec as P

WIDTH = 2048
RANK = 256
FS = ("fs_0", "fs_1")
TP = ("tp_0", "tp_1")
MATS = 3
IN_CUTS = (0, 512, 2048)
OUT_CUTS = (0, 512, 2048)
SIDE = 4
SMALL_GRANT = 24 * 1024 * 1024
REDUCE_GRANT = 56 * 1024 * 1024
MOMENT_GRANT = 60 * 1024 * 1024
LARGE_GRANT = 60 * 1024 * 1024

F32 = jnp.float32
BF16 = jnp.bfloat16

FAR = ((0, 0), (2, 0), (0, 2), (2, 2))
NEAR = ((0, 0), (1, 0), (0, 1), (3, 3))


def cost(flops, moved):
    return pl.CostEstimate(flops=flops, bytes_accessed=moved, transcendentals=0)


def params(grant=SMALL_GRANT):
    return pltpu.CompilerParams(vmem_limit_bytes=grant)


def round_kernel(*refs):
    out = refs[MATS]
    cols = refs[0].shape[1]
    for m in range(MATS):
        out[:, m * cols : (m + 1) * cols] = refs[m][...].astype(BF16)


def rounded(weights):
    rows, cols = weights[0].shape
    return pl.pallas_call(
        round_kernel,
        out_shape=jax.ShapeDtypeStruct((rows, MATS * cols), BF16),
        compiler_params=params(LARGE_GRANT),
        cost_estimate=cost(1 << 20, 1 << 19),
        name="rounded",
    )(*weights)


def reduce_kernel(count, cuts, core, source, *refs):
    bases, out = refs[:count], refs[count]
    rows_in, basis_in, sums, sems = refs[count + 1 :]
    half = out.shape[0]
    mine = pl.ds(pl.multiple_of(core[0] * half, half), half)
    copies = []
    for c, (low, high) in enumerate(zip(cuts, cuts[1:])):
        at = slice(low, high)
        pieces = [(source.at[mine, at], rows_in.at[:, at])]
        pieces += [(bases[m].at[at, :], basis_in.at[m, at, :]) for m in range(count)]
        copies.append(
            [pltpu.make_async_copy(a, b, sems.at[c, p]) for p, (a, b) in enumerate(pieces)]
        )
        for copy in copies[-1]:
            copy.start()
    for c, (low, high) in enumerate(zip(cuts, cuts[1:])):
        at = slice(low, high)
        for copy in copies[c]:
            copy.wait()
        for m in range(count):
            to = slice(m * RANK, (m + 1) * RANK)
            part = jnp.dot(rows_in[:, at], basis_in[m, at, :], preferred_element_type=F32)
            if c > 0:
                part = sums[:, to] + part
            if c < len(cuts) - 2:
                sums[:, to] = part
            else:
                out[:, to] = part.astype(BF16)


def reduce_half(core, source, bases, cuts):
    tokens, width = source.shape
    half, count = tokens // 2, len(bases)
    anywhere = pl.BlockSpec(memory_space=pl.ANY)
    return pl.pallas_call(
        functools.partial(reduce_kernel, count, cuts),
        in_specs=[
            pl.BlockSpec(memory_space=pltpu.SMEM),
            *(anywhere for _ in range(1 + count)),
        ],
        out_specs=pl.BlockSpec(memory_space=pltpu.VMEM),
        scratch_shapes=[
            pltpu.VMEM((half, width), BF16),
            pltpu.VMEM((count, width, RANK), BF16),
            pltpu.VMEM((half, count * RANK), F32),
            pltpu.SemaphoreType.DMA((len(cuts) - 1, 1 + count)),
        ],
        out_shape=jax.ShapeDtypeStruct((half, count * RANK), BF16),
        compiler_params=params(REDUCE_GRANT),
        cost_estimate=cost(2 * half * RANK * width * count, 6 << 20),
    )(core, source, *bases)


def contract_rows(left, right):
    return lax.dot_general(
        left, right, (((0,), (0,)), ((), ())), preferred_element_type=F32
    )


def contract_near_kernel(core, own, other, own_out, qc, fc, mixed, out):
    half = own.shape[0]
    mine = pl.ds(pl.multiple_of(core[0] * half, half), half)
    theirs = pl.ds(pl.multiple_of((1 - core[0]) * half, half), half)
    for m, cotangent in enumerate((qc, fc)):
        at = slice(m * RANK, (m + 1) * RANK)
        out[m] = contract_rows(own[:, at], cotangent[mine, :]) + contract_rows(
            other[:, at], cotangent[theirs, :]
        )
    out[2] = contract_rows(own_out[...], mixed[mine, :])


def contract_far_kernel(core, sums, other_out, mixed, out):
    half = other_out.shape[0]
    theirs = pl.ds(pl.multiple_of((1 - core[0]) * half, half), half)
    groups, rows = out.shape[0], out.shape[1] // MATS
    last = sums[2] + contract_rows(other_out[...], mixed[theirs, :])
    for m, total in enumerate((sums[0], sums[1], last)):
        out[:, m * rows : (m + 1) * rows, :] = total.astype(BF16).reshape(
            groups, rows, total.shape[1]
        )


def contract(core, own, other, own_out, other_out, cotangents, groups):
    cols = cotangents[0].shape[1]
    half = own.shape[0]
    smem = pl.BlockSpec(memory_space=pltpu.SMEM)
    vmem = pl.BlockSpec(memory_space=pltpu.VMEM)
    sums = pl.pallas_call(
        contract_near_kernel,
        in_specs=[smem, *(vmem for _ in range(6))],
        out_specs=vmem,
        out_shape=jax.ShapeDtypeStruct((MATS, RANK, cols), F32),
        compiler_params=params(),
        cost_estimate=cost(5 * 2 * half * RANK * cols, 6 << 20),
        name="contract_near",
    )(core, own, other, own_out, *cotangents)
    return pl.pallas_call(
        contract_far_kernel,
        in_specs=[smem, *(vmem for _ in range(3))],
        out_specs=vmem,
        out_shape=jax.ShapeDtypeStruct((groups, MATS * (RANK // groups), cols), BF16),
        compiler_params=params(),
        cost_estimate=cost(2 * half * RANK * cols, 1 << 20),
        name="contract_far",
    )(core, sums, other_out, cotangents[2])


def moment_kernel(arrived, *refs):
    state, state_new = refs[: 2 * MATS], refs[2 * MATS : 4 * MATS]
    directions, held, sems = refs[4 * MATS :]
    groups = arrived.shape[0]
    rows = arrived.shape[1] // MATS
    copies = [
        pltpu.make_async_copy(state[n], held.at[n], sems.at[n]) for n in range(2 * MATS)
    ]
    for copy in copies:
        copy.start()
    projected = arrived[0].astype(F32)
    for g in range(1, groups):
        projected = projected + arrived[g].astype(F32)
    for copy in copies:
        copy.wait()
    for m in range(MATS):
        at = slice(m * rows, (m + 1) * rows)
        value = projected[at]
        first_new = 0.8 * held[m] + 0.2 * value
        second_new = 0.95 * held[MATS + m] + 0.05 * value * value
        state_new[m][...] = first_new
        state_new[MATS + m][...] = second_new
        direction = (first_new / (jnp.sqrt(second_new) + 1e-08)).astype(BF16)
        for g in range(groups):
            directions[g, at, :] = direction


def moments(arrived, state):
    vmem = pl.BlockSpec(memory_space=pltpu.VMEM)
    anywhere = pl.BlockSpec(memory_space=pl.ANY)
    results = pl.pallas_call(
        moment_kernel,
        in_specs=[vmem, *(anywhere for _ in state)],
        out_specs=[vmem for _ in range(1 + len(state))],
        out_shape=[
            *(jax.ShapeDtypeStruct(a.shape, F32) for a in state),
            jax.ShapeDtypeStruct(arrived.shape, BF16),
        ],
        scratch_shapes=[
            pltpu.VMEM((len(state), *state[0].shape), F32),
            pltpu.SemaphoreType.DMA((len(state),)),
        ],
        compiler_params=params(MOMENT_GRANT),
        cost_estimate=cost(1 << 22, 1 << 20),
        name="moments",
    )(arrived, *state)
    return results[: len(state)], results[len(state)]


def square_kernel(gathered, out):
    rows = gathered.shape[1] // MATS
    out[...] = jnp.zeros_like(out)
    for m in range(MATS):
        values = gathered[:, m * rows : (m + 1) * rows, :].astype(F32)
        total = jnp.sum(values * values)
        out[m : m + 1, :] = jnp.full((1, out.shape[1]), total, F32)


def squares(gathered):
    return pl.pallas_call(
        square_kernel,
        out_shape=jax.ShapeDtypeStruct((8, 128), F32),
        compiler_params=params(),
        cost_estimate=cost(1 << 22, 1 << 19),
        name="squares",
    )(gathered)


def step_kernel(gathered, qb, fb, ob, out):
    rank_rows, cols = gathered.shape[1] // MATS, gathered.shape[2]
    for m, basis in enumerate((qb, fb, ob)):
        direction = gathered[:, m * rank_rows : (m + 1) * rank_rows, :].reshape(RANK, cols)

        def piece(i, carry):
            at = pl.ds(pl.multiple_of(i * 512, 512), 512)
            out[m, at, :] = jnp.dot(basis[at, :], direction, preferred_element_type=F32)
            return carry

        lax.fori_loop(0, basis.shape[0] // 512, piece, 0)


def steps(gathered, bases):
    width, cols = bases[0].shape[0], gathered.shape[2]
    return pl.pallas_call(
        step_kernel,
        out_shape=jax.ShapeDtypeStruct((MATS, width, cols), F32),
        compiler_params=params(),
        cost_estimate=cost(MATS * 2 * width * RANK * cols, 9 << 20),
        name="steps",
    )(gathered, *bases)


def apply_kernel(me, totals, stepped, *refs):
    weights = refs[: len(NEAR)]
    updates = refs[len(NEAR) : len(NEAR) + MATS]
    copies = refs[len(NEAR) + MATS :]
    rows, cols = updates[0].shape
    scales = [
        lax.rsqrt(totals[m : m + 1, :1] * (1.0 / (RANK * WIDTH)) + 1e-06) for m in range(MATS)
    ]
    mine = pl.ds(pl.multiple_of((me[0] * SIDE + me[1]) * rows, rows), rows)
    for m in range(MATS):
        updates[m][...] = stepped[m, mine, :] * scales[m]

    def block(j, carry):
        far = (2 * lax.rem(j, 2), 2 * lax.div(j, 2))
        for near, weight in zip(NEAR, weights):
            z = lax.rem(me[0] + 2 * SIDE - near[0] - far[0], SIDE)
            y = lax.rem(me[1] + 2 * SIDE - near[1] - far[1], SIDE)
            at = pl.ds(pl.multiple_of((z * SIDE + y) * rows, rows), rows)
            for m in range(MATS):
                old = weight[j, :, m * cols : (m + 1) * cols].astype(F32)
                new = old - 0.05 * (stepped[m, at, :] * scales[m])
                copies[m][at, :] = new.astype(BF16)
        return carry

    lax.fori_loop(0, len(FAR), block, 0)


def applied(me, totals, stepped, weights, rows):
    width, cols = stepped.shape[1:]
    smem = pl.BlockSpec(memory_space=pltpu.SMEM)
    vmem = pl.BlockSpec(memory_space=pltpu.VMEM)
    return pl.pallas_call(
        apply_kernel,
        in_specs=[smem, *(vmem for _ in range(2 + len(weights)))],
        out_specs=[vmem for _ in range(2 * MATS)],
        out_shape=[
            *(jax.ShapeDtypeStruct((rows, cols), F32) for _ in range(MATS)),
            *(jax.ShapeDtypeStruct((width, cols), BF16) for _ in range(MATS)),
        ],
        compiler_params=params(),
        cost_estimate=cost(1 << 24, 12 << 20),
        name="applied",
    )(me, totals, stepped, *weights)


def moved_by(value, offset):
    pairs = []
    for z in range(SIDE):
        for y in range(SIDE):
            target = ((z + offset[0]) % SIDE) * SIDE + (y + offset[1]) % SIDE
            pairs.append((z * SIDE + y, target))
    return lax.ppermute(value, FS, pairs)


def gathered_by(value, offsets):
    moved = []
    for offset in offsets[1:]:
        moved.append(moved_by(value, offset))
    return moved


def summed_over_tp(value):
    value = value + lax.ppermute(value, "tp_1", [(0, 1), (1, 0)])
    arrived = [
        lax.ppermute(value, "tp_0", [(i, (i + far) % SIDE) for i in range(SIDE)])
        for far in (1, 2, 3)
    ]
    return value + (arrived[0] + arrived[2]) + arrived[1]


def body(
    saved_input,
    query_cotangent,
    forget_cotangent,
    mixed_output,
    out_cotangent,
    query_basis,
    forget_basis,
    out_basis,
    query_weight,
    forget_weight,
    out_weight,
    *state,
):
    rows = query_weight.shape[0]
    groups = lax.axis_size(FS)
    bases = (query_basis, forget_basis, out_basis)
    cotangents = (query_cotangent, forget_cotangent, mixed_output)
    core = lax.axis_index("tp_1").astype(jnp.int32).reshape(1)
    me = jnp.stack([lax.axis_index("fs_0"), lax.axis_index("fs_1")]).astype(jnp.int32)
    swap = [(0, 1), (1, 0)]

    weights = rounded((query_weight, forget_weight, out_weight))
    four = jnp.stack([weights, *gathered_by(weights, FAR)])
    all_weights = (four, *gathered_by(four, NEAR))

    own = reduce_half(core, saved_input, bases[:2], IN_CUTS)
    other = lax.ppermute(own, "tp_1", swap)
    own_out = reduce_half(core, out_cotangent, bases[2:], OUT_CUTS)
    other_out = lax.ppermute(own_out, "tp_1", swap)
    blocks = contract(core, own, other, own_out, other_out, cotangents, groups)

    arrived = lax.all_to_all(blocks, FS, 0, 0, tiled=True)
    state_new, directions = moments(arrived, state)
    gathered = lax.all_to_all(directions, FS, 0, 0, tiled=True)
    totals = summed_over_tp(squares(gathered))
    stepped = steps(gathered, bases)
    outs = applied(me, totals, stepped, all_weights, rows)
    return (*outs[:MATS], *state_new, *outs[MATS:])


def solution(mesh):
    split = Mesh(mesh.devices.reshape(4, 4, 4, 2), ("fs_0", "fs_1", "tp_0", "tp_1"))
    in_specs = (
        P(FS, None),
        P(FS, TP),
        P(FS, TP),
        P(FS, TP),
        P(FS, None),
        P(),
        P(),
        P(),
        *(P(FS, TP) for _ in range(9)),
    )
    out_specs = (*(P(FS, TP) for _ in range(9)), *(P(None, TP) for _ in range(3)))
    return jax.shard_map(body, mesh=split, in_specs=in_specs, out_specs=out_specs, check_vma=False)
```

time: 97 us -> 89 us (0.918)
  starting transfers between devices: 5.59 us -> 24.9 us
  blocking collectives: 33.1 us -> 19.3 us
  between operations: 14 us -> 0.86 us
  waiting for transfers between devices: 3.52 us -> 13.1 us
  Pallas kernels: 34.2 us -> 25.4 us
  other arithmetic: 4.71 us -> 1.99 us
  local copies, waits for them, and re-layouts: 0 us -> 1.97 us
    all_to_all x2 -> x1, blocking collectives: 33.1 us -> 19.3 us  [body(): gathered = lax.all_to_all(directions, FS, 0, 0, tiled=True)]
    ppermute x3 -> x12, starting transfers between devices: 5.55 us -> 17 us  [the longest x6 8.31 us: moved_by(): return lax.ppermute(value, FS, pairs)]
    ppermute x3 -> x12, waiting for transfers between devices: 3.5 us -> 13.1 us  [the longest x6 12 us: moved_by(): return lax.ppermute(value, FS, pairs)]
    all_to_all x0 -> x1, starting transfers between devices: none -> 7.88 us  [body(): arrived = lax.all_to_all(blocks, FS, 0, 0, tiled=True)]
    pallas_call x3 -> x8, Pallas kernels: 32.4 us -> 25.2 us  [the longest x2 10.3 us: reduce_half(): pl.pallas_call(functools.partial(reduce_kernel, count, cuts), in_specs=[p...]
    convert_element_type x3 -> x0, other arithmetic: 2.74 us -> none  [local(): w.astype(BF16)]
    another operation x0 -> x2, other arithmetic: none -> 1.98 us  [the longest x1 1.91 us: body(): four = jnp.stack([weights, *gathered_by(weights, FAR)])]
    unnamed x0 -> x18, local copies, waits for them, and re-layouts: none -> 1.97 us
  transfers between devices with their start and end apart: 4 -> 13, of which waited for: 3 -> 5; matrix products, arithmetic and copies ran while one was open for 1% -> 2% of each run, Pallas kernels for 26% -> 16%
where the time goes in v2:
time: 89 us; the launch traced here: 87.6 us
  Pallas kernels  25.4 us (29%)
  starting transfers between devices  24.9 us (28%)
  blocking collectives  19.3 us (22%)
  waiting for transfers between devices  13.1 us (15%)
  other arithmetic  1.99 us (2%)
  local copies, waits for them, and re-layouts  1.97 us (2%)
    all_to_all x1, blocking collectives, body(): gathered = lax.all_to_all(directions, FS, 0, 0, tiled=True)  19.3 us
    ppermute x6, waiting for transfers between devices, moved_by(): return lax.ppermute(value, FS, pairs)  12 us
    pallas_call x2, Pallas kernels, reduce_half(): pl.pallas_call(functools.partial(reduce_kernel, count, cuts), in_specs=[p...  10.3 us
    ppermute x6, starting transfers between devices, moved_by(): return lax.ppermute(value, FS, pairs)  8.31 us
    all_to_all x1, starting transfers between devices, body(): arrived = lax.all_to_all(blocks, FS, 0, 0, tiled=True)  7.88 us
    ppermute x3, starting transfers between devices, summed_over_tp(): lax.ppermute(value, 'tp_0', [(i, (i + far) % SIDE) for i in range(SIDE)])  4.81 us
    pallas_call x1, Pallas kernels, applied(): pl.pallas_call(apply_kernel, in_specs=[smem, *(vmem for _ in range(2 + le...  4.61 us
    pallas_call x1, Pallas kernels, steps(): pl.pallas_call(step_kernel, out_shape=jax.ShapeDtypeStruct((MATS, width,...  2.73 us
  transfers between devices with their start and end apart: 13, of which 5 were waited for; matrix products, arithmetic and copies ran while one was open for 2% of the time, Pallas kernels for 16%

profile of v2, /device:TPU:1, one launch (start us, length us, event | category | flops | bytes accessed | tf_op | source)
XLA Modules:
  0.0 87.6 jit_solution(2822837329803564479)
XLA Ops:
  0.7 5.8 %shard_map.256.own = bf16[1024,512]{1,0:T(8,128)(2,1)} custom-call(s32[1]{0:T(128)} %bitcast.2.core, bf16[2048,2048]{1,0:T(8,128)(2,1)} %source.2, bf16[2048,256]{1,0:T(8,128)(2,1)} %qb.1, bf16[2048,256]{1,0:T(8,128)(2,1)} %fb.1), custom_call_target="tpu_custom_call" | custom-call | flops 2147483648 | bytes 6291456 | tf_op jit(solution)/shard_map/pallas_call | solution.py:91
  6.5 1.5 %collective-permute-start = (bf16[1024,512]{1,0:T(8,128)(2,1)}, bf16[1024,512]{1,0:T(8,128)(2,1)}, u32[]{:S(2)}, u32[]{:S(2)}) collective-permute-start(bf16[1024,512]{1,0:T(8,128)(2,1)} %shard_map.256.own), channel_id=1, source_target_pairs={{0,1},{1,0},{2,3},{3,2},{4,5},{5,4},{6,7},{7,6},{8,9},{9,8},{10,11... | collective-permute-start | bytes 3145736 | tf_op jit(solution)/shard_map/ppermute | solution.py:353
  7.9 4.5 %shard_map.257.own_out = bf16[1024,256]{1,0:T(8,128)(2,1)} custom-call(s32[1]{0:T(128)} %bitcast.2.core, bf16[2048,2048]{1,0:T(8,128)(2,1)} %source.3, bf16[2048,256]{1,0:T(8,128)(2,1)} %ob.1), custom_call_target="tpu_custom_call" | custom-call | flops 1073741824 | bytes 6291456 | tf_op jit(solution)/shard_map/pallas_call | solution.py:91
  12.7 1.2 %copy-done.5 = bf16[1024,256]{1,0:T(8,128)(2,1)S(1)} copy-done((bf16[1024,256]{1,0:T(8,128)(2,1)S(1)}, bf16[1024,256]{1,0:T(8,128)(2,1)}, u32[]{:S(2)}) %copy-start.5) | copy-done | bytes 524312
  13.9 2.1 %contract_near.1.sums = f32[3,256,256]{2,1,0:T(8,128)S(1)} custom-call(s32[1]{0:T(128)} %bitcast.2.core, bf16[1024,512]{1,0:T(8,128)(2,1)S(1)} %copy-done.3, bf16[1024,512]{1,0:T(8,128)(2,1)} %collective-permute-done.other, bf16[1024,256]{1,0:T(8,128)(2,1)S(1)} %copy-done.5, bf16[2048,256]{1,0:T(8,128)(2,1)S(1)} %copy-done.6, ...), custom_call_target="tpu_custom_call" | custom-call | flops 671088640 | bytes 6291456 | tf_op jit(solution)/shard_map/contract_near/pallas_call | solution.py:144
  16.0 1.1 %contract_far.1 = bf16[16,48,256]{2,1,0:T(8,128)(2,1)} custom-call(s32[1]{0:T(128)} %bitcast.2.core, f32[3,256,256]{2,1,0:T(8,128)S(1)} %contract_near.1.sums, bf16[1024,256]{1,0:T(8,128)(2,1)S(1)} %collective-permute-done.1.other_out, bf16[2048,256]{1,0:T(8,128)(2,1)S(1)} %copy-done.4), custom_call_target="tpu_custom_call" | custom-call | flops 134217728 | bytes 1048576 | tf_op jit(solution)/shard_map/contract_far/pallas_call | solution.py:153
  17.1 7.9 %all-to-all-start = ((bf16[16,48,256]{2,1,0:T(8,128)(2,1)}), bf16[16,48,256]{2,1,0:T(8,128)(2,1)S(1)}, u32[]{:S(2)}, u32[]{:S(2)}) async-start(bf16[16,48,256]{2,1,0:T(8,128)(2,1)} %contract_far.1), calls=%async_computation | async-start | bytes 786432 | tf_op jit(solution)/shard_map/all_to_all | solution.py:358
  25.0 1.7 %rounded.1 = bf16[128,768]{1,0:T(8,128)(2,1)} custom-call(f32[128,256]{1,0:T(8,128)} %refs_0_.7, f32[128,256]{1,0:T(8,128)} %refs_1_.5, f32[128,256]{1,0:T(8,128)} %refs_2_.3), custom_call_target="tpu_custom_call" | custom-call | flops 1048576 | bytes 524288 | tf_op jit(solution)/shard_map/rounded/pallas_call | solution.py:48
  26.7 5.3 %collective-permute-start.8 = (bf16[128,768]{1,0:T(8,128)(2,1)}, bf16[128,768]{1,0:T(8,128)(2,1)S(1)}, u32[]{:S(2)}, u32[]{:S(2)}) collective-permute-start(bf16[128,768]{1,0:T(8,128)(2,1)} %rounded.1), channel_id=1, source_target_pairs={{0,80},{8,88},{16,64},{24,72},{32,112},{40,120},{48,96},{56,104},{... | collective-permute-start | bytes 589832 | tf_op jit(solution)/shard_map/ppermute | solution.py:307
  32.4 6.5 %collective-permute-done.8 = bf16[128,768]{1,0:T(8,128)(2,1)S(1)} collective-permute-done((bf16[128,768]{1,0:T(8,128)(2,1)}, bf16[128,768]{1,0:T(8,128)(2,1)S(1)}, u32[]{:S(2)}, u32[]{:S(2)}) %collective-permute-start.8) | collective-permute-done | bytes 196640 | tf_op jit(solution)/shard_map/ppermute | solution.py:307
  38.9 1.8 %collective-permute-done.7 = bf16[128,768]{1,0:T(8,128)(2,1)S(1)} collective-permute-done((bf16[128,768]{1,0:T(8,128)(2,1)}, bf16[128,768]{1,0:T(8,128)(2,1)S(1)}, u32[]{:S(2)}, u32[]{:S(2)}) %collective-permute-start.7) | collective-permute-done | bytes 196640 | tf_op jit(solution)/shard_map/ppermute | solution.py:307
  40.7 3.7 %collective-permute-done.6 = bf16[128,768]{1,0:T(8,128)(2,1)S(1)} collective-permute-done((bf16[128,768]{1,0:T(8,128)(2,1)}, bf16[128,768]{1,0:T(8,128)(2,1)S(1)}, u32[]{:S(2)}, u32[]{:S(2)}) %collective-permute-start.6) | collective-permute-done | bytes 196640 | tf_op jit(solution)/shard_map/ppermute | solution.py:307
  44.4 1.9 %pad_maximum_fusion.refs_0_ = bf16[4,128,768]{2,1,0:T(8,128)(2,1)} fusion(bf16[1,128,768]{2,1,0:T(8,128)(2,1)S(1)} %bitcast.8, bf16[1,128,768]{2,1,0:T(8,128)(2,1)S(1)} %bitcast.9, bf16[1,128,768]{2,1,0:T(8,128)(2,1)S(1)} %bitcast.10, bf16[1,128,768]{2,1,0:T(8,128)(2,1)} %bitcast.7), kind=kLoop, calls=%fused_computation | loop fusion | flops 1179648 | bytes 1572864 | tf_op jit(solution)/shard_map/stack | solution.py:349
  46.3 1.8 %collective-permute-start.11 = (bf16[4,128,768]{2,1,0:T(8,128)(2,1)}, bf16[4,128,768]{2,1,0:T(8,128)(2,1)}, u32[]{:S(2)}, u32[]{:S(2)}) collective-permute-start(bf16[4,128,768]{2,1,0:T(8,128)(2,1)} %pad_maximum_fusion.refs_0_), channel_id=1, source_target_pairs={{0,120},{8,96},{16,104},{24,112},{32,24},{40,0},{48,8},{56,16},{64... | collective-permute-start | bytes 2359304 | tf_op jit(solution)/shard_map/ppermute | solution.py:307
  48.9 0.7 copy-done.8
  49.7 2.6 %moments.1 = (f32[16,256]{1,0:T(8,128)}, f32[16,256]{1,0:T(8,128)}, f32[16,256]{1,0:T(8,128)}, f32[16,256]{1,0:T(8,128)}, f32[16,256]{1,0:T(8,128)}, /*index=5*/f32[16,256]{1,0:T(8,128)}, bf16[16,48,256]{2,1,0:T(8,128)(2,1)}) custom-call(bf16[16,48,256]{2,1,0:T(8,128)(2,1)} %copy-done.8, f32[16,256]{1,0:T(8,128)} %refs_0_.6, f32[16,256]{1,0:T(8,128)} %refs_1_.4, ...), custom_call_target="tpu_custom_call" | custom-call | flops 4194304 | bytes 1048576 | tf_op jit(solution)/shard_map/moments/pallas_call | solution.py:194
  52.3 19.3 %all_to_all.10.gathered = bf16[16,48,256]{2,1,0:T(8,128)(2,1)S(1)} all-to-all(bf16[16,48,256]{2,1,0:T(8,128)(2,1)} %get-tuple-element.25), channel_id=1, replica_groups=mesh['fs_0'=4,'fs_1'=4,'tp_0'=4,'tp_1'=2] {'fs_0','fs_1'}, dimensions={0} | all-to-all | bytes 786432 | tf_op jit(solution)/shard_map/all_to_all | solution.py:360
  71.9 2.3 %collective-permute-start.2 = (f32[8,128]{1,0:T(8,128)S(1)}, f32[8,128]{1,0:T(8,128)S(1)}, u32[]{:S(2)}, u32[]{:S(2)}) collective-permute-start(f32[8,128]{1,0:T(8,128)S(1)} %squares.1), channel_id=1, source_target_pairs={{0,1},{1,0},{2,3},{3,2},{4,5},{5,4},{6,7},{7,6},{8,9},{9,8},{10,11... | collective-permute-start | bytes 12296 | tf_op jit(solution)/shard_map/ppermute | solution.py:318
  74.2 0.8 collective-permute-done.2
  75.0 2.7 %collective-permute-start.5 = (f32[8,128]{1,0:T(8,128)S(1)}, f32[8,128]{1,0:T(8,128)S(1)}, u32[]{:S(2)}, u32[]{:S(2)}) collective-permute-start(f32[8,128]{1,0:T(8,128)S(1)} %add.12), channel_id=1, source_target_pairs={{0,4},{2,6},{4,0},{6,2},{1,5},{3,7},{5,1},{7,3},{8,12},{10,14},{12... | collective-permute-start | bytes 12296 | tf_op jit(solution)/shard_map/ppermute | solution.py:320
  77.8 0.9 collective-permute-start.4
  79.0 1.2 %collective-permute-start.3 = (f32[8,128]{1,0:T(8,128)S(1)}, f32[8,128]{1,0:T(8,128)S(1)}, u32[]{:S(2)}, u32[]{:S(2)}) collective-permute-start(f32[8,128]{1,0:T(8,128)S(1)} %add.12), channel_id=1, source_target_pairs={{0,2},{2,4},{4,6},{6,0},{1,3},{3,5},{5,7},{7,1},{8,10},{10,12},{12... | collective-permute-start | bytes 12296 | tf_op jit(solution)/shard_map/ppermute | solution.py:320
  80.2 2.7 %steps.1.stepped = f32[3,2048,256]{2,1,0:T(8,128)S(1)} custom-call(bf16[16,48,256]{2,1,0:T(8,128)(2,1)S(1)} %all_to_all.10.gathered, bf16[2048,256]{1,0:T(8,128)(2,1)S(1)} %copy-done, bf16[2048,256]{1,0:T(8,128)(2,1)S(1)} %copy-done.1, bf16[2048,256]{1,0:T(8,128)(2,1)S(1)} %copy-done.2), custom_call_target="tpu_custom_call" | custom-call | flops 805306368 | bytes 9437184 | tf_op jit(solution)/shard_map/steps/pallas_call | solution.py:247
  83.0 4.6 %applied.1 = (f32[128,256]{1,0:T(8,128)}, f32[128,256]{1,0:T(8,128)}, f32[128,256]{1,0:T(8,128)}, bf16[2048,256]{1,0:T(8,128)(2,1)}, bf16[2048,256]{1,0:T(8,128)(2,1)}, /*index=5*/bf16[2048,256]{1,0:T(8,128)(2,1)}) custom-call(s32[2]{0:T(128)S(1)} %pad_add_fusion.me, f32[8,128]{1,0:T(8,128)S(1)} %add_add_fusion.totals, f32[3,2048,256]{2,1,0:T(8,128)S(1)} %steps.1.stepped, ...), custom_call_target="tpu_custom_call" | custom-call | flops 16777216 | bytes 12582912 | tf_op jit(solution)/shard_map/applied/pallas_call | solution.py:287
  (34 shorter events, 2.0 us)
Async XLA Ops:
  0.6 12.0 %copy-start.4 = (bf16[2048,256]{1,0:T(8,128)(2,1)S(1)}, bf16[2048,256]{1,0:T(8,128)(2,1)}, u32[]{:S(2)}) copy-start(bf16[2048,256]{1,0:T(8,128)(2,1)} %mixed.3) | copy-start | bytes 3145732
  0.7 12.0 %copy-start.6 = (bf16[2048,256]{1,0:T(8,128)(2,1)S(1)}, bf16[2048,256]{1,0:T(8,128)(2,1)}, u32[]{:S(2)}) copy-start(bf16[2048,256]{1,0:T(8,128)(2,1)} %qc.1) | copy-start | bytes 3145732
  0.7 12.0 %copy-start.7 = (bf16[2048,256]{1,0:T(8,128)(2,1)S(1)}, bf16[2048,256]{1,0:T(8,128)(2,1)}, u32[]{:S(2)}) copy-start(bf16[2048,256]{1,0:T(8,128)(2,1)} %fc.1) | copy-start | bytes 3145732
  6.4 6.3 %copy-start.3 = (bf16[1024,512]{1,0:T(8,128)(2,1)S(1)}, bf16[1024,512]{1,0:T(8,128)(2,1)}, u32[]{:S(2)}) copy-start(bf16[1024,512]{1,0:T(8,128)(2,1)} %shard_map.256.own) | copy-start | bytes 3145732
  6.5 6.2 %collective-permute-start = (bf16[1024,512]{1,0:T(8,128)(2,1)}, bf16[1024,512]{1,0:T(8,128)(2,1)}, u32[]{:S(2)}, u32[]{:S(2)}) collective-permute-start(bf16[1024,512]{1,0:T(8,128)(2,1)} %shard_map.256.own), channel_id=1, source_target_pairs={{0,1},{1,0},{2,3},{3,2},{4,5},{5,4},{6,7},{7,6},{8,9},{9,8},{10,11... | collective-permute-start | bytes 3145736 | tf_op jit(solution)/shard_map/ppermute | solution.py:353
  12.5 67.7 %copy-start = (bf16[2048,256]{1,0:T(8,128)(2,1)S(1)}, bf16[2048,256]{1,0:T(8,128)(2,1)}, u32[]{:S(2)}) copy-start(bf16[2048,256]{1,0:T(8,128)(2,1)} %qb.1) | copy-start | bytes 3145732
  12.5 67.7 %copy-start.1 = (bf16[2048,256]{1,0:T(8,128)(2,1)S(1)}, bf16[2048,256]{1,0:T(8,128)(2,1)}, u32[]{:S(2)}) copy-start(bf16[2048,256]{1,0:T(8,128)(2,1)} %fb.1) | copy-start | bytes 3145732
  12.5 67.7 %copy-start.2 = (bf16[2048,256]{1,0:T(8,128)(2,1)S(1)}, bf16[2048,256]{1,0:T(8,128)(2,1)}, u32[]{:S(2)}) copy-start(bf16[2048,256]{1,0:T(8,128)(2,1)} %ob.1) | copy-start | bytes 3145732
  12.5 3.5 %collective-permute-start.1 = (bf16[1024,256]{1,0:T(8,128)(2,1)}, bf16[1024,256]{1,0:T(8,128)(2,1)S(1)}, u32[]{:S(2)}, u32[]{:S(2)}) collective-permute-start(bf16[1024,256]{1,0:T(8,128)(2,1)} %shard_map.257.own_out), channel_id=1, source_target_pairs={{0,1},{1,0},{2,3},{3,2},{4,5},{5,4},{6,7},{7,6},{8,9},{9,8},{10,11... | collective-permute-start | bytes 1572872 | tf_op jit(solution)/shard_map/ppermute | solution.py:355
  12.7 1.2 %copy-start.5 = (bf16[1024,256]{1,0:T(8,128)(2,1)S(1)}, bf16[1024,256]{1,0:T(8,128)(2,1)}, u32[]{:S(2)}) copy-start(bf16[1024,256]{1,0:T(8,128)(2,1)} %shard_map.257.own_out) | copy-start | bytes 1572868
  17.1 31.8 %all-to-all-start = ((bf16[16,48,256]{2,1,0:T(8,128)(2,1)}), bf16[16,48,256]{2,1,0:T(8,128)(2,1)S(1)}, u32[]{:S(2)}, u32[]{:S(2)}) async-start(bf16[16,48,256]{2,1,0:T(8,128)(2,1)} %contract_far.1), calls=%async_computation | async-start | bytes 786432 | tf_op jit(solution)/shard_map/all_to_all | solution.py:358
  26.7 12.1 %collective-permute-start.8 = (bf16[128,768]{1,0:T(8,128)(2,1)}, bf16[128,768]{1,0:T(8,128)(2,1)S(1)}, u32[]{:S(2)}, u32[]{:S(2)}) collective-permute-start(bf16[128,768]{1,0:T(8,128)(2,1)} %rounded.1), channel_id=1, source_target_pairs={{0,80},{8,88},{16,64},{24,72},{32,112},{40,120},{48,96},{56,104},{... | collective-permute-start | bytes 589832 | tf_op jit(solution)/shard_map/ppermute | solution.py:307
  32.0 8.6 %collective-permute-start.7 = (bf16[128,768]{1,0:T(8,128)(2,1)}, bf16[128,768]{1,0:T(8,128)(2,1)S(1)}, u32[]{:S(2)}, u32[]{:S(2)}) collective-permute-start(bf16[128,768]{1,0:T(8,128)(2,1)} %rounded.1), channel_id=1, source_target_pairs={{0,16},{8,24},{16,0},{24,8},{32,48},{40,56},{48,32},{56,40},{64,80... | collective-permute-start | bytes 589832 | tf_op jit(solution)/shard_map/ppermute | solution.py:307
  32.3 12.1 %collective-permute-start.6 = (bf16[128,768]{1,0:T(8,128)(2,1)}, bf16[128,768]{1,0:T(8,128)(2,1)S(1)}, u32[]{:S(2)}, u32[]{:S(2)}) collective-permute-start(bf16[128,768]{1,0:T(8,128)(2,1)} %rounded.1), channel_id=1, source_target_pairs={{0,64},{8,72},{16,80},{24,88},{32,96},{40,104},{48,112},{56,120},{... | collective-permute-start | bytes 589832 | tf_op jit(solution)/shard_map/ppermute | solution.py:307
  46.3 36.7 %collective-permute-start.11 = (bf16[4,128,768]{2,1,0:T(8,128)(2,1)}, bf16[4,128,768]{2,1,0:T(8,128)(2,1)}, u32[]{:S(2)}, u32[]{:S(2)}) collective-permute-start(bf16[4,128,768]{2,1,0:T(8,128)(2,1)} %pad_maximum_fusion.refs_0_), channel_id=1, source_target_pairs={{0,120},{8,96},{16,104},{24,112},{32,24},{40,0},{48,8},{56,16},{64... | collective-permute-start | bytes 2359304 | tf_op jit(solution)/shard_map/ppermute | solution.py:307
  48.1 34.8 %collective-permute-start.10 = (bf16[4,128,768]{2,1,0:T(8,128)(2,1)}, bf16[4,128,768]{2,1,0:T(8,128)(2,1)}, u32[]{:S(2)}, u32[]{:S(2)}) collective-permute-start(bf16[4,128,768]{2,1,0:T(8,128)(2,1)} %pad_maximum_fusion.refs_0_), channel_id=1, source_target_pairs={{0,8},{8,16},{16,24},{24,0},{32,40},{40,48},{48,56},{56,32},{64,72... | collective-permute-start | bytes 2359304 | tf_op jit(solution)/shard_map/ppermute | solution.py:307
  48.3 34.7 %collective-permute-start.9 = (bf16[4,128,768]{2,1,0:T(8,128)(2,1)}, bf16[4,128,768]{2,1,0:T(8,128)(2,1)}, u32[]{:S(2)}, u32[]{:S(2)}) collective-permute-start(bf16[4,128,768]{2,1,0:T(8,128)(2,1)} %pad_maximum_fusion.refs_0_), channel_id=1, source_target_pairs={{0,32},{8,40},{16,48},{24,56},{32,64},{40,72},{48,80},{56,88},{64,... | collective-permute-start | bytes 2359304 | tf_op jit(solution)/shard_map/ppermute | solution.py:307
  48.9 0.7 copy-start.8
  71.9 3.1 %collective-permute-start.2 = (f32[8,128]{1,0:T(8,128)S(1)}, f32[8,128]{1,0:T(8,128)S(1)}, u32[]{:S(2)}, u32[]{:S(2)}) collective-permute-start(f32[8,128]{1,0:T(8,128)S(1)} %squares.1), channel_id=1, source_target_pairs={{0,1},{1,0},{2,3},{3,2},{4,5},{5,4},{6,7},{7,6},{8,9},{9,8},{10,11... | collective-permute-start | bytes 12296 | tf_op jit(solution)/shard_map/ppermute | solution.py:318
  75.0 4.0 %collective-permute-start.5 = (f32[8,128]{1,0:T(8,128)S(1)}, f32[8,128]{1,0:T(8,128)S(1)}, u32[]{:S(2)}, u32[]{:S(2)}) collective-permute-start(f32[8,128]{1,0:T(8,128)S(1)} %add.12), channel_id=1, source_target_pairs={{0,4},{2,6},{4,0},{6,2},{1,5},{3,7},{5,1},{7,3},{8,12},{10,14},{12... | collective-permute-start | bytes 12296 | tf_op jit(solution)/shard_map/ppermute | solution.py:320
  77.8 5.1 %collective-permute-start.4 = (f32[8,128]{1,0:T(8,128)S(1)}, f32[8,128]{1,0:T(8,128)S(1)}, u32[]{:S(2)}, u32[]{:S(2)}) collective-permute-start(f32[8,128]{1,0:T(8,128)S(1)} %add.12), channel_id=1, source_target_pairs={{0,6},{2,0},{4,2},{6,4},{1,7},{3,1},{5,3},{7,5},{8,14},{10,8},{12,... | collective-permute-start | bytes 12296 | tf_op jit(solution)/shard_map/ppermute | solution.py:320
  79.0 4.0 %collective-permute-start.3 = (f32[8,128]{1,0:T(8,128)S(1)}, f32[8,128]{1,0:T(8,128)S(1)}, u32[]{:S(2)}, u32[]{:S(2)}) collective-permute-start(f32[8,128]{1,0:T(8,128)S(1)} %add.12), channel_id=1, source_target_pairs={{0,2},{2,4},{4,6},{6,0},{1,3},{3,5},{5,7},{7,1},{8,10},{10,12},{12... | collective-permute-start | bytes 12296 | tf_op jit(solution)/shard_map/ppermute | solution.py:320

commit v3 on v2

v3 whole, which is shorter than its diff:
```python
import functools

import jax
import jax.numpy as jnp
from jax import lax
from jax.experimental import pallas as pl
from jax.experimental.pallas import tpu as pltpu
from jax.sharding import Mesh
from jax.sharding import PartitionSpec as P

WIDTH = 2048
RANK = 256
FS = ("fs_0", "fs_1")
TP = ("tp_0", "tp_1")
MATS = 3
IN_CUTS = (0, 512, 2048)
OUT_CUTS = (0, 512, 2048)
SIDE = 4
GRANT = 24 * 1024 * 1024

F32 = jnp.float32
BF16 = jnp.bfloat16

FAR = ((0, 0), (2, 0), (0, 2), (2, 2))
NEAR = ((0, 0), (1, 0), (0, 1), (3, 3))


SMEM = pl.BlockSpec(memory_space=pltpu.SMEM)
VMEM = pl.BlockSpec(memory_space=pltpu.VMEM)
HBM = pl.BlockSpec(memory_space=pltpu.HBM)


def cost(flops, moved):
    return pl.CostEstimate(flops=flops, bytes_accessed=moved, transcendentals=0)


def params():
    return pltpu.CompilerParams(vmem_limit_bytes=GRANT)


def in_hbm(*arrays):
    return [pltpu.with_memory_space_constraint(a, pltpu.HBM) for a in arrays]


def in_vmem(*arrays):
    return [pltpu.with_memory_space_constraint(a, pltpu.VMEM) for a in arrays]


def contract_rows(left, right):
    return lax.dot_general(
        left, right, (((0,), (0,)), ((), ())), preferred_element_type=F32
    )


def half_of(which, half):
    return pl.ds(pl.multiple_of(which * half, half), half)


def reduce_in_kernel(core, source, qb, fb, qw, fw, ow, *refs):
    state, (out, rounded, packed) = refs[: 2 * MATS], refs[2 * MATS : 2 * MATS + 3]
    rows_in, basis_in, weights_in, sums, sems, weight_sems, state_sems = refs[2 * MATS + 3 :]
    bases, weights = (qb, fb), (qw, fw, ow)
    mine = half_of(core[0], out.shape[0])
    copies = []
    for c, (low, high) in enumerate(zip(IN_CUTS, IN_CUTS[1:])):
        at = slice(low, high)
        pieces = [(source.at[mine, at], rows_in.at[:, at])]
        pieces += [(b.at[at, :], basis_in.at[m, at, :]) for m, b in enumerate(bases)]
        copies.append(
            [pltpu.make_async_copy(a, b, sems.at[c, p]) for p, (a, b) in enumerate(pieces)]
        )
    weight_copies = [
        pltpu.make_async_copy(w, weights_in.at[m], weight_sems.at[m])
        for m, w in enumerate(weights)
    ]
    state_copies = [
        pltpu.make_async_copy(a, packed.at[n], state_sems.at[n]) for n, a in enumerate(state)
    ]
    for copy in (*copies[0], *weight_copies, *copies[1], *state_copies):
        copy.start()
    for c, (low, high) in enumerate(zip(IN_CUTS, IN_CUTS[1:])):
        at = slice(low, high)
        for copy in copies[c]:
            copy.wait()
        for m in range(len(bases)):
            to = slice(m * RANK, (m + 1) * RANK)
            part = jnp.dot(rows_in[:, at], basis_in[m, at, :], preferred_element_type=F32)
            if c == 0:
                sums[:, to] = part
            else:
                out[:, to] = (sums[:, to] + part).astype(BF16)
        if c == 0:
            cols = weights_in.shape[2]
            for m, copy in enumerate(weight_copies):
                copy.wait()
                rounded[:, m * cols : (m + 1) * cols] = weights_in[m].astype(BF16)
    for copy in state_copies:
        copy.wait()


def reduce_in(core, source, bases, weights, state):
    tokens, width = source.shape
    half, count = tokens // 2, len(bases)
    rows, cols = weights[0].shape
    return pl.pallas_call(
        reduce_in_kernel,
        in_specs=[SMEM, *(HBM for _ in range(1 + count + MATS + len(state)))],
        out_specs=[VMEM, VMEM, VMEM],
        out_shape=[
            pltpu.VMEM((half, count * RANK), BF16),
            pltpu.VMEM((rows, MATS * cols), BF16),
            pltpu.VMEM((len(state), *state[0].shape), F32),
        ],
        scratch_shapes=[
            pltpu.VMEM((half, width), BF16),
            pltpu.VMEM((count, width, RANK), BF16),
            pltpu.VMEM((MATS, rows, cols), F32),
            pltpu.VMEM((half, count * RANK), F32),
            pltpu.SemaphoreType.DMA((len(IN_CUTS) - 1, 1 + count)),
            pltpu.SemaphoreType.DMA((MATS,)),
            pltpu.SemaphoreType.DMA((len(state),)),
        ],
        compiler_params=params(),
        cost_estimate=cost(2 * half * RANK * width * count, 6 << 20),
        name="reduce_in",
    )(core, *in_hbm(source, *bases, *weights, *state))


def reduce_out_kernel(core, own, qc, fc, mixed, source, basis, out, sums, *scratch):
    rows_in, basis_in, total, sems = scratch
    mine = half_of(core[0], out.shape[0])
    copies = []
    for c, (low, high) in enumerate(zip(OUT_CUTS, OUT_CUTS[1:])):
        at = slice(low, high)
        copies.append(
            [
                pltpu.make_async_copy(source.at[mine, at], rows_in.at[:, at], sems.at[c, 0]),
                pltpu.make_async_copy(basis.at[at, :], basis_in.at[at, :], sems.at[c, 1]),
            ]
        )
        for copy in copies[c]:
            copy.start()
    for m, cotangent in enumerate((qc, fc)):
        sums[m] = contract_rows(own[:, m * RANK : (m + 1) * RANK], cotangent[mine, :])
    for c, (low, high) in enumerate(zip(OUT_CUTS, OUT_CUTS[1:])):
        at = slice(low, high)
        for copy in copies[c]:
            copy.wait()
        part = jnp.dot(rows_in[:, at], basis_in[at, :], preferred_element_type=F32)
        if c == 0:
            total[...] = part
        else:
            out[...] = (total[...] + part).astype(BF16)
    sums[2] = contract_rows(out[...], mixed[mine, :])


def reduce_out(core, own, cotangents, source, basis):
    tokens, width = source.shape
    half, cols = tokens // 2, cotangents[0].shape[1]
    return pl.pallas_call(
        reduce_out_kernel,
        in_specs=[SMEM, *(VMEM for _ in range(1 + MATS)), HBM, HBM],
        out_specs=[VMEM, VMEM],
        out_shape=[pltpu.VMEM((half, RANK), BF16), pltpu.VMEM((MATS, RANK, cols), F32)],
        scratch_shapes=[
            pltpu.VMEM((half, width), BF16),
            pltpu.VMEM((width, RANK), BF16),
            pltpu.VMEM((half, RANK), F32),
            pltpu.SemaphoreType.DMA((len(OUT_CUTS) - 1, 2)),
        ],
        compiler_params=params(),
        cost_estimate=cost(2 * half * RANK * (width + 3 * cols), 6 << 20),
        name="reduce_out",
    )(core, *in_vmem(own, *cotangents), *in_hbm(source, basis))


def contract_kernel(picked, core, sums, other, *refs):
    cotangents = refs[: len(picked)]
    out, held, sems = refs[-3:]
    groups, rows = out.shape[0], out.shape[1] // MATS
    theirs = half_of(1 - core[0], other.shape[0])
    copies = []
    for k, (m, cotangent) in enumerate(zip(picked, cotangents)):
        total = sums[m] + contract_rows(
            other[:, k * RANK : (k + 1) * RANK], cotangent[theirs, :]
        )
        held[k] = total.astype(BF16).reshape(groups, rows, total.shape[1])
        copies.append(
            pltpu.make_async_copy(
                held.at[k], out.at[:, m * rows : (m + 1) * rows, :], sems.at[k]
            )
        )
        copies[k].start()
    for copy in copies:
        copy.wait()


def contract(picked, core, sums, other, cotangents, groups, into):
    cols = sums.shape[2]
    rows = RANK // groups
    count = len(picked)
    earlier = [] if into is None else in_hbm(into)
    return pl.pallas_call(
        functools.partial(contract_kernel, picked),
        in_specs=[SMEM, *(VMEM for _ in range(2 + count)), *(HBM for _ in earlier)],
        out_specs=HBM,
        out_shape=pltpu.HBM((groups, MATS * rows, cols), BF16),
        scratch_shapes=[
            pltpu.VMEM((count, groups, rows, cols), BF16),
            pltpu.SemaphoreType.DMA((count,)),
        ],
        input_output_aliases={3 + count: 0} if earlier else {},
        compiler_params=params(),
        cost_estimate=cost(2 * count * other.shape[0] * RANK * cols, count << 20),
    )(core, *in_vmem(sums, other, *(cotangents[m] for m in picked)), *earlier)


def moment_kernel(arrived, held, *refs):
    state_new = refs[: 2 * MATS]
    directions, direction, sems = refs[2 * MATS :]
    groups = arrived.shape[0]
    rows = arrived.shape[1] // MATS
    for m in range(MATS):
        at = slice(m * rows, (m + 1) * rows)
        value = arrived[0, at, :].astype(F32)
        for g in range(1, groups):
            value = value + arrived[g, at, :].astype(F32)
        first_new = 0.8 * held[m] + 0.2 * value
        second_new = 0.95 * held[MATS + m] + 0.05 * value * value
        state_new[m][...] = first_new
        state_new[MATS + m][...] = second_new
        direction[at, :] = (first_new / (jnp.sqrt(second_new) + 1e-08)).astype(BF16)
    sends = [
        pltpu.make_async_copy(direction, directions.at[g], sems.at[g]) for g in range(groups)
    ]
    for send in sends:
        send.start()
    for send in sends:
        send.wait()


def moments(arrived, packed):
    groups, rows, cols = arrived.shape
    count = packed.shape[0]
    results = pl.pallas_call(
        moment_kernel,
        in_specs=[VMEM, VMEM],
        out_specs=[*(VMEM for _ in range(count)), HBM],
        out_shape=[
            *(jax.ShapeDtypeStruct(packed.shape[1:], F32) for _ in range(count)),
            pltpu.HBM(arrived.shape, BF16),
        ],
        scratch_shapes=[
            pltpu.VMEM((rows, cols), BF16),
            pltpu.SemaphoreType.DMA((groups,)),
        ],
        compiler_params=params(),
        cost_estimate=cost(1 << 22, 1 << 20),
        name="moments",
    )(*in_vmem(arrived, packed))
    return results[:count], results[count]


def collect_kernel(*refs):
    for k, block in enumerate(refs[: len(FAR)]):
        refs[len(FAR)][k] = block[...]


def collected(blocks):
    return pl.pallas_call(
        collect_kernel,
        in_specs=[VMEM for _ in blocks],
        out_specs=VMEM,
        out_shape=pltpu.HBM((len(blocks), *blocks[0].shape), BF16),
        compiler_params=params(),
        cost_estimate=cost(1 << 20, 2 << 20),
        name="collected",
    )(*in_vmem(*blocks))


def square_kernel(gathered, out):
    rows = gathered.shape[1] // MATS
    out[...] = jnp.zeros_like(out)
    for m in range(MATS):
        values = gathered[:, m * rows : (m + 1) * rows, :].astype(F32)
        total = jnp.sum(values * values)
        out[m : m + 1, :] = jnp.full((1, out.shape[1]), total, F32)


def squares(gathered):
    return pl.pallas_call(
        square_kernel,
        out_shape=jax.ShapeDtypeStruct((8, 128), F32),
        compiler_params=params(),
        cost_estimate=cost(1 << 22, 1 << 19),
        name="squares",
    )(gathered)


def step_kernel(gathered, qb, fb, ob, out):
    rank_rows, cols = gathered.shape[1] // MATS, gathered.shape[2]
    for m, basis in enumerate((qb, fb, ob)):
        direction = gathered[:, m * rank_rows : (m + 1) * rank_rows, :].reshape(RANK, cols)

        def piece(i, carry):
            at = pl.ds(pl.multiple_of(i * 512, 512), 512)
            out[m, at, :] = jnp.dot(basis[at, :], direction, preferred_element_type=F32)
            return carry

        lax.fori_loop(0, basis.shape[0] // 512, piece, 0)


def steps(gathered, bases):
    width, cols = bases[0].shape[0], gathered.shape[2]
    return pl.pallas_call(
        step_kernel,
        out_shape=jax.ShapeDtypeStruct((MATS, width, cols), F32),
        compiler_params=params(),
        cost_estimate=cost(MATS * 2 * width * RANK * cols, 9 << 20),
        name="steps",
    )(gathered, *bases)


def apply_kernel(me, totals, stepped, *refs):
    weights = refs[: len(NEAR)]
    updates = refs[len(NEAR) : len(NEAR) + MATS]
    copies = refs[len(NEAR) + MATS : len(NEAR) + 2 * MATS]
    stepped_own, held, sems = refs[len(NEAR) + 2 * MATS :]
    rows, cols = stepped_own.shape[1:]
    mine = pl.ds(pl.multiple_of((me[0] * SIDE + me[1]) * rows, rows), rows)
    stores = []
    for m in range(MATS):
        total = totals[m : m + 1, :1]
        scale = lax.rsqrt(total * (1.0 / (RANK * WIDTH)) + 1e-06)
        factor = 0.05 * scale
        stepped_own[m] = stepped[m, mine, :] * scale

        def block(j, carry):
            far_z, far_y = 2 * lax.rem(j, 2), 2 * lax.div(j, 2)
            for near, weight in zip(NEAR, weights):
                z = lax.rem(me[0] + 2 * SIDE - near[0] - far_z, SIDE)
                y = lax.rem(me[1] + 2 * SIDE - near[1] - far_y, SIDE)
                at = pl.ds(pl.multiple_of((z * SIDE + y) * rows, rows), rows)
                old = weight[j, :, m * cols : (m + 1) * cols].astype(F32)
                held[m, at, :] = (old - factor * stepped[m, at, :]).astype(BF16)
            return carry

        lax.fori_loop(0, len(FAR), block, 0)
        stores.append(pltpu.make_async_copy(held.at[m], copies[m], sems.at[m]))
        stores.append(pltpu.make_async_copy(stepped_own.at[m], updates[m], sems.at[MATS + m]))
        stores[-2].start()
        stores[-1].start()
    for store in stores:
        store.wait()


def applied(me, totals, stepped, weights, rows):
    width, cols = stepped.shape[1:]
    return pl.pallas_call(
        apply_kernel,
        in_specs=[SMEM, *(VMEM for _ in range(2 + len(weights)))],
        out_specs=[HBM for _ in range(2 * MATS)],
        out_shape=[
            *(pltpu.HBM((rows, cols), F32) for _ in range(MATS)),
            *(pltpu.HBM((width, cols), BF16) for _ in range(MATS)),
        ],
        scratch_shapes=[
            pltpu.VMEM((MATS, rows, cols), F32),
            pltpu.VMEM((MATS, width, cols), BF16),
            pltpu.SemaphoreType.DMA((2 * MATS,)),
        ],
        compiler_params=params(),
        cost_estimate=cost(1 << 24, 12 << 20),
        name="applied",
    )(me, *in_vmem(totals, stepped, *weights))


def moved_by(value, offset):
    pairs = []
    for z in range(SIDE):
        for y in range(SIDE):
            target = ((z + offset[0]) % SIDE) * SIDE + (y + offset[1]) % SIDE
            pairs.append((z * SIDE + y, target))
    return lax.ppermute(value, FS, pairs)


def gathered_by(value, offsets):
    moved = []
    for offset in offsets[1:]:
        moved.append(moved_by(value, offset))
    return moved


def summed_over_tp(value):
    value = value + lax.ppermute(value, "tp_1", [(0, 1), (1, 0)])
    arrived = [
        lax.ppermute(value, "tp_0", [(i, (i + far) % SIDE) for i in range(SIDE)])
        for far in (1, 2, 3)
    ]
    return value + (arrived[0] + arrived[2]) + arrived[1]


def body(
    saved_input,
    query_cotangent,
    forget_cotangent,
    mixed_output,
    out_cotangent,
    query_basis,
    forget_basis,
    out_basis,
    query_weight,
    forget_weight,
    out_weight,
    *state,
):
    rows = query_weight.shape[0]
    groups = lax.axis_size(FS)
    bases = (query_basis, forget_basis, out_basis)
    cotangents = (query_cotangent, forget_cotangent, mixed_output)
    core = lax.axis_index("tp_1").astype(jnp.int32).reshape(1)
    me = jnp.stack([lax.axis_index("fs_0"), lax.axis_index("fs_1")]).astype(jnp.int32)

    own, weights, packed = reduce_in(
        core, saved_input, bases[:2], (query_weight, forget_weight, out_weight), state
    )
    other = lax.ppermute(own, "tp_1", [(0, 1), (1, 0)])
    own_out, sums = reduce_out(core, own, cotangents, out_cotangent, out_basis)
    other_out = lax.ppermute(own_out, "tp_1", [(0, 1), (1, 0)])
    blocks = contract((0, 1), core, sums, other, cotangents, groups, None)
    blocks = contract((2,), core, sums, other_out, cotangents, groups, blocks)
    four = collected((weights, *gathered_by(weights, FAR)))
    all_weights = (four, *gathered_by(four, NEAR))
    arrived = lax.all_to_all(blocks, FS, 0, 0, tiled=True)
    state_new, directions = moments(arrived, packed)
    gathered = lax.all_to_all(directions, FS, 0, 0, tiled=True)
    totals = summed_over_tp(squares(gathered))
    stepped = steps(gathered, bases)
    outs = applied(me, totals, stepped, all_weights, rows)
    return (*outs[:MATS], *state_new, *outs[MATS:])


def solution(mesh):
    split = Mesh(mesh.devices.reshape(4, 4, 4, 2), ("fs_0", "fs_1", "tp_0", "tp_1"))
    in_specs = (
        P(FS, None),
        P(FS, TP),
        P(FS, TP),
        P(FS, TP),
        P(FS, None),
        P(),
        P(),
        P(),
        *(P(FS, TP) for _ in range(9)),
    )
    out_specs = (*(P(FS, TP) for _ in range(9)), *(P(None, TP) for _ in range(3)))
    return jax.shard_map(body, mesh=split, in_specs=in_specs, out_specs=out_specs, check_vma=False)
```

time: 89 us -> 85.9 us (0.965)
  Pallas kernels: 25.4 us -> 20.9 us
  blocking collectives: 19.3 us -> 21.4 us
  other arithmetic: 1.99 us -> 0.09 us
    pallas_call x7, Pallas kernels: 22.5 us -> 17.9 us  [the longest x1 5.03 us: reduce_in(): pl.pallas_call(reduce_in_kernel, in_specs=[SMEM, *(HBM for _ in range(1 +...]
    all_to_all x1, blocking collectives: 19.3 us -> 21.4 us  [body(): gathered = lax.all_to_all(directions, FS, 0, 0, tiled=True)]
    another operation x1 -> x0, other arithmetic: 1.91 us -> none  [body(): four = jnp.stack([weights, *gathered_by(weights, FAR)])]
    unnamed x18 -> x16, local copies, waits for them, and re-layouts: 1.97 us -> 2.48 us
  transfers between devices with their start and end apart: 13 -> 13, of which waited for: 5 -> 6; matrix products, arithmetic and copies ran while one was open for 2% -> 0% of each run, Pallas kernels for 16% -> 13%
where the time goes in v3:
time: 85.9 us; the launch traced here: 85.1 us
  starting transfers between devices  25.6 us (30%)
  blocking collectives  21.4 us (25%)
  Pallas kernels  20.9 us (24%)
  waiting for transfers between devices  13.8 us (16%)
  local copies, waits for them, and re-layouts  2.48 us (3%)
    all_to_all x1, blocking collectives, body(): gathered = lax.all_to_all(directions, FS, 0, 0, tiled=True)  21.4 us
    ppermute x6, waiting for transfers between devices, moved_by(): return lax.ppermute(value, FS, pairs)  12 us
    ppermute x6, starting transfers between devices, moved_by(): return lax.ppermute(value, FS, pairs)  8.89 us
    all_to_all x1, starting transfers between devices, body(): arrived = lax.all_to_all(blocks, FS, 0, 0, tiled=True)  7.89 us
    pallas_call x1, Pallas kernels, reduce_in(): pl.pallas_call(reduce_in_kernel, in_specs=[SMEM, *(HBM for _ in range(1 +...  5.03 us
    ppermute x3, starting transfers between devices, summed_over_tp(): lax.ppermute(value, 'tp_0', [(i, (i + far) % SIDE) for i in range(SIDE)])  4.81 us
    pallas_call x1, Pallas kernels, reduce_out(): pl.pallas_call(reduce_out_kernel, in_specs=[SMEM, *(VMEM for _ in range(1...  4.4 us
    pallas_call x1, Pallas kernels, applied(): pl.pallas_call(apply_kernel, in_specs=[SMEM, *(VMEM for _ in range(2 + le...  3.77 us
  transfers between devices with their start and end apart: 13, of which 6 were waited for; matrix products, arithmetic and copies ran while one was open for 0% of the time, Pallas kernels for 13%

profile of v3, /device:TPU:1, one launch (start us, length us, event | category | flops | bytes accessed | tf_op | source)
XLA Modules:
  0.0 85.1 jit_solution(7357955995369617704)
XLA Ops:
  0.7 5.0 %reduce_in.1 = (bf16[1024,512]{1,0:T(8,128)(2,1)S(1)}, bf16[128,768]{1,0:T(8,128)(2,1)S(1)}, f32[6,16,256]{2,1,0:T(8,128)S(1)}) custom-call(s32[1]{0:T(128)} %bitcast.2.core, bf16[2048,2048]{1,0:T(8,128)(2,1)} %source.2, bf16[2048,256]{1,0:T(8,128)(2,1)} %qb.3, bf16[2048,256]{1,0:T(8,128)(2,1)} %fb.3, f32[128,256]{1,0:T(8,128)} %qw.1, f32[128,256]{1,0:T(8,128)} %fw.1, ...), custom_call_target="tpu_custom_call" | custom-call | flops 2147483648 | bytes 6291456 | tf_op jit(solution)/shard_map/reduce_in/pallas_call | solution.py:105
  5.7 1.5 %collective-permute-start.1 = (bf16[1024,512]{1,0:T(8,128)(2,1)S(1)}, bf16[1024,512]{1,0:T(8,128)(2,1)S(1)}, u32[]{:S(2)}, u32[]{:S(2)}) collective-permute-start(bf16[1024,512]{1,0:T(8,128)(2,1)S(1)} %get-tuple-element.30.own), channel_id=1, source_target_pairs={{0,1},{1,0},{2,3},{3,2},{4,5},{5,4},{6,7},{7,6},{8,9},{9,8},{10,11... | collective-permute-start | bytes 3145736 | tf_op jit(solution)/shard_map/ppermute | solution.py:427
  7.2 4.4 %reduce_out.1 = (bf16[1024,256]{1,0:T(8,128)(2,1)S(1)}, f32[3,256,256]{2,1,0:T(8,128)S(1)}) custom-call(s32[1]{0:T(128)} %bitcast.2.core, bf16[1024,512]{1,0:T(8,128)(2,1)S(1)} %get-tuple-element.30.own, bf16[2048,256]{1,0:T(8,128)(2,1)S(1)} %copy-done, bf16[2048,256]{1,0:T(8,128)(2,1)S(1)} %copy-done.1, bf16[2048,256]{1,0:T(8,128)(2,1)S(1)} %copy-done.5, ...), custom_call_target="tpu_custom_call" | custom-call | flops 1476395008 | bytes 6291456 | tf_op jit(solution)/shard_map/reduce_out/pallas_call | solution.py:160
  11.7 1.2 %shard_map.256.refs_1_ = bf16[16,48,256]{2,1,0:T(8,128)(2,1)} custom-call(s32[1]{0:T(128)} %bitcast.2.core, f32[3,256,256]{2,1,0:T(8,128)S(1)} %get-tuple-element.31.sums, bf16[1024,512]{1,0:T(8,128)(2,1)S(1)} %collective-permute-done.1.other, bf16[2048,256]{1,0:T(8,128)(2,1)S(1)} %copy-done, bf16[2048,256]{1,0:T(8,128)(2,1)S(1)} %copy-done.1), custom_call_target="tpu_custom_call" | custom-call | flops 268435456 | bytes 2097152 | tf_op jit(solution)/shard_map/pallas_call | solution.py:203
  12.9 0.7 collective-permute-done.other
  13.6 1.0 %shard_map.257 = bf16[16,48,256]{2,1,0:T(8,128)(2,1)} custom-call(s32[1]{0:T(128)} %bitcast.2.core, f32[3,256,256]{2,1,0:T(8,128)S(1)} %get-tuple-element.31.sums, bf16[1024,256]{1,0:T(8,128)(2,1)S(1)} %collective-permute-done.other, bf16[2048,256]{1,0:T(8,128)(2,1)S(1)} %copy-done.6, ...), custom_call_target="tpu_custom_call", output_to_operand_aliasing={{}: (4, {})} | custom-call | flops 134217728 | bytes 1048576 | tf_op jit(solution)/shard_map/pallas_call | solution.py:203
  14.6 7.9 %all-to-all-start = ((bf16[16,48,256]{2,1,0:T(8,128)(2,1)}), bf16[16,48,256]{2,1,0:T(8,128)(2,1)S(1)}, u32[]{:S(2)}, u32[]{:S(2)}) async-start(bf16[16,48,256]{2,1,0:T(8,128)(2,1)} %shard_map.257), calls=%async_computation | async-start | bytes 786432 | tf_op jit(solution)/shard_map/all_to_all | solution.py:434
  22.5 5.3 %collective-permute-start.8 = (bf16[128,768]{1,0:T(8,128)(2,1)S(1)}, bf16[128,768]{1,0:T(8,128)(2,1)S(1)}, u32[]{:S(2)}, u32[]{:S(2)}) collective-permute-start(bf16[128,768]{1,0:T(8,128)(2,1)S(1)} %get-tuple-element.35.refs_0_), channel_id=1, source_target_pairs={{0,80},{8,88},{16,64},{24,72},{32,112},{40,120},{48,96},{56,104},{... | collective-permute-start | bytes 589832 | tf_op jit(solution)/shard_map/ppermute | solution.py:384
  28.3 8.5 %collective-permute-done.8.refs_3_ = bf16[128,768]{1,0:T(8,128)(2,1)S(1)} collective-permute-done((bf16[128,768]{1,0:T(8,128)(2,1)S(1)}, bf16[128,768]{1,0:T(8,128)(2,1)S(1)}, u32[]{:S(2)}, u32[]{:S(2)}) %collective-permute-start.8) | collective-permute-done | bytes 196640 | tf_op jit(solution)/shard_map/ppermute | solution.py:384
  36.8 1.8 %collective-permute-done.7.refs_2_ = bf16[128,768]{1,0:T(8,128)(2,1)S(1)} collective-permute-done((bf16[128,768]{1,0:T(8,128)(2,1)S(1)}, bf16[128,768]{1,0:T(8,128)(2,1)S(1)}, u32[]{:S(2)}, u32[]{:S(2)}) %collective-permute-start.7) | collective-permute-done | bytes 196640 | tf_op jit(solution)/shard_map/ppermute | solution.py:384
  38.6 1.7 %collective-permute-done.6.refs_1_ = bf16[128,768]{1,0:T(8,128)(2,1)S(1)} collective-permute-done((bf16[128,768]{1,0:T(8,128)(2,1)S(1)}, bf16[128,768]{1,0:T(8,128)(2,1)S(1)}, u32[]{:S(2)}, u32[]{:S(2)}) %collective-permute-start.6) | collective-permute-done | bytes 196640 | tf_op jit(solution)/shard_map/ppermute | solution.py:384
  40.3 0.9 %collected.1.refs_0_ = bf16[4,128,768]{2,1,0:T(8,128)(2,1)} custom-call(bf16[128,768]{1,0:T(8,128)(2,1)S(1)} %get-tuple-element.35.refs_0_, bf16[128,768]{1,0:T(8,128)(2,1)S(1)} %collective-permute-done.6.refs_1_, bf16[128,768]{1,0:T(8,128)(2,1)S(1)} %collective-permute-done.7.refs_2_, bf16[128,768]{1,0:T(8,128)(2,1)S(1)} %collective-permute-done.8.refs_3_), custom_call_target="tpu_custom_call" | custom-call | flops 1048576 | bytes 2097152 | tf_op jit(solution)/shard_map/collected/pallas_call | solution.py:270
  41.2 2.6 %collective-permute-start.11 = (bf16[4,128,768]{2,1,0:T(8,128)(2,1)}, bf16[4,128,768]{2,1,0:T(8,128)(2,1)S(1)}, u32[]{:S(2)}, u32[]{:S(2)}) collective-permute-start(bf16[4,128,768]{2,1,0:T(8,128)(2,1)} %collected.1.refs_0_), channel_id=1, source_target_pairs={{0,120},{8,96},{16,104},{24,112},{32,24},{40,0},{48,8},{56,16},{64... | collective-permute-start | bytes 2359304 | tf_op jit(solution)/shard_map/ppermute | solution.py:384
  44.4 1.6 %moments.1 = (f32[16,256]{1,0:T(8,128)}, f32[16,256]{1,0:T(8,128)}, f32[16,256]{1,0:T(8,128)}, f32[16,256]{1,0:T(8,128)}, f32[16,256]{1,0:T(8,128)}, /*index=5*/f32[16,256]{1,0:T(8,128)}, bf16[16,48,256]{2,1,0:T(8,128)(2,1)}) custom-call(bf16[16,48,256]{2,1,0:T(8,128)(2,1)S(1)} %all-to-all-done.arrived, f32[6,16,256]{2,1,0:T(8,128)S(1)} %get-tuple-element.33.held), custom_call_target="tpu_custom_call" | custom-call | flops 4194304 | bytes 1048576 | tf_op jit(solution)/shard_map/moments/pallas_call | solution.py:245
  46.0 21.4 %all_to_all.10.gathered = bf16[16,48,256]{2,1,0:T(8,128)(2,1)S(1)} all-to-all(bf16[16,48,256]{2,1,0:T(8,128)(2,1)} %get-tuple-element.34), channel_id=1, replica_groups=mesh['fs_0'=4,'fs_1'=4,'tp_0'=4,'tp_1'=2] {'fs_0','fs_1'}, dimensions={0} | all-to-all | bytes 786432 | tf_op jit(solution)/shard_map/all_to_all | solution.py:436
  67.7 2.4 %collective-permute-start.2 = (f32[8,128]{1,0:T(8,128)S(1)}, f32[8,128]{1,0:T(8,128)S(1)}, u32[]{:S(2)}, u32[]{:S(2)}) collective-permute-start(f32[8,128]{1,0:T(8,128)S(1)} %squares.1), channel_id=1, source_target_pairs={{0,1},{1,0},{2,3},{3,2},{4,5},{5,4},{6,7},{7,6},{8,9},{9,8},{10,11... | collective-permute-start | bytes 12296 | tf_op jit(solution)/shard_map/ppermute | solution.py:395
  70.1 0.8 collective-permute-done.2
  70.9 2.7 %collective-permute-start.5 = (f32[8,128]{1,0:T(8,128)S(1)}, f32[8,128]{1,0:T(8,128)S(1)}, u32[]{:S(2)}, u32[]{:S(2)}) collective-permute-start(f32[8,128]{1,0:T(8,128)S(1)} %add.12), channel_id=1, source_target_pairs={{0,4},{2,6},{4,0},{6,2},{1,5},{3,7},{5,1},{7,3},{8,12},{10,14},{12... | collective-permute-start | bytes 12296 | tf_op jit(solution)/shard_map/ppermute | solution.py:397
  73.7 0.9 %collective-permute-start.4 = (f32[8,128]{1,0:T(8,128)S(1)}, f32[8,128]{1,0:T(8,128)S(1)}, u32[]{:S(2)}, u32[]{:S(2)}) collective-permute-start(f32[8,128]{1,0:T(8,128)S(1)} %add.12), channel_id=1, source_target_pairs={{0,6},{2,0},{4,2},{6,4},{1,7},{3,1},{5,3},{7,5},{8,14},{10,8},{12,... | collective-permute-start | bytes 12296 | tf_op jit(solution)/shard_map/ppermute | solution.py:397
  74.9 1.2 %collective-permute-start.3 = (f32[8,128]{1,0:T(8,128)S(1)}, f32[8,128]{1,0:T(8,128)S(1)}, u32[]{:S(2)}, u32[]{:S(2)}) collective-permute-start(f32[8,128]{1,0:T(8,128)S(1)} %add.12), channel_id=1, source_target_pairs={{0,2},{2,4},{4,6},{6,0},{1,3},{3,5},{5,7},{7,1},{8,10},{10,12},{12... | collective-permute-start | bytes 12296 | tf_op jit(solution)/shard_map/ppermute | solution.py:397
  76.1 1.2 %copy-done.3 = bf16[2048,256]{1,0:T(8,128)(2,1)S(1)} copy-done((bf16[2048,256]{1,0:T(8,128)(2,1)S(1)}, bf16[2048,256]{1,0:T(8,128)(2,1)}, u32[]{:S(2)}) %copy-start.3) | copy-done | bytes 1048600
  77.3 1.2 %copy-done.4 = bf16[2048,256]{1,0:T(8,128)(2,1)S(1)} copy-done((bf16[2048,256]{1,0:T(8,128)(2,1)S(1)}, bf16[2048,256]{1,0:T(8,128)(2,1)}, u32[]{:S(2)}) %copy-start.4) | copy-done | bytes 1048600
  78.5 2.7 %steps.1.stepped = f32[3,2048,256]{2,1,0:T(8,128)S(1)} custom-call(bf16[16,48,256]{2,1,0:T(8,128)(2,1)S(1)} %all_to_all.10.gathered, bf16[2048,256]{1,0:T(8,128)(2,1)S(1)} %copy-done.2, bf16[2048,256]{1,0:T(8,128)(2,1)S(1)} %copy-done.3, bf16[2048,256]{1,0:T(8,128)(2,1)S(1)} %copy-done.4), custom_call_target="tpu_custom_call" | custom-call | flops 805306368 | bytes 9437184 | tf_op jit(solution)/shard_map/steps/pallas_call | solution.py:315
  81.4 3.8 %applied.1 = (f32[128,256]{1,0:T(8,128)}, f32[128,256]{1,0:T(8,128)}, f32[128,256]{1,0:T(8,128)}, bf16[2048,256]{1,0:T(8,128)(2,1)}, bf16[2048,256]{1,0:T(8,128)(2,1)}, /*index=5*/bf16[2048,256]{1,0:T(8,128)(2,1)}) custom-call(s32[2]{0:T(128)S(1)} %pad_add_fusion.me, f32[8,128]{1,0:T(8,128)S(1)} %add_add_fusion.totals, f32[3,2048,256]{2,1,0:T(8,128)S(1)} %steps.1.stepped, ...), custom_call_target="tpu_custom_call" | custom-call | flops 16777216 | bytes 12582912 | tf_op jit(solution)/shard_map/applied/pallas_call | solution.py:359
  (31 shorter events, 1.8 us)
Async XLA Ops:
  0.6 6.5 %copy-start.5 = (bf16[2048,256]{1,0:T(8,128)(2,1)S(1)}, bf16[2048,256]{1,0:T(8,128)(2,1)}, u32[]{:S(2)}) copy-start(bf16[2048,256]{1,0:T(8,128)(2,1)} %refs_0_.5) | copy-start | bytes 3145732
  0.7 6.5 %copy-start.1 = (bf16[2048,256]{1,0:T(8,128)(2,1)S(1)}, bf16[2048,256]{1,0:T(8,128)(2,1)}, u32[]{:S(2)}) copy-start(bf16[2048,256]{1,0:T(8,128)(2,1)} %refs_1_.3) | copy-start | bytes 3145732
  0.7 6.5 %copy-start = (bf16[2048,256]{1,0:T(8,128)(2,1)S(1)}, bf16[2048,256]{1,0:T(8,128)(2,1)}, u32[]{:S(2)}) copy-start(bf16[2048,256]{1,0:T(8,128)(2,1)} %refs_0_.4) | copy-start | bytes 3145732
  5.7 7.9 %copy-start.6 = (bf16[2048,256]{1,0:T(8,128)(2,1)S(1)}, bf16[2048,256]{1,0:T(8,128)(2,1)}, u32[]{:S(2)}) copy-start(bf16[2048,256]{1,0:T(8,128)(2,1)} %refs_0_.5) | copy-start | bytes 3145732
  5.7 6.0 %collective-permute-start.1 = (bf16[1024,512]{1,0:T(8,128)(2,1)S(1)}, bf16[1024,512]{1,0:T(8,128)(2,1)S(1)}, u32[]{:S(2)}, u32[]{:S(2)}) collective-permute-start(bf16[1024,512]{1,0:T(8,128)(2,1)S(1)} %get-tuple-element.30.own), channel_id=1, source_target_pairs={{0,1},{1,0},{2,3},{3,2},{4,5},{5,4},{6,7},{7,6},{8,9},{9,8},{10,11... | collective-permute-start | bytes 3145736 | tf_op jit(solution)/shard_map/ppermute | solution.py:427
  11.6 64.5 %copy-start.2 = (bf16[2048,256]{1,0:T(8,128)(2,1)S(1)}, bf16[2048,256]{1,0:T(8,128)(2,1)}, u32[]{:S(2)}) copy-start(bf16[2048,256]{1,0:T(8,128)(2,1)} %qb.3) | copy-start | bytes 3145732
  11.6 2.0 %collective-permute-start = (bf16[1024,256]{1,0:T(8,128)(2,1)S(1)}, bf16[1024,256]{1,0:T(8,128)(2,1)S(1)}, u32[]{:S(2)}, u32[]{:S(2)}) collective-permute-start(bf16[1024,256]{1,0:T(8,128)(2,1)S(1)} %get-tuple-element.32), channel_id=1, source_target_pairs={{0,1},{1,0},{2,3},{3,2},{4,5},{5,4},{6,7},{7,6},{8,9},{9,8},{10,11... | collective-permute-start | bytes 1572872 | tf_op jit(solution)/shard_map/ppermute | solution.py:429
  14.6 29.7 %all-to-all-start = ((bf16[16,48,256]{2,1,0:T(8,128)(2,1)}), bf16[16,48,256]{2,1,0:T(8,128)(2,1)S(1)}, u32[]{:S(2)}, u32[]{:S(2)}) async-start(bf16[16,48,256]{2,1,0:T(8,128)(2,1)} %shard_map.257), calls=%async_computation | async-start | bytes 786432 | tf_op jit(solution)/shard_map/all_to_all | solution.py:434
  22.5 14.3 %collective-permute-start.8 = (bf16[128,768]{1,0:T(8,128)(2,1)S(1)}, bf16[128,768]{1,0:T(8,128)(2,1)S(1)}, u32[]{:S(2)}, u32[]{:S(2)}) collective-permute-start(bf16[128,768]{1,0:T(8,128)(2,1)S(1)} %get-tuple-element.35.refs_0_), channel_id=1, source_target_pairs={{0,80},{8,88},{16,64},{24,72},{32,112},{40,120},{48,96},{56,104},{... | collective-permute-start | bytes 589832 | tf_op jit(solution)/shard_map/ppermute | solution.py:384
  27.8 10.8 %collective-permute-start.7 = (bf16[128,768]{1,0:T(8,128)(2,1)S(1)}, bf16[128,768]{1,0:T(8,128)(2,1)S(1)}, u32[]{:S(2)}, u32[]{:S(2)}) collective-permute-start(bf16[128,768]{1,0:T(8,128)(2,1)S(1)} %get-tuple-element.35.refs_0_), channel_id=1, source_target_pairs={{0,16},{8,24},{16,0},{24,8},{32,48},{40,56},{48,32},{56,40},{64,80... | collective-permute-start | bytes 589832 | tf_op jit(solution)/shard_map/ppermute | solution.py:384
  28.1 12.2 %collective-permute-start.6 = (bf16[128,768]{1,0:T(8,128)(2,1)S(1)}, bf16[128,768]{1,0:T(8,128)(2,1)S(1)}, u32[]{:S(2)}, u32[]{:S(2)}) collective-permute-start(bf16[128,768]{1,0:T(8,128)(2,1)S(1)} %get-tuple-element.35.refs_0_), channel_id=1, source_target_pairs={{0,64},{8,72},{16,80},{24,88},{32,96},{40,104},{48,112},{56,120},{... | collective-permute-start | bytes 589832 | tf_op jit(solution)/shard_map/ppermute | solution.py:384
  41.2 40.1 %copy-start.7 = (bf16[4,128,768]{2,1,0:T(8,128)(2,1)S(1)}, bf16[4,128,768]{2,1,0:T(8,128)(2,1)}, u32[]{:S(2)}) copy-start(bf16[4,128,768]{2,1,0:T(8,128)(2,1)} %collected.1.refs_0_) | copy-start | bytes 2359300
  41.2 40.1 %collective-permute-start.11 = (bf16[4,128,768]{2,1,0:T(8,128)(2,1)}, bf16[4,128,768]{2,1,0:T(8,128)(2,1)S(1)}, u32[]{:S(2)}, u32[]{:S(2)}) collective-permute-start(bf16[4,128,768]{2,1,0:T(8,128)(2,1)} %collected.1.refs_0_), channel_id=1, source_target_pairs={{0,120},{8,96},{16,104},{24,112},{32,24},{40,0},{48,8},{56,16},{64... | collective-permute-start | bytes 2359304 | tf_op jit(solution)/shard_map/ppermute | solution.py:384
  43.8 37.5 %collective-permute-start.10 = (bf16[4,128,768]{2,1,0:T(8,128)(2,1)}, bf16[4,128,768]{2,1,0:T(8,128)(2,1)}, u32[]{:S(2)}, u32[]{:S(2)}) collective-permute-start(bf16[4,128,768]{2,1,0:T(8,128)(2,1)} %collected.1.refs_0_), channel_id=1, source_target_pairs={{0,8},{8,16},{16,24},{24,0},{32,40},{40,48},{48,56},{56,32},{64,72... | collective-permute-start | bytes 2359304 | tf_op jit(solution)/shard_map/ppermute | solution.py:384
  43.8 37.5 %collective-permute-start.9 = (bf16[4,128,768]{2,1,0:T(8,128)(2,1)}, bf16[4,128,768]{2,1,0:T(8,128)(2,1)}, u32[]{:S(2)}, u32[]{:S(2)}) collective-permute-start(bf16[4,128,768]{2,1,0:T(8,128)(2,1)} %collected.1.refs_0_), channel_id=1, source_target_pairs={{0,32},{8,40},{16,48},{24,56},{32,64},{40,72},{48,80},{56,88},{64,... | collective-permute-start | bytes 2359304 | tf_op jit(solution)/shard_map/ppermute | solution.py:384
  67.7 3.2 %collective-permute-start.2 = (f32[8,128]{1,0:T(8,128)S(1)}, f32[8,128]{1,0:T(8,128)S(1)}, u32[]{:S(2)}, u32[]{:S(2)}) collective-permute-start(f32[8,128]{1,0:T(8,128)S(1)} %squares.1), channel_id=1, source_target_pairs={{0,1},{1,0},{2,3},{3,2},{4,5},{5,4},{6,7},{7,6},{8,9},{9,8},{10,11... | collective-permute-start | bytes 12296 | tf_op jit(solution)/shard_map/ppermute | solution.py:395
  70.9 4.0 %collective-permute-start.5 = (f32[8,128]{1,0:T(8,128)S(1)}, f32[8,128]{1,0:T(8,128)S(1)}, u32[]{:S(2)}, u32[]{:S(2)}) collective-permute-start(f32[8,128]{1,0:T(8,128)S(1)} %add.12), channel_id=1, source_target_pairs={{0,4},{2,6},{4,0},{6,2},{1,5},{3,7},{5,1},{7,3},{8,12},{10,14},{12... | collective-permute-start | bytes 12296 | tf_op jit(solution)/shard_map/ppermute | solution.py:397
  73.7 7.6 %collective-permute-start.4 = (f32[8,128]{1,0:T(8,128)S(1)}, f32[8,128]{1,0:T(8,128)S(1)}, u32[]{:S(2)}, u32[]{:S(2)}) collective-permute-start(f32[8,128]{1,0:T(8,128)S(1)} %add.12), channel_id=1, source_target_pairs={{0,6},{2,0},{4,2},{6,4},{1,7},{3,1},{5,3},{7,5},{8,14},{10,8},{12,... | collective-permute-start | bytes 12296 | tf_op jit(solution)/shard_map/ppermute | solution.py:397
  74.9 6.4 %collective-permute-start.3 = (f32[8,128]{1,0:T(8,128)S(1)}, f32[8,128]{1,0:T(8,128)S(1)}, u32[]{:S(2)}, u32[]{:S(2)}) collective-permute-start(f32[8,128]{1,0:T(8,128)S(1)} %add.12), channel_id=1, source_target_pairs={{0,2},{2,4},{4,6},{6,0},{1,3},{3,5},{5,7},{7,1},{8,10},{10,12},{12... | collective-permute-start | bytes 12296 | tf_op jit(solution)/shard_map/ppermute | solution.py:397
  76.1 1.2 %copy-start.3 = (bf16[2048,256]{1,0:T(8,128)(2,1)S(1)}, bf16[2048,256]{1,0:T(8,128)(2,1)}, u32[]{:S(2)}) copy-start(bf16[2048,256]{1,0:T(8,128)(2,1)} %fb.3) | copy-start | bytes 3145732
  77.3 1.2 %copy-start.4 = (bf16[2048,256]{1,0:T(8,128)(2,1)S(1)}, bf16[2048,256]{1,0:T(8,128)(2,1)}, u32[]{:S(2)}) copy-start(bf16[2048,256]{1,0:T(8,128)(2,1)} %ob.1) | copy-start | bytes 3145732

commit v4 on v3

v4 whole, which is shorter than its diff:
```python
import jax
import jax.numpy as jnp
from jax import lax
from jax.experimental import pallas as pl
from jax.experimental.pallas import tpu as pltpu
from jax.sharding import Mesh
from jax.sharding import PartitionSpec as P

WIDTH = 2048
RANK = 256
FS = ("fs_0", "fs_1")
TP = ("tp_0", "tp_1")
MATS = 3
IN_CUTS = (0, 512, 2048)
SIDE = 4
GRANT = 24 * 1024 * 1024

F32 = jnp.float32
BF16 = jnp.bfloat16

FAR = ((0, 0), (2, 0), (0, 2), (2, 2))
NEAR = ((0, 0), (3, 0), (0, 3), (1, 1))


SMEM = pl.BlockSpec(memory_space=pltpu.SMEM)
VMEM = pl.BlockSpec(memory_space=pltpu.VMEM)
HBM = pl.BlockSpec(memory_space=pltpu.HBM)


def cost(flops, moved):
    return pl.CostEstimate(flops=flops, bytes_accessed=moved, transcendentals=0)


def params():
    return pltpu.CompilerParams(vmem_limit_bytes=GRANT)


def in_hbm(*arrays):
    return [pltpu.with_memory_space_constraint(a, pltpu.HBM) for a in arrays]


def in_vmem(*arrays):
    return [pltpu.with_memory_space_constraint(a, pltpu.VMEM) for a in arrays]


def contract_rows(left, right):
    return lax.dot_general(
        left, right, (((0,), (0,)), ((), ())), preferred_element_type=F32
    )


def half_of(which, half):
    return pl.ds(pl.multiple_of(which * half, half), half)


def reduce_in_kernel(core, source, qb, fb, qw, fw, ow, grad, ob, *refs):
    state, refs = refs[: 2 * MATS], refs[2 * MATS :]
    out, rounded, packed, grad_half, ob_held = refs[:5]
    rows_in, basis_in, weights_in, sums, sems, weight_sems, state_sems, next_sems = refs[5:]
    bases, weights = (qb, fb), (qw, fw, ow)
    mine = half_of(core[0], out.shape[0])
    copies = []
    for c, (low, high) in enumerate(zip(IN_CUTS, IN_CUTS[1:])):
        at = slice(low, high)
        pieces = [(source.at[mine, at], rows_in.at[:, at])]
        pieces += [(b.at[at, :], basis_in.at[m, at, :]) for m, b in enumerate(bases)]
        copies.append(
            [pltpu.make_async_copy(a, b, sems.at[c, p]) for p, (a, b) in enumerate(pieces)]
        )
    weight_copies = [
        pltpu.make_async_copy(w, weights_in.at[m], weight_sems.at[m])
        for m, w in enumerate(weights)
    ]
    state_copies = [
        pltpu.make_async_copy(a, packed.at[n], state_sems.at[n]) for n, a in enumerate(state)
    ]
    next_copies = [
        pltpu.make_async_copy(grad.at[mine, :], grad_half, next_sems.at[0]),
        pltpu.make_async_copy(ob, ob_held, next_sems.at[1]),
    ]
    for copy in (*copies[0], *weight_copies, *copies[1]):
        copy.start()
    for c, (low, high) in enumerate(zip(IN_CUTS, IN_CUTS[1:])):
        at = slice(low, high)
        for copy in copies[c]:
            copy.wait()
        if c > 0:
            for copy in (*next_copies, *state_copies):
                copy.start()
        for m in range(len(bases)):
            to = slice(m * RANK, (m + 1) * RANK)
            part = jnp.dot(rows_in[:, at], basis_in[m, at, :], preferred_element_type=F32)
            if c == 0:
                sums[:, to] = part
            else:
                out[:, to] = (sums[:, to] + part).astype(BF16)
        if c == 0:
            cols = weights_in.shape[2]
            for m, copy in enumerate(weight_copies):
                copy.wait()
                rounded[:, m * cols : (m + 1) * cols] = weights_in[m].astype(BF16)
    for copy in (*state_copies, *next_copies):
        copy.wait()


def reduce_in(core, source, bases, weights, grad, ob, state):
    tokens, width = source.shape
    half, count = tokens // 2, len(bases)
    rows, cols = weights[0].shape
    return pl.pallas_call(
        reduce_in_kernel,
        in_specs=[SMEM, *(HBM for _ in range(3 + count + MATS + len(state)))],
        out_specs=[VMEM for _ in range(5)],
        out_shape=[
            pltpu.VMEM((half, count * RANK), BF16),
            pltpu.VMEM((rows, MATS * cols), BF16),
            pltpu.VMEM((len(state), *state[0].shape), F32),
            pltpu.VMEM((half, width), BF16),
            pltpu.VMEM((width, RANK), BF16),
        ],
        scratch_shapes=[
            pltpu.VMEM((half, width), BF16),
            pltpu.VMEM((count, width, RANK), BF16),
            pltpu.VMEM((MATS, rows, cols), F32),
            pltpu.VMEM((half, count * RANK), F32),
            pltpu.SemaphoreType.DMA((len(IN_CUTS) - 1, 1 + count)),
            pltpu.SemaphoreType.DMA((MATS,)),
            pltpu.SemaphoreType.DMA((len(state),)),
            pltpu.SemaphoreType.DMA((2,)),
        ],
        compiler_params=params(),
        cost_estimate=cost(2 * half * RANK * width * count, 6 << 20),
        name="reduce_in",
    )(core, *in_hbm(source, *bases, *weights, grad, ob, *state))


def reduce_out_kernel(core, own, qc, fc, mixed, source, basis, out, sums):
    mine = half_of(core[0], out.shape[0])
    out[...] = jnp.dot(source[...], basis[...], preferred_element_type=F32).astype(BF16)
    for m, cotangent in enumerate((qc, fc)):
        sums[m] = contract_rows(own[:, m * RANK : (m + 1) * RANK], cotangent[mine, :])
    sums[2] = contract_rows(out[...], mixed[mine, :])


def reduce_out(core, own, cotangents, source, basis):
    half, width = source.shape
    cols = cotangents[0].shape[1]
    return pl.pallas_call(
        reduce_out_kernel,
        in_specs=[SMEM, *(VMEM for _ in range(3 + MATS))],
        out_specs=[VMEM, VMEM],
        out_shape=[pltpu.VMEM((half, RANK), BF16), pltpu.VMEM((MATS, RANK, cols), F32)],
        compiler_params=params(),
        cost_estimate=cost(2 * half * RANK * (width + 3 * cols), 6 << 20),
        name="reduce_out",
    )(core, *in_vmem(own, *cotangents, source, basis))


def contract_one(sums, other, cotangent, theirs, m, k):
    return sums[m] + contract_rows(other[:, k * RANK : (k + 1) * RANK], cotangent[theirs, :])


def contract_near_kernel(core, sums, other, qc, fc, out, held, sems):
    groups, rows = out.shape[0], out.shape[1] // MATS
    theirs = half_of(1 - core[0], other.shape[0])
    copies = []
    for m, cotangent in enumerate((qc, fc)):
        total = contract_one(sums, other, cotangent, theirs, m, m)
        held[m] = total.astype(BF16).reshape(groups, rows, total.shape[1])
        copies.append(
            pltpu.make_async_copy(held.at[m], out.at[:, m * rows : (m + 1) * rows, :], sems.at[m])
        )
        copies[m].start()
    for copy in copies:
        copy.wait()


def contract_near(core, sums, other, cotangents, groups):
    cols = sums.shape[2]
    rows = RANK // groups
    return pl.pallas_call(
        contract_near_kernel,
        in_specs=[SMEM, *(VMEM for _ in range(4))],
        out_specs=HBM,
        out_shape=pltpu.HBM((groups, MATS * rows, cols), BF16),
        scratch_shapes=[
            pltpu.VMEM((2, groups, rows, cols), BF16),
            pltpu.SemaphoreType.DMA((2,)),
        ],
        compiler_params=params(),
        cost_estimate=cost(4 * other.shape[0] * RANK * cols, 2 << 20),
        name="contract_near",
    )(core, *in_vmem(sums, other, *cotangents[:2]))


def contract_far_kernel(core, sums, other, mixed, _, out, held, sems):
    groups, rows = out.shape[0], out.shape[1] // MATS
    theirs = half_of(1 - core[0], other.shape[0])
    total = contract_one(sums, other, mixed, theirs, 2, 0)
    held[...] = total.astype(BF16).reshape(groups, rows, total.shape[1])
    copy = pltpu.make_async_copy(held, out.at[:, 2 * rows : 3 * rows, :], sems.at[0])
    copy.start()
    copy.wait()


def contract_far(core, sums, other, mixed, blocks):
    groups, rows, cols = blocks.shape
    return pl.pallas_call(
        contract_far_kernel,
        in_specs=[SMEM, *(VMEM for _ in range(3)), HBM],
        out_specs=HBM,
        out_shape=pltpu.HBM(blocks.shape, BF16),
        scratch_shapes=[
            pltpu.VMEM((groups, rows // MATS, cols), BF16),
            pltpu.SemaphoreType.DMA((1,)),
        ],
        input_output_aliases={4: 0},
        compiler_params=params(),
        cost_estimate=cost(2 * other.shape[0] * RANK * cols, 1 << 20),
        name="contract_far",
    )(core, *in_vmem(sums, other, mixed), *in_hbm(blocks))


def moment_kernel(arrived, held, *refs):
    state_new = refs[: 2 * MATS]
    directions, direction, held_new, sems, state_sems = refs[2 * MATS :]
    groups = arrived.shape[0]
    rows = arrived.shape[1] // MATS
    for m in range(MATS):
        at = slice(m * rows, (m + 1) * rows)
        value = arrived[0, at, :].astype(F32)
        for g in range(1, groups):
            value = value + arrived[g, at, :].astype(F32)
        first_new = 0.8 * held[m] + 0.2 * value
        second_new = 0.95 * held[MATS + m] + 0.05 * value * value
        held_new[m] = first_new
        held_new[MATS + m] = second_new
        direction[at, :] = (first_new / (jnp.sqrt(second_new) + 1e-08)).astype(BF16)
    sends = [
        pltpu.make_async_copy(direction, directions.at[g], sems.at[g]) for g in range(groups)
    ]
    sends += [
        pltpu.make_async_copy(held_new.at[n], ref, state_sems.at[n])
        for n, ref in enumerate(state_new)
    ]
    for send in sends:
        send.start()
    for send in sends:
        send.wait()


def moments(arrived, packed):
    groups, rows, cols = arrived.shape
    count = packed.shape[0]
    results = pl.pallas_call(
        moment_kernel,
        in_specs=[VMEM, VMEM],
        out_specs=[HBM for _ in range(count + 1)],
        out_shape=[
            *(pltpu.HBM(packed.shape[1:], F32) for _ in range(count)),
            pltpu.HBM(arrived.shape, BF16),
        ],
        scratch_shapes=[
            pltpu.VMEM((rows, cols), BF16),
            pltpu.VMEM(packed.shape, F32),
            pltpu.SemaphoreType.DMA((groups,)),
            pltpu.SemaphoreType.DMA((count,)),
        ],
        compiler_params=params(),
        cost_estimate=cost(1 << 22, 1 << 20),
        name="moments",
    )(*in_vmem(arrived, packed))
    return results[:count], results[count]


def collect_kernel(*refs):
    for k, block in enumerate(refs[: len(FAR)]):
        refs[len(FAR)][k] = block[...]


def collected(blocks):
    return pl.pallas_call(
        collect_kernel,
        in_specs=[VMEM for _ in blocks],
        out_specs=VMEM,
        out_shape=pltpu.HBM((len(blocks), *blocks[0].shape), BF16),
        compiler_params=params(),
        cost_estimate=cost(1 << 20, 2 << 20),
        name="collected",
    )(*in_vmem(*blocks))


def square_kernel(gathered, out):
    rows = gathered.shape[1] // MATS
    out[...] = jnp.zeros_like(out)
    for m in range(MATS):
        values = gathered[:, m * rows : (m + 1) * rows, :].astype(F32)
        total = jnp.sum(values * values)
        out[m : m + 1, :] = jnp.full((1, out.shape[1]), total, F32)


def squares(gathered):
    return pl.pallas_call(
        square_kernel,
        out_shape=jax.ShapeDtypeStruct((8, 128), F32),
        compiler_params=params(),
        cost_estimate=cost(1 << 22, 1 << 19),
        name="squares",
    )(gathered)


def step_kernel(gathered, qb, fb, ob, out, held, sems):
    rank_rows, cols = gathered.shape[1] // MATS, gathered.shape[2]
    copies = [
        pltpu.make_async_copy(b, held.at[m], sems.at[m]) for m, b in enumerate((qb, fb, ob))
    ]
    for copy in copies:
        copy.start()
    for m, copy in enumerate(copies):
        direction = gathered[:, m * rank_rows : (m + 1) * rank_rows, :].reshape(RANK, cols)
        copy.wait()

        def piece(i, carry):
            at = pl.ds(pl.multiple_of(i * 512, 512), 512)
            out[m, at, :] = jnp.dot(held[m, at, :], direction, preferred_element_type=F32)
            return carry

        lax.fori_loop(0, held.shape[1] // 512, piece, 0)


def steps(gathered, bases):
    width, cols = bases[0].shape[0], gathered.shape[2]
    return pl.pallas_call(
        step_kernel,
        in_specs=[VMEM, *(HBM for _ in bases)],
        out_specs=VMEM,
        out_shape=pltpu.VMEM((MATS, width, cols), F32),
        scratch_shapes=[
            pltpu.VMEM((MATS, width, RANK), BF16),
            pltpu.SemaphoreType.DMA((MATS,)),
        ],
        compiler_params=params(),
        cost_estimate=cost(MATS * 2 * width * RANK * cols, 9 << 20),
        name="steps",
    )(*in_vmem(gathered), *in_hbm(*bases))


def rows_at(me, near, j, rows):
    z = lax.rem(me[0] + 2 * SIDE - near[0] - 2 * lax.rem(j, 2), SIDE)
    y = lax.rem(me[1] + 2 * SIDE - near[1] - 2 * lax.div(j, 2), SIDE)
    return pl.ds(pl.multiple_of((z * SIDE + y) * rows, rows), rows)


def scale_of(totals, m):
    return lax.rsqrt(totals[m : m + 1, :1] * (1.0 / (RANK * WIDTH)) + 1e-06)


def updated(weight, j, m, factor, stepped, at):
    cols = stepped.shape[2]
    old = weight[j, :, m * cols : (m + 1) * cols].astype(F32)
    return (old - factor * stepped[m, at, :]).astype(BF16)


def apply_far_kernel(me, totals, stepped, four, *refs):
    updates, pieces, held, sems = refs[:MATS], refs[MATS], refs[MATS + 1], refs[MATS + 2]
    rows = held.shape[1]
    mine = pl.ds(pl.multiple_of((me[0] * SIDE + me[1]) * rows, rows), rows)
    stores = []
    for m in range(MATS):
        held[m] = stepped[m, mine, :] * scale_of(totals, m)
        stores.append(pltpu.make_async_copy(held.at[m], updates[m], sems.at[m]))
        stores[m].start()
    for m in range(MATS):
        factor = 0.05 * scale_of(totals, m)
        for j in range(len(FAR)):
            pieces[m, j] = updated(four, j, m, factor, stepped, rows_at(me, NEAR[0], j, rows))
    for store in stores:
        store.wait()


def apply_far(me, totals, stepped, four):
    cols = stepped.shape[2]
    count, rows = four.shape[:2]
    results = pl.pallas_call(
        apply_far_kernel,
        in_specs=[SMEM, VMEM, VMEM, VMEM],
        out_specs=[*(HBM for _ in range(MATS)), VMEM],
        out_shape=[
            *(pltpu.HBM((rows, cols), F32) for _ in range(MATS)),
            pltpu.VMEM((MATS, count, rows, cols), BF16),
        ],
        scratch_shapes=[
            pltpu.VMEM((MATS, rows, cols), F32),
            pltpu.SemaphoreType.DMA((MATS,)),
        ],
        compiler_params=params(),
        cost_estimate=cost(1 << 23, 3 << 20),
        name="apply_far",
    )(me, *in_vmem(totals, stepped, four))
    return results[:MATS], results[MATS]


def apply_near_kernel(me, totals, stepped, pieces, *refs):
    weights, copies, (held, sems) = refs[:MATS], refs[MATS : 2 * MATS], refs[2 * MATS :]
    rows = pieces.shape[2]
    stores = []
    for m in range(MATS):
        factor = 0.05 * scale_of(totals, m)

        def block(j, carry):
            held[m, rows_at(me, NEAR[0], j, rows), :] = pieces[m, j]
            for near, weight in zip(NEAR[1:], weights):
                at = rows_at(me, near, j, rows)
                held[m, at, :] = updated(weight, j, m, factor, stepped, at)
            return carry

        lax.fori_loop(0, len(FAR), block, 0)
        stores.append(pltpu.make_async_copy(held.at[m], copies[m], sems.at[m]))
        stores[m].start()
    for store in stores:
        store.wait()


def apply_near(me, totals, stepped, pieces, weights):
    width, cols = stepped.shape[1:]
    return pl.pallas_call(
        apply_near_kernel,
        in_specs=[SMEM, *(VMEM for _ in range(3 + len(weights)))],
        out_specs=[HBM for _ in range(MATS)],
        out_shape=[pltpu.HBM((width, cols), BF16) for _ in range(MATS)],
        scratch_shapes=[
            pltpu.VMEM((MATS, width, cols), BF16),
            pltpu.SemaphoreType.DMA((MATS,)),
        ],
        compiler_params=params(),
        cost_estimate=cost(1 << 24, 9 << 20),
        name="apply_near",
    )(me, *in_vmem(totals, stepped, pieces, *weights))


def moved_by(value, offset):
    pairs = []
    for z in range(SIDE):
        for y in range(SIDE):
            target = ((z + offset[0]) % SIDE) * SIDE + (y + offset[1]) % SIDE
            pairs.append((z * SIDE + y, target))
    return lax.ppermute(value, FS, pairs)


def gathered_by(value, offsets):
    moved = []
    for offset in offsets[1:]:
        moved.append(moved_by(value, offset))
    return moved


def summed_over_tp(value):
    value = value + lax.ppermute(value, "tp_1", [(0, 1), (1, 0)])
    arrived = [
        lax.ppermute(value, "tp_0", [(i, (i + far) % SIDE) for i in range(SIDE)])
        for far in (1, 2, 3)
    ]
    return value + (arrived[0] + arrived[2]) + arrived[1]


def body(
    saved_input,
    query_cotangent,
    forget_cotangent,
    mixed_output,
    out_cotangent,
    query_basis,
    forget_basis,
    out_basis,
    query_weight,
    forget_weight,
    out_weight,
    *state,
):
    groups = lax.axis_size(FS)
    bases = (query_basis, forget_basis, out_basis)
    cotangents = (query_cotangent, forget_cotangent, mixed_output)
    core = lax.axis_index("tp_1").astype(jnp.int32).reshape(1)
    me = jnp.stack([lax.axis_index("fs_0"), lax.axis_index("fs_1")]).astype(jnp.int32)

    own, weights, packed, grad_half, ob_held = reduce_in(
        core,
        saved_input,
        bases[:2],
        (query_weight, forget_weight, out_weight),
        out_cotangent,
        out_basis,
        state,
    )
    other = lax.ppermute(own, "tp_1", [(0, 1), (1, 0)])
    own_out, sums = reduce_out(core, own, cotangents, grad_half, ob_held)
    other_out = lax.ppermute(own_out, "tp_1", [(0, 1), (1, 0)])
    blocks = contract_near(core, sums, other, cotangents, groups)
    blocks = contract_far(core, sums, other_out, mixed_output, blocks)
    four = collected((weights, *gathered_by(weights, FAR)))
    near_weights = gathered_by(four, NEAR)

    arrived = lax.all_to_all(blocks, FS, 0, 0, tiled=True)
    state_new, directions = moments(arrived, packed)
    gathered = lax.all_to_all(directions, FS, 0, 0, tiled=True)
    totals = summed_over_tp(squares(gathered))
    stepped = steps(gathered, bases)
    updates, pieces = apply_far(me, totals, stepped, four)
    copies = apply_near(me, totals, stepped, pieces, near_weights)
    return (*updates, *state_new, *copies)


def solution(mesh):
    split = Mesh(mesh.devices.reshape(4, 4, 4, 2), ("fs_0", "fs_1", "tp_0", "tp_1"))
    in_specs = (
        P(FS, None),
        P(FS, TP),
        P(FS, TP),
        P(FS, TP),
        P(FS, None),
        P(),
        P(),
        P(),
        *(P(FS, TP) for _ in range(9)),
    )
    out_specs = (*(P(FS, TP) for _ in range(9)), *(P(None, TP) for _ in range(3)))
    return jax.shard_map(body, mesh=split, in_specs=in_specs, out_specs=out_specs, check_vma=False)
```

time: 85.9 us -> 67.7 us (0.79)
  blocking collectives: 21.4 us -> 0 us
  starting transfers between devices: 25.6 us -> 35 us
  waiting for transfers between devices: 13.8 us -> 11.1 us
  local copies, waits for them, and re-layouts: 2.48 us -> 0.02 us
    all_to_all x1 -> x0, blocking collectives: 21.4 us -> none  [body(): gathered = lax.all_to_all(directions, FS, 0, 0, tiled=True)]
    ppermute x6, waiting for transfers between devices: 12 us -> 4.23 us  [moved_by(): return lax.ppermute(value, FS, pairs)]
    ppermute x1, starting transfers between devices: 2.41 us -> 8.1 us  [summed_over_tp(): value = value + lax.ppermute(value, 'tp_1', [(0, 1), (1, 0)])]
    all_to_all x1, waiting for transfers between devices: 0.01 us -> 3.88 us  [body(): arrived = lax.all_to_all(blocks, FS, 0, 0, tiled=True)]
    all_to_all x0 -> x1, starting transfers between devices: none -> 3.57 us  [body(): gathered = lax.all_to_all(directions, FS, 0, 0, tiled=True)]
    unnamed x16 -> x8, local copies, waits for them, and re-layouts: 2.48 us -> 0.02 us
    pallas_call x7 -> x8, Pallas kernels: 19.7 us -> 19 us  [the longest x1 5.82 us: reduce_in(): pl.pallas_call(reduce_in_kernel, in_specs=[SMEM, *(HBM for _ in range(3 +...]
  transfers between devices with their start and end apart: 13 -> 14, of which waited for: 6 -> 7; matrix products, arithmetic and copies ran while one was open for 0% -> 0% of each run, Pallas kernels for 13% -> 16%
where the time goes in v4:
time: 67.7 us; the launch traced here: 67.3 us
  starting transfers between devices  35 us (52%)
  Pallas kernels  20.2 us (30%)
  waiting for transfers between devices  11.1 us (16%)
  between operations  0.84 us (1%)
    ppermute x6, starting transfers between devices, moved_by(): return lax.ppermute(value, FS, pairs)  8.38 us
    ppermute x1, starting transfers between devices, summed_over_tp(): value = value + lax.ppermute(value, 'tp_1', [(0, 1), (1, 0)])  8.1 us
    all_to_all x1, starting transfers between devices, body(): arrived = lax.all_to_all(blocks, FS, 0, 0, tiled=True)  7.89 us
    pallas_call x1, Pallas kernels, reduce_in(): pl.pallas_call(reduce_in_kernel, in_specs=[SMEM, *(HBM for _ in range(3 +...  5.82 us
    ppermute x3, starting transfers between devices, summed_over_tp(): lax.ppermute(value, 'tp_0', [(i, (i + far) % SIDE) for i in range(SIDE)])  5.53 us
    ppermute x6, waiting for transfers between devices, moved_by(): return lax.ppermute(value, FS, pairs)  4.23 us
    pallas_call x1, Pallas kernels, steps(): pl.pallas_call(step_kernel, in_specs=[VMEM, *(HBM for _ in bases)], out_s...  4 us
    all_to_all x1, waiting for transfers between devices, body(): arrived = lax.all_to_all(blocks, FS, 0, 0, tiled=True)  3.88 us
  transfers between devices with their start and end apart: 14, of which 7 were waited for; matrix products, arithmetic and copies ran while one was open for 0% of the time, Pallas kernels for 16%

profile of v4, /device:TPU:1, one launch (start us, length us, event | category | flops | bytes accessed | tf_op | source)
XLA Modules:
  0.0 67.3 jit_solution(13062842597329281612)
XLA Ops:
  0.7 5.8 %reduce_in.1 = (bf16[1024,512]{1,0:T(8,128)(2,1)S(1)}, bf16[128,768]{1,0:T(8,128)(2,1)S(1)}, f32[6,16,256]{2,1,0:T(8,128)S(1)}, bf16[1024,2048]{1,0:T(8,128)(2,1)S(1)}, bf16[2048,256]{1,0:T(8,128)(2,1)S(1)}) custom-call(s32[1]{0:T(128)} %bitcast.2.core, bf16[2048,2048]{1,0:T(8,128)(2,1)} %source.1, bf16[2048,256]{1,0:T(8,128)(2,1)} %qb.3, ...), custom_call_target="tpu_custom_call" | custom-call | flops 2147483648 | bytes 6291456 | tf_op jit(solution)/shard_map/reduce_in/pallas_call | solution.py:110
  6.5 1.5 %collective-permute-start.1 = (bf16[1024,512]{1,0:T(8,128)(2,1)S(1)}, bf16[1024,512]{1,0:T(8,128)(2,1)S(1)}, u32[]{:S(2)}, u32[]{:S(2)}) collective-permute-start(bf16[1024,512]{1,0:T(8,128)(2,1)S(1)} %get-tuple-element.33.own), channel_id=1, source_target_pairs={{0,1},{1,0},{2,3},{3,2},{4,5},{5,4},{6,7},{7,6},{8,9},{9,8},{10,11... | collective-permute-start | bytes 3145736 | tf_op jit(solution)/shard_map/ppermute | solution.py:495
  8.0 1.9 %reduce_out.1 = (bf16[1024,256]{1,0:T(8,128)(2,1)S(1)}, f32[3,256,256]{2,1,0:T(8,128)S(1)}) custom-call(s32[1]{0:T(128)} %bitcast.2.core, bf16[1024,512]{1,0:T(8,128)(2,1)S(1)} %get-tuple-element.33.own, bf16[2048,256]{1,0:T(8,128)(2,1)S(1)} %copy-done, bf16[2048,256]{1,0:T(8,128)(2,1)S(1)} %copy-done.1, bf16[2048,256]{1,0:T(8,128)(2,1)S(1)} %copy-done.2, ...), custom_call_target="tpu_custom_call" | custom-call | flops 1476395008 | bytes 6291456 | tf_op jit(solution)/shard_map/reduce_out/pallas_call | solution.py:148
  10.3 1.2 %contract_near.1._ = bf16[16,48,256]{2,1,0:T(8,128)(2,1)} custom-call(s32[1]{0:T(128)} %bitcast.2.core, f32[3,256,256]{2,1,0:T(8,128)S(1)} %get-tuple-element.36.sums, bf16[1024,512]{1,0:T(8,128)(2,1)S(1)} %collective-permute-done.1.other, bf16[2048,256]{1,0:T(8,128)(2,1)S(1)} %copy-done, bf16[2048,256]{1,0:T(8,128)(2,1)S(1)} %copy-done.1), custom_call_target="tpu_custom_call" | custom-call | flops 268435456 | bytes 2097152 | tf_op jit(solution)/shard_map/contract_near/pallas_call | solution.py:181
  11.9 1.0 %contract_far.1 = bf16[16,48,256]{2,1,0:T(8,128)(2,1)} custom-call(s32[1]{0:T(128)} %bitcast.2.core, f32[3,256,256]{2,1,0:T(8,128)S(1)} %get-tuple-element.36.sums, bf16[1024,256]{1,0:T(8,128)(2,1)S(1)} %collective-permute-done.other, bf16[2048,256]{1,0:T(8,128)(2,1)S(1)} %copy-done.2, ...), custom_call_target="tpu_custom_call", output_to_operand_aliasing={{}: (4, {})} | custom-call | flops 134217728 | bytes 1048576 | tf_op jit(solution)/shard_map/contract_far/pallas_call | solution.py:208
  12.9 7.9 %all-to-all-start = ((bf16[16,48,256]{2,1,0:T(8,128)(2,1)}), bf16[16,48,256]{2,1,0:T(8,128)(2,1)S(1)}, u32[]{:S(2)}, u32[]{:S(2)}) async-start(bf16[16,48,256]{2,1,0:T(8,128)(2,1)} %contract_far.1), calls=%async_computation | async-start | bytes 786432 | tf_op jit(solution)/shard_map/all_to_all | solution.py:503
  20.8 2.9 %collective-permute-start.6 = (bf16[128,768]{1,0:T(8,128)(2,1)S(1)}, bf16[128,768]{1,0:T(8,128)(2,1)S(1)}, u32[]{:S(2)}, u32[]{:S(2)}) collective-permute-start(bf16[128,768]{1,0:T(8,128)(2,1)S(1)} %get-tuple-element.40.refs_0_), channel_id=1, source_target_pairs={{0,64},{8,72},{16,80},{24,88},{32,96},{40,104},{48,112},{56,120},{... | collective-permute-start | bytes 589832 | tf_op jit(solution)/shard_map/ppermute | solution.py:447
  23.7 2.7 %collective-permute-start.7 = (bf16[128,768]{1,0:T(8,128)(2,1)S(1)}, bf16[128,768]{1,0:T(8,128)(2,1)S(1)}, u32[]{:S(2)}, u32[]{:S(2)}) collective-permute-start(bf16[128,768]{1,0:T(8,128)(2,1)S(1)} %get-tuple-element.40.refs_0_), channel_id=1, source_target_pairs={{0,16},{8,24},{16,0},{24,8},{32,48},{40,56},{48,32},{56,40},{64,80... | collective-permute-start | bytes 589832 | tf_op jit(solution)/shard_map/ppermute | solution.py:447
  26.5 3.9 %all-to-all-done.arrived = bf16[16,48,256]{2,1,0:T(8,128)(2,1)S(1)} async-done(((bf16[16,48,256]{2,1,0:T(8,128)(2,1)}), bf16[16,48,256]{2,1,0:T(8,128)(2,1)S(1)}, u32[]{:S(2)}, u32[]{:S(2)}) %all-to-all-start) | async-done | bytes 393248 | tf_op jit(solution)/shard_map/all_to_all | solution.py:503
  30.4 1.0 %moments.1 = (f32[16,256]{1,0:T(8,128)}, f32[16,256]{1,0:T(8,128)}, f32[16,256]{1,0:T(8,128)}, f32[16,256]{1,0:T(8,128)}, f32[16,256]{1,0:T(8,128)}, /*index=5*/f32[16,256]{1,0:T(8,128)}, bf16[16,48,256]{2,1,0:T(8,128)(2,1)}) custom-call(bf16[16,48,256]{2,1,0:T(8,128)(2,1)S(1)} %all-to-all-done.arrived, f32[6,16,256]{2,1,0:T(8,128)S(1)} %get-tuple-element.38.held), custom_call_target="tpu_custom_call" | custom-call | flops 4194304 | bytes 1048576 | tf_op jit(solution)/shard_map/moments/pallas_call | solution.py:255
  31.4 3.6 %all-to-all-start.1 = ((bf16[16,48,256]{2,1,0:T(8,128)(2,1)}), bf16[16,48,256]{2,1,0:T(8,128)(2,1)S(1)}, u32[]{:S(2)}, u32[]{:S(2)}) async-start(bf16[16,48,256]{2,1,0:T(8,128)(2,1)} %get-tuple-element.39), calls=%async_computation.1 | async-start | bytes 786432 | tf_op jit(solution)/shard_map/all_to_all | solution.py:505
  35.0 4.2 %collective-permute-done.8.refs_3_ = bf16[128,768]{1,0:T(8,128)(2,1)S(1)} collective-permute-done((bf16[128,768]{1,0:T(8,128)(2,1)S(1)}, bf16[128,768]{1,0:T(8,128)(2,1)S(1)}, u32[]{:S(2)}, u32[]{:S(2)}) %collective-permute-start.8) | collective-permute-done | bytes 196640 | tf_op jit(solution)/shard_map/ppermute | solution.py:447
  39.3 0.9 %collected.1.four = bf16[4,128,768]{2,1,0:T(8,128)(2,1)} custom-call(bf16[128,768]{1,0:T(8,128)(2,1)S(1)} %get-tuple-element.40.refs_0_, bf16[128,768]{1,0:T(8,128)(2,1)S(1)} %collective-permute-done.6.refs_1_, bf16[128,768]{1,0:T(8,128)(2,1)S(1)} %collective-permute-done.7.refs_2_, bf16[128,768]{1,0:T(8,128)(2,1)S(1)} %collective-permute-done.8.refs_3_), custom_call_target="tpu_custom_call" | custom-call | flops 1048576 | bytes 2097152 | tf_op jit(solution)/shard_map/collected/pallas_call | solution.py:282
  40.2 0.9 %collective-permute-start.9 = (bf16[4,128,768]{2,1,0:T(8,128)(2,1)}, bf16[4,128,768]{2,1,0:T(8,128)(2,1)S(1)}, u32[]{:S(2)}, u32[]{:S(2)}) collective-permute-start(bf16[4,128,768]{2,1,0:T(8,128)(2,1)} %collected.1.four), channel_id=1, source_target_pairs={{0,96},{8,104},{16,112},{24,120},{32,0},{40,8},{48,16},{56,24},{64... | collective-permute-start | bytes 2359304 | tf_op jit(solution)/shard_map/ppermute | solution.py:447
  41.1 0.9 %collective-permute-start.10 = (bf16[4,128,768]{2,1,0:T(8,128)(2,1)}, bf16[4,128,768]{2,1,0:T(8,128)(2,1)S(1)}, u32[]{:S(2)}, u32[]{:S(2)}) collective-permute-start(bf16[4,128,768]{2,1,0:T(8,128)(2,1)} %collected.1.four), channel_id=1, source_target_pairs={{0,24},{8,0},{16,8},{24,16},{32,56},{40,32},{48,40},{56,48},{64,88... | collective-permute-start | bytes 2359304 | tf_op jit(solution)/shard_map/ppermute | solution.py:447
  42.0 0.8 %collective-permute-start.11 = (bf16[4,128,768]{2,1,0:T(8,128)(2,1)}, bf16[4,128,768]{2,1,0:T(8,128)(2,1)S(1)}, u32[]{:S(2)}, u32[]{:S(2)}) collective-permute-start(bf16[4,128,768]{2,1,0:T(8,128)(2,1)} %collected.1.four), channel_id=1, source_target_pairs={{0,40},{8,48},{16,56},{24,32},{32,72},{40,80},{48,88},{56,64},{64,... | collective-permute-start | bytes 2359304 | tf_op jit(solution)/shard_map/ppermute | solution.py:447
  43.5 8.1 %collective-permute-start.2 = (f32[8,128]{1,0:T(8,128)S(1)}, f32[8,128]{1,0:T(8,128)S(1)}, u32[]{:S(2)}, u32[]{:S(2)}) collective-permute-start(f32[8,128]{1,0:T(8,128)S(1)} %squares.1), channel_id=1, source_target_pairs={{0,1},{1,0},{2,3},{3,2},{4,5},{5,4},{6,7},{7,6},{8,9},{9,8},{10,11... | collective-permute-start | bytes 12296 | tf_op jit(solution)/shard_map/ppermute | solution.py:458
  51.6 0.8 %collective-permute-done.2 = f32[8,128]{1,0:T(8,128)S(1)} collective-permute-done((f32[8,128]{1,0:T(8,128)S(1)}, f32[8,128]{1,0:T(8,128)S(1)}, u32[]{:S(2)}, u32[]{:S(2)}) %collective-permute-start.2) | collective-permute-done | bytes 4128 | tf_op jit(solution)/shard_map/ppermute | solution.py:458
  52.4 2.7 %collective-permute-start.5 = (f32[8,128]{1,0:T(8,128)S(1)}, f32[8,128]{1,0:T(8,128)S(1)}, u32[]{:S(2)}, u32[]{:S(2)}) collective-permute-start(f32[8,128]{1,0:T(8,128)S(1)} %add.12), channel_id=1, source_target_pairs={{0,4},{2,6},{4,0},{6,2},{1,5},{3,7},{5,1},{7,3},{8,12},{10,14},{12... | collective-permute-start | bytes 12296 | tf_op jit(solution)/shard_map/ppermute | solution.py:460
  55.5 1.1 %collective-permute-done.5 = f32[8,128]{1,0:T(8,128)S(1)} collective-permute-done((f32[8,128]{1,0:T(8,128)S(1)}, f32[8,128]{1,0:T(8,128)S(1)}, u32[]{:S(2)}, u32[]{:S(2)}) %collective-permute-start.5) | collective-permute-done | bytes 4128 | tf_op jit(solution)/shard_map/ppermute | solution.py:460
  56.6 2.5 %collective-permute-start.4 = (f32[8,128]{1,0:T(8,128)S(1)}, f32[8,128]{1,0:T(8,128)S(1)}, u32[]{:S(2)}, u32[]{:S(2)}) collective-permute-start(f32[8,128]{1,0:T(8,128)S(1)} %add.12), channel_id=1, source_target_pairs={{0,6},{2,0},{4,2},{6,4},{1,7},{3,1},{5,3},{7,5},{8,14},{10,8},{12,... | collective-permute-start | bytes 12296 | tf_op jit(solution)/shard_map/ppermute | solution.py:460
  59.1 4.0 %steps.1.stepped = f32[3,2048,256]{2,1,0:T(8,128)S(1)} custom-call(bf16[16,48,256]{2,1,0:T(8,128)(2,1)S(1)} %all-to-all-done.1.gathered, bf16[2048,256]{1,0:T(8,128)(2,1)} %qb.3, bf16[2048,256]{1,0:T(8,128)(2,1)} %fb.3, bf16[2048,256]{1,0:T(8,128)(2,1)} %ob.3), custom_call_target="tpu_custom_call" | custom-call | flops 805306368 | bytes 9437184 | tf_op jit(solution)/shard_map/steps/pallas_call | solution.py:333
  63.2 1.5 %apply_far.1 = (f32[128,256]{1,0:T(8,128)}, f32[128,256]{1,0:T(8,128)}, f32[128,256]{1,0:T(8,128)}, bf16[3,4,128,256]{3,2,1,0:T(8,128)(2,1)S(1)}) custom-call(s32[2]{0:T(128)S(1)} %pad_add_fusion.me, f32[8,128]{1,0:T(8,128)S(1)} %add_add_fusion.totals, f32[3,2048,256]{2,1,0:T(8,128)S(1)} %steps.1.stepped, bf16[4,128,768]{2,1,0:T(8,128)(2,1)S(1)} %copy-done.3), custom_call_target="tpu_custom_call" | custom-call | flops 8388608 | bytes 3145728 | tf_op jit(solution)/shard_map/apply_far/pallas_call | solution.py:384
  64.7 2.6 %apply_near.1 = (bf16[2048,256]{1,0:T(8,128)(2,1)}, bf16[2048,256]{1,0:T(8,128)(2,1)}, bf16[2048,256]{1,0:T(8,128)(2,1)}) custom-call(s32[2]{0:T(128)S(1)} %pad_add_fusion.me, f32[8,128]{1,0:T(8,128)S(1)} %add_add_fusion.totals, f32[3,2048,256]{2,1,0:T(8,128)S(1)} %steps.1.stepped, bf16[3,4,128,256]{3,2,1,0:T(8,128)(2,1)S(1)} %get-tuple-element.50.pieces, ...), custom_call_target="tpu_custom_call" | custom-call | flops 16777216 | bytes 9437184 | tf_op jit(solution)/shard_map/apply_near/pallas_call | solution.py:426
  (25 shorter events, 2.0 us)
Async XLA Ops:
  0.7 7.3 %copy-start = (bf16[2048,256]{1,0:T(8,128)(2,1)S(1)}, bf16[2048,256]{1,0:T(8,128)(2,1)}, u32[]{:S(2)}) copy-start(bf16[2048,256]{1,0:T(8,128)(2,1)} %qc.3) | copy-start | bytes 3145732
  0.7 7.3 %copy-start.1 = (bf16[2048,256]{1,0:T(8,128)(2,1)S(1)}, bf16[2048,256]{1,0:T(8,128)(2,1)}, u32[]{:S(2)}) copy-start(bf16[2048,256]{1,0:T(8,128)(2,1)} %fc.3) | copy-start | bytes 3145732
  0.7 7.3 %copy-start.2 = (bf16[2048,256]{1,0:T(8,128)(2,1)S(1)}, bf16[2048,256]{1,0:T(8,128)(2,1)}, u32[]{:S(2)}) copy-start(bf16[2048,256]{1,0:T(8,128)(2,1)} %mixed.3) | copy-start | bytes 3145732
  6.5 3.7 %collective-permute-start.1 = (bf16[1024,512]{1,0:T(8,128)(2,1)S(1)}, bf16[1024,512]{1,0:T(8,128)(2,1)S(1)}, u32[]{:S(2)}, u32[]{:S(2)}) collective-permute-start(bf16[1024,512]{1,0:T(8,128)(2,1)S(1)} %get-tuple-element.33.own), channel_id=1, source_target_pairs={{0,1},{1,0},{2,3},{3,2},{4,5},{5,4},{6,7},{7,6},{8,9},{9,8},{10,11... | collective-permute-start | bytes 3145736 | tf_op jit(solution)/shard_map/ppermute | solution.py:495
  9.9 2.0 %collective-permute-start = (bf16[1024,256]{1,0:T(8,128)(2,1)S(1)}, bf16[1024,256]{1,0:T(8,128)(2,1)S(1)}, u32[]{:S(2)}, u32[]{:S(2)}) collective-permute-start(bf16[1024,256]{1,0:T(8,128)(2,1)S(1)} %get-tuple-element.37), channel_id=1, source_target_pairs={{0,1},{1,0},{2,3},{3,2},{4,5},{5,4},{6,7},{7,6},{8,9},{9,8},{10,11... | collective-permute-start | bytes 1572872 | tf_op jit(solution)/shard_map/ppermute | solution.py:497
  12.9 17.5 %all-to-all-start = ((bf16[16,48,256]{2,1,0:T(8,128)(2,1)}), bf16[16,48,256]{2,1,0:T(8,128)(2,1)S(1)}, u32[]{:S(2)}, u32[]{:S(2)}) async-start(bf16[16,48,256]{2,1,0:T(8,128)(2,1)} %contract_far.1), calls=%async_computation | async-start | bytes 786432 | tf_op jit(solution)/shard_map/all_to_all | solution.py:503
  20.8 14.2 %collective-permute-start.6 = (bf16[128,768]{1,0:T(8,128)(2,1)S(1)}, bf16[128,768]{1,0:T(8,128)(2,1)S(1)}, u32[]{:S(2)}, u32[]{:S(2)}) collective-permute-start(bf16[128,768]{1,0:T(8,128)(2,1)S(1)} %get-tuple-element.40.refs_0_), channel_id=1, source_target_pairs={{0,64},{8,72},{16,80},{24,88},{32,96},{40,104},{48,112},{56,120},{... | collective-permute-start | bytes 589832 | tf_op jit(solution)/shard_map/ppermute | solution.py:447
  23.7 11.4 %collective-permute-start.7 = (bf16[128,768]{1,0:T(8,128)(2,1)S(1)}, bf16[128,768]{1,0:T(8,128)(2,1)S(1)}, u32[]{:S(2)}, u32[]{:S(2)}) collective-permute-start(bf16[128,768]{1,0:T(8,128)(2,1)S(1)} %get-tuple-element.40.refs_0_), channel_id=1, source_target_pairs={{0,16},{8,24},{16,0},{24,8},{32,48},{40,56},{48,32},{56,40},{64,80... | collective-permute-start | bytes 589832 | tf_op jit(solution)/shard_map/ppermute | solution.py:447
  26.3 12.9 %collective-permute-start.8 = (bf16[128,768]{1,0:T(8,128)(2,1)S(1)}, bf16[128,768]{1,0:T(8,128)(2,1)S(1)}, u32[]{:S(2)}, u32[]{:S(2)}) collective-permute-start(bf16[128,768]{1,0:T(8,128)(2,1)S(1)} %get-tuple-element.40.refs_0_), channel_id=1, source_target_pairs={{0,80},{8,88},{16,64},{24,72},{32,112},{40,120},{48,96},{56,104},{... | collective-permute-start | bytes 589832 | tf_op jit(solution)/shard_map/ppermute | solution.py:447
  31.4 11.8 %all-to-all-start.1 = ((bf16[16,48,256]{2,1,0:T(8,128)(2,1)}), bf16[16,48,256]{2,1,0:T(8,128)(2,1)S(1)}, u32[]{:S(2)}, u32[]{:S(2)}) async-start(bf16[16,48,256]{2,1,0:T(8,128)(2,1)} %get-tuple-element.39), calls=%async_computation.1 | async-start | bytes 786432 | tf_op jit(solution)/shard_map/all_to_all | solution.py:505
  40.2 23.0 %copy-start.3 = (bf16[4,128,768]{2,1,0:T(8,128)(2,1)S(1)}, bf16[4,128,768]{2,1,0:T(8,128)(2,1)}, u32[]{:S(2)}) copy-start(bf16[4,128,768]{2,1,0:T(8,128)(2,1)} %collected.1.four) | copy-start | bytes 2359300
  40.2 24.5 %collective-permute-start.9 = (bf16[4,128,768]{2,1,0:T(8,128)(2,1)}, bf16[4,128,768]{2,1,0:T(8,128)(2,1)S(1)}, u32[]{:S(2)}, u32[]{:S(2)}) collective-permute-start(bf16[4,128,768]{2,1,0:T(8,128)(2,1)} %collected.1.four), channel_id=1, source_target_pairs={{0,96},{8,104},{16,112},{24,120},{32,0},{40,8},{48,16},{56,24},{64... | collective-permute-start | bytes 2359304 | tf_op jit(solution)/shard_map/ppermute | solution.py:447
  41.1 23.6 %collective-permute-start.10 = (bf16[4,128,768]{2,1,0:T(8,128)(2,1)}, bf16[4,128,768]{2,1,0:T(8,128)(2,1)S(1)}, u32[]{:S(2)}, u32[]{:S(2)}) collective-permute-start(bf16[4,128,768]{2,1,0:T(8,128)(2,1)} %collected.1.four), channel_id=1, source_target_pairs={{0,24},{8,0},{16,8},{24,16},{32,56},{40,32},{48,40},{56,48},{64,88... | collective-permute-start | bytes 2359304 | tf_op jit(solution)/shard_map/ppermute | solution.py:447
  42.0 22.7 %collective-permute-start.11 = (bf16[4,128,768]{2,1,0:T(8,128)(2,1)}, bf16[4,128,768]{2,1,0:T(8,128)(2,1)S(1)}, u32[]{:S(2)}, u32[]{:S(2)}) collective-permute-start(bf16[4,128,768]{2,1,0:T(8,128)(2,1)} %collected.1.four), channel_id=1, source_target_pairs={{0,40},{8,48},{16,56},{24,32},{32,72},{40,80},{48,88},{56,64},{64,... | collective-permute-start | bytes 2359304 | tf_op jit(solution)/shard_map/ppermute | solution.py:447
  43.5 8.9 %collective-permute-start.2 = (f32[8,128]{1,0:T(8,128)S(1)}, f32[8,128]{1,0:T(8,128)S(1)}, u32[]{:S(2)}, u32[]{:S(2)}) collective-permute-start(f32[8,128]{1,0:T(8,128)S(1)} %squares.1), channel_id=1, source_target_pairs={{0,1},{1,0},{2,3},{3,2},{4,5},{5,4},{6,7},{7,6},{8,9},{9,8},{10,11... | collective-permute-start | bytes 12296 | tf_op jit(solution)/shard_map/ppermute | solution.py:458
  52.4 4.3 %collective-permute-start.5 = (f32[8,128]{1,0:T(8,128)S(1)}, f32[8,128]{1,0:T(8,128)S(1)}, u32[]{:S(2)}, u32[]{:S(2)}) collective-permute-start(f32[8,128]{1,0:T(8,128)S(1)} %add.12), channel_id=1, source_target_pairs={{0,4},{2,6},{4,0},{6,2},{1,5},{3,7},{5,1},{7,3},{8,12},{10,14},{12... | collective-permute-start | bytes 12296 | tf_op jit(solution)/shard_map/ppermute | solution.py:460
  55.2 7.9 %collective-permute-start.3 = (f32[8,128]{1,0:T(8,128)S(1)}, f32[8,128]{1,0:T(8,128)S(1)}, u32[]{:S(2)}, u32[]{:S(2)}) collective-permute-start(f32[8,128]{1,0:T(8,128)S(1)} %add.12), channel_id=1, source_target_pairs={{0,2},{2,4},{4,6},{6,0},{1,3},{3,5},{5,7},{7,1},{8,10},{10,12},{12... | collective-permute-start | bytes 12296 | tf_op jit(solution)/shard_map/ppermute | solution.py:460
  56.6 6.5 %collective-permute-start.4 = (f32[8,128]{1,0:T(8,128)S(1)}, f32[8,128]{1,0:T(8,128)S(1)}, u32[]{:S(2)}, u32[]{:S(2)}) collective-permute-start(f32[8,128]{1,0:T(8,128)S(1)} %add.12), channel_id=1, source_target_pairs={{0,6},{2,0},{4,2},{6,4},{1,7},{3,1},{5,3},{7,5},{8,14},{10,8},{12,... | collective-permute-start | bytes 12296 | tf_op jit(solution)/shard_map/ppermute | solution.py:460

commit v5 on v4

--- a/solution.py
+++ b/solution.py
@@ -11,7 +11,7 @@
 FS = ("fs_0", "fs_1")
 TP = ("tp_0", "tp_1")
 MATS = 3
-IN_CUTS = (0, 512, 2048)
+IN_CUTS = (0, 1024, 2048)
 SIDE = 4
 GRANT = 24 * 1024 * 1024
 
@@ -53,10 +53,10 @@
     return pl.ds(pl.multiple_of(which * half, half), half)
 
 
-def reduce_in_kernel(core, source, qb, fb, qw, fw, ow, grad, ob, *refs):
+def reduce_in_kernel(core, source, qb, fb, qw, fw, ow, grad, ob, qc, fc, mixed, *refs):
     state, refs = refs[: 2 * MATS], refs[2 * MATS :]
-    out, rounded, packed, grad_half, ob_held = refs[:5]
-    rows_in, basis_in, weights_in, sums, sems, weight_sems, state_sems, next_sems = refs[5:]
+    out, rounded, packed, grad_half, ob_held, cots = refs[:6]
+    rows_in, basis_in, weights_in, sums, sems, weight_sems, state_sems, next_sems = refs[6:]
     bases, weights = (qb, fb), (qw, fw, ow)
     mine = half_of(core[0], out.shape[0])
     copies = []
@@ -77,6 +77,10 @@
     next_copies = [
         pltpu.make_async_copy(grad.at[mine, :], grad_half, next_sems.at[0]),
         pltpu.make_async_copy(ob, ob_held, next_sems.at[1]),
+        *(
+            pltpu.make_async_copy(a.at[mine, :], cots.at[m], next_sems.at[2 + m])
+            for m, a in enumerate((qc, fc, mixed))
+        ),
     ]
     for copy in (*copies[0], *weight_copies, *copies[1]):
         copy.start()
@@ -84,7 +88,7 @@
         at = slice(low, high)
         for copy in copies[c]:
             copy.wait()
-        if c > 0:
+        if c == 0:
             for copy in (*next_copies, *state_copies):
                 copy.start()
         for m in range(len(bases)):
@@ -103,20 +107,21 @@
         copy.wait()
 
 
-def reduce_in(core, source, bases, weights, grad, ob, state):
+def reduce_in(core, source, bases, weights, grad, ob, cotangents, state):
     tokens, width = source.shape
     half, count = tokens // 2, len(bases)
     rows, cols = weights[0].shape
     return pl.pallas_call(
         reduce_in_kernel,
-        in_specs=[SMEM, *(HBM for _ in range(3 + count + MATS + len(state)))],
-        out_specs=[VMEM for _ in range(5)],
+        in_specs=[SMEM, *(HBM for _ in range(3 + count + 2 * MATS + len(state)))],
+        out_specs=[VMEM for _ in range(6)],
         out_shape=[
             pltpu.VMEM((half, count * RANK), BF16),
             pltpu.VMEM((rows, MATS * cols), BF16),
             pltpu.VMEM((len(state), *state[0].shape), F32),
             pltpu.VMEM((half, width), BF16),
             pltpu.VMEM((width, RANK), BF16),
+            pltpu.VMEM((MATS, half, cols), BF16),
         ],
         scratch_shapes=[
             pltpu.VMEM((half, width), BF16),
@@ -126,46 +131,54 @@
             pltpu.SemaphoreType.DMA((len(IN_CUTS) - 1, 1 + count)),
             pltpu.SemaphoreType.DMA((MATS,)),
             pltpu.SemaphoreType.DMA((len(state),)),
-            pltpu.SemaphoreType.DMA((2,)),
-        ],
-        compiler_params=params(),
-        cost_estimate=cost(2 * half * RANK * width * count, 6 << 20),
+            pltpu.SemaphoreType.DMA((2 + MATS,)),
+        ],
+        compiler_params=params(),
+        cost_estimate=cost(2 * half * RANK * width * count, 14 << 20),
         name="reduce_in",
-    )(core, *in_hbm(source, *bases, *weights, grad, ob, *state))
-
-
-def reduce_out_kernel(core, own, qc, fc, mixed, source, basis, out, sums):
-    mine = half_of(core[0], out.shape[0])
+    )(core, *in_hbm(source, *bases, *weights, grad, ob, *cotangents, *state))
+
+
+def reduce_out_kernel(core, own, cots, source, basis, qc, fc, mixed, out, sums, rest, sems):
+    theirs = half_of(1 - core[0], out.shape[0])
+    copies = [
+        pltpu.make_async_copy(a.at[theirs, :], rest.at[m], sems.at[m])
+        for m, a in enumerate((qc, fc, mixed))
+    ]
+    for copy in copies:
+        copy.start()
     out[...] = jnp.dot(source[...], basis[...], preferred_element_type=F32).astype(BF16)
-    for m, cotangent in enumerate((qc, fc)):
-        sums[m] = contract_rows(own[:, m * RANK : (m + 1) * RANK], cotangent[mine, :])
-    sums[2] = contract_rows(out[...], mixed[mine, :])
-
-
-def reduce_out(core, own, cotangents, source, basis):
+    for m in range(2):
+        sums[m] = contract_rows(own[:, m * RANK : (m + 1) * RANK], cots[m])
+    sums[2] = contract_rows(out[...], cots[2])
+    for copy in copies:
+        copy.wait()
+
+
+def reduce_out(core, own, cots, source, basis, cotangents):
     half, width = source.shape
-    cols = cotangents[0].shape[1]
+    cols = cots.shape[2]
     return pl.pallas_call(
         reduce_out_kernel,
-        in_specs=[SMEM, *(VMEM for _ in range(3 + MATS))],
-        out_specs=[VMEM, VMEM],
-        out_shape=[pltpu.VMEM((half, RANK), BF16), pltpu.VMEM((MATS, RANK, cols), F32)],
+        in_specs=[SMEM, *(VMEM for _ in range(4)), *(HBM for _ in cotangents)],
+        out_specs=[VMEM for _ in range(3)],
+        out_shape=[
+            pltpu.VMEM((half, RANK), BF16),
+            pltpu.VMEM((MATS, RANK, cols), F32),
+            pltpu.VMEM(cots.shape, BF16),
+        ],
+        scratch_shapes=[pltpu.SemaphoreType.DMA((MATS,))],
         compiler_params=params(),
         cost_estimate=cost(2 * half * RANK * (width + 3 * cols), 6 << 20),
         name="reduce_out",
-    )(core, *in_vmem(own, *cotangents, source, basis))
-
-
-def contract_one(sums, other, cotangent, theirs, m, k):
-    return sums[m] + contract_rows(other[:, k * RANK : (k + 1) * RANK], cotangent[theirs, :])
-
-
-def contract_near_kernel(core, sums, other, qc, fc, out, held, sems):
+    )(core, *in_vmem(own, cots, source, basis), *in_hbm(*cotangents))
+
+
+def contract_near_kernel(sums, other, cots, out, held, sems):
     groups, rows = out.shape[0], out.shape[1] // MATS
-    theirs = half_of(1 - core[0], other.shape[0])
     copies = []
-    for m, cotangent in enumerate((qc, fc)):
-        total = contract_one(sums, other, cotangent, theirs, m, m)
+    for m in range(2):
+        total = sums[m] + contract_rows(other[:, m * RANK : (m + 1) * RANK], cots[m])
         held[m] = total.astype(BF16).reshape(groups, rows, total.shape[1])
         copies.append(
             pltpu.make_async_copy(held.at[m], out.at[:, m * rows : (m + 1) * rows, :], sems.at[m])
@@ -175,12 +188,12 @@
         copy.wait()
 
 
-def contract_near(core, sums, other, cotangents, groups):
+def contract_near(sums, other, cots, groups):
     cols = sums.shape[2]
     rows = RANK // groups
     return pl.pallas_call(
         contract_near_kernel,
-        in_specs=[SMEM, *(VMEM for _ in range(4))],
+        in_specs=[VMEM for _ in range(3)],
         out_specs=HBM,
         out_shape=pltpu.HBM((groups, MATS * rows, cols), BF16),
         scratch_shapes=[
@@ -190,35 +203,34 @@
         compiler_params=params(),
         cost_estimate=cost(4 * other.shape[0] * RANK * cols, 2 << 20),
         name="contract_near",
-    )(core, *in_vmem(sums, other, *cotangents[:2]))
-
-
-def contract_far_kernel(core, sums, other, mixed, _, out, held, sems):
+    )(*in_vmem(sums, other, cots))
+
+
+def contract_far_kernel(sums, other, cots, _, out, held, sems):
     groups, rows = out.shape[0], out.shape[1] // MATS
-    theirs = half_of(1 - core[0], other.shape[0])
-    total = contract_one(sums, other, mixed, theirs, 2, 0)
+    total = sums[2] + contract_rows(other[...], cots[2])
     held[...] = total.astype(BF16).reshape(groups, rows, total.shape[1])
     copy = pltpu.make_async_copy(held, out.at[:, 2 * rows : 3 * rows, :], sems.at[0])
     copy.start()
     copy.wait()
 
 
-def contract_far(core, sums, other, mixed, blocks):
+def contract_far(sums, other, cots, blocks):
     groups, rows, cols = blocks.shape
     return pl.pallas_call(
         contract_far_kernel,
-        in_specs=[SMEM, *(VMEM for _ in range(3)), HBM],
+        in_specs=[*(VMEM for _ in range(3)), HBM],
         out_specs=HBM,
         out_shape=pltpu.HBM(blocks.shape, BF16),
         scratch_shapes=[
             pltpu.VMEM((groups, rows // MATS, cols), BF16),
             pltpu.SemaphoreType.DMA((1,)),
         ],
-        input_output_aliases={4: 0},
+        input_output_aliases={3: 0},
         compiler_params=params(),
         cost_estimate=cost(2 * other.shape[0] * RANK * cols, 1 << 20),
         name="contract_far",
-    )(core, *in_vmem(sums, other, mixed), *in_hbm(blocks))
+    )(*in_vmem(sums, other, cots), *in_hbm(blocks))
 
 
 def moment_kernel(arrived, held, *refs):
@@ -355,14 +367,14 @@
     return lax.rsqrt(totals[m : m + 1, :1] * (1.0 / (RANK * WIDTH)) + 1e-06)
 
 
-def updated(weight, j, m, factor, stepped, at):
-    cols = stepped.shape[2]
+def updated(weight, j, m, change, at):
+    cols = change.shape[2]
     old = weight[j, :, m * cols : (m + 1) * cols].astype(F32)
-    return (old - factor * stepped[m, at, :]).astype(BF16)
+    return (old - change[m, at, :]).astype(BF16)
 
 
 def apply_far_kernel(me, totals, stepped, four, *refs):
-    updates, pieces, held, sems = refs[:MATS], refs[MATS], refs[MATS + 1], refs[MATS + 2]
+    updates, (pieces, change, held, sems) = refs[:MATS], refs[MATS:]
     rows = held.shape[1]
     mine = pl.ds(pl.multiple_of((me[0] * SIDE + me[1]) * rows, rows), rows)
     stores = []
@@ -371,9 +383,9 @@
         stores.append(pltpu.make_async_copy(held.at[m], updates[m], sems.at[m]))
         stores[m].start()
     for m in range(MATS):
-        factor = 0.05 * scale_of(totals, m)
+        change[m] = (0.05 * scale_of(totals, m)) * stepped[m]
         for j in range(len(FAR)):
-            pieces[m, j] = updated(four, j, m, factor, stepped, rows_at(me, NEAR[0], j, rows))
+            pieces[m, j] = updated(four, j, m, change, rows_at(me, NEAR[0], j, rows))
     for store in stores:
         store.wait()
 
@@ -384,10 +396,11 @@
     results = pl.pallas_call(
         apply_far_kernel,
         in_specs=[SMEM, VMEM, VMEM, VMEM],
-        out_specs=[*(HBM for _ in range(MATS)), VMEM],
+        out_specs=[*(HBM for _ in range(MATS)), VMEM, VMEM],
         out_shape=[
             *(pltpu.HBM((rows, cols), F32) for _ in range(MATS)),
             pltpu.VMEM((MATS, count, rows, cols), BF16),
+            pltpu.VMEM(stepped.shape, F32),
         ],
         scratch_shapes=[
             pltpu.VMEM((MATS, rows, cols), F32),
@@ -397,21 +410,20 @@
         cost_estimate=cost(1 << 23, 3 << 20),
         name="apply_far",
     )(me, *in_vmem(totals, stepped, four))
-    return results[:MATS], results[MATS]
-
-
-def apply_near_kernel(me, totals, stepped, pieces, *refs):
+    return results[:MATS], results[MATS], results[MATS + 1]
+
+
+def apply_near_kernel(me, change, pieces, *refs):
     weights, copies, (held, sems) = refs[:MATS], refs[MATS : 2 * MATS], refs[2 * MATS :]
     rows = pieces.shape[2]
     stores = []
     for m in range(MATS):
-        factor = 0.05 * scale_of(totals, m)
 
         def block(j, carry):
             held[m, rows_at(me, NEAR[0], j, rows), :] = pieces[m, j]
             for near, weight in zip(NEAR[1:], weights):
                 at = rows_at(me, near, j, rows)
-                held[m, at, :] = updated(weight, j, m, factor, stepped, at)
+                held[m, at, :] = updated(weight, j, m, change, at)
             return carry
 
         lax.fori_loop(0, len(FAR), block, 0)
@@ -421,11 +433,11 @@
         store.wait()
 
 
-def apply_near(me, totals, stepped, pieces, weights):
-    width, cols = stepped.shape[1:]
+def apply_near(me, change, pieces, weights):
+    width, cols = change.shape[1:]
     return pl.pallas_call(
         apply_near_kernel,
-        in_specs=[SMEM, *(VMEM for _ in range(3 + len(weights)))],
+        in_specs=[SMEM, *(VMEM for _ in range(2 + len(weights)))],
         out_specs=[HBM for _ in range(MATS)],
         out_shape=[pltpu.HBM((width, cols), BF16) for _ in range(MATS)],
         scratch_shapes=[
@@ -435,7 +447,7 @@
         compiler_params=params(),
         cost_estimate=cost(1 << 24, 9 << 20),
         name="apply_near",
-    )(me, *in_vmem(totals, stepped, pieces, *weights))
+    )(me, *in_vmem(change, pieces, *weights))
 
 
 def moved_by(value, offset):
@@ -483,20 +495,21 @@
     core = lax.axis_index("tp_1").astype(jnp.int32).reshape(1)
     me = jnp.stack([lax.axis_index("fs_0"), lax.axis_index("fs_1")]).astype(jnp.int32)
 
-    own, weights, packed, grad_half, ob_held = reduce_in(
+    own, weights, packed, grad_half, ob_held, cots = reduce_in(
         core,
         saved_input,
         bases[:2],
         (query_weight, forget_weight, out_weight),
         out_cotangent,
         out_basis,
+        cotangents,
         state,
     )
     other = lax.ppermute(own, "tp_1", [(0, 1), (1, 0)])
-    own_out, sums = reduce_out(core, own, cotangents, grad_half, ob_held)
+    own_out, sums, rest = reduce_out(core, own, cots, grad_half, ob_held, cotangents)
     other_out = lax.ppermute(own_out, "tp_1", [(0, 1), (1, 0)])
-    blocks = contract_near(core, sums, other, cotangents, groups)
-    blocks = contract_far(core, sums, other_out, mixed_output, blocks)
+    blocks = contract_near(sums, other, rest, groups)
+    blocks = contract_far(sums, other_out, rest, blocks)
     four = collected((weights, *gathered_by(weights, FAR)))
     near_weights = gathered_by(four, NEAR)
 
@@ -505,8 +518,8 @@
     gathered = lax.all_to_all(directions, FS, 0, 0, tiled=True)
     totals = summed_over_tp(squares(gathered))
     stepped = steps(gathered, bases)
-    updates, pieces = apply_far(me, totals, stepped, four)
-    copies = apply_near(me, totals, stepped, pieces, near_weights)
+    updates, pieces, change = apply_far(me, totals, stepped, four)
+    copies = apply_near(me, change, pieces, near_weights)
     return (*updates, *state_new, *copies)
 
 

time: 67.7 us -> 66.5 us (0.982)
  starting transfers between devices: 35 us -> 34.1 us
    ppermute x3, starting transfers between devices: 5.53 us -> 4.22 us  [summed_over_tp(): lax.ppermute(value, 'tp_0', [(i, (i + far) % SIDE) for i in range(SIDE)])]
    ppermute x6, starting transfers between devices: 8.38 us -> 9.59 us  [moved_by(): return lax.ppermute(value, FS, pairs)]
    ppermute x1, starting transfers between devices: 8.1 us -> 7.3 us  [summed_over_tp(): value = value + lax.ppermute(value, 'tp_1', [(0, 1), (1, 0)])]
  transfers between devices with their start and end apart: 14 -> 14, of which waited for: 7 -> 6; matrix products, arithmetic and copies ran while one was open for 0% -> 0% of each run, Pallas kernels for 16% -> 17%
where the time goes in v5:
time: 66.5 us; the launch traced here: 65.5 us
  starting transfers between devices  34.1 us (51%)
  Pallas kernels  19.6 us (29%)
  waiting for transfers between devices  10.9 us (16%)
  between operations  0.81 us (1%)
    ppermute x6, starting transfers between devices, moved_by(): return lax.ppermute(value, FS, pairs)  9.59 us
    all_to_all x1, starting transfers between devices, body(): arrived = lax.all_to_all(blocks, FS, 0, 0, tiled=True)  7.89 us
    ppermute x1, starting transfers between devices, summed_over_tp(): value = value + lax.ppermute(value, 'tp_1', [(0, 1), (1, 0)])  7.3 us
    pallas_call x1, Pallas kernels, reduce_in(): pl.pallas_call(reduce_in_kernel, in_specs=[SMEM, *(HBM for _ in range(3 +...  5.29 us
    ppermute x6, waiting for transfers between devices, moved_by(): return lax.ppermute(value, FS, pairs)  4.23 us
    ppermute x3, starting transfers between devices, summed_over_tp(): lax.ppermute(value, 'tp_0', [(i, (i + far) % SIDE) for i in range(SIDE)])  4.22 us
    pallas_call x1, Pallas kernels, steps(): pl.pallas_call(step_kernel, in_specs=[VMEM, *(HBM for _ in bases)], out_s...  3.99 us
    all_to_all x1, waiting for transfers between devices, body(): arrived = lax.all_to_all(blocks, FS, 0, 0, tiled=True)  3.88 us
  transfers between devices with their start and end apart: 14, of which 6 were waited for; matrix products, arithmetic and copies ran while one was open for 0% of the time, Pallas kernels for 17%

profile of v5, /device:TPU:1, one launch (start us, length us, event | category | flops | bytes accessed | tf_op | source)
XLA Modules:
  0.0 65.5 jit_solution(5745565033058681715)
XLA Ops:
  0.7 5.3 %reduce_in.1 = (bf16[1024,512]{1,0:T(8,128)(2,1)S(1)}, bf16[128,768]{1,0:T(8,128)(2,1)S(1)}, f32[6,16,256]{2,1,0:T(8,128)S(1)}, bf16[1024,2048]{1,0:T(8,128)(2,1...) custom-call(s32[1]{0:T(128)} %bitcast.2.core, bf16[2048,2048]{1,0:T(8,128)(2,1)} %source.1, ...), custom_call_target="tpu_custom_call" | custom-call | flops 2147483648 | bytes 14680064 | tf_op jit(solution)/shard_map/reduce_in/pallas_call | solution.py:114
  5.9 1.5 %collective-permute-start.1 = (bf16[1024,512]{1,0:T(8,128)(2,1)S(1)}, bf16[1024,512]{1,0:T(8,128)(2,1)S(1)}, u32[]{:S(2)}, u32[]{:S(2)}) collective-permute-start(bf16[1024,512]{1,0:T(8,128)(2,1)S(1)} %get-tuple-element.36.own), channel_id=1, source_target_pairs={{0,1},{1,0},{2,3},{3,2},{4,5},{5,4},{6,7},{7,6},{8,9},{9,8},{10,11... | collective-permute-start | bytes 3145736 | tf_op jit(solution)/shard_map/ppermute | solution.py:508
  7.4 1.9 %reduce_out.1 = (bf16[1024,256]{1,0:T(8,128)(2,1)S(1)}, f32[3,256,256]{2,1,0:T(8,128)S(1)}, bf16[3,1024,256]{2,1,0:T(8,128)(2,1)S(1)}) custom-call(s32[1]{0:T(128)} %bitcast.2.core, bf16[1024,512]{1,0:T(8,128)(2,1)S(1)} %get-tuple-element.36.own, bf16[3,1024,256]{2,1,0:T(8,128)(2,1)S(1)} %get-tuple-element.37.cots, ...), custom_call_target="tpu_custom_call" | custom-call | flops 1476395008 | bytes 6291456 | tf_op jit(solution)/shard_map/reduce_out/pallas_call | solution.py:161
  9.7 1.2 %contract_near.1._ = bf16[16,48,256]{2,1,0:T(8,128)(2,1)} custom-call(f32[3,256,256]{2,1,0:T(8,128)S(1)} %get-tuple-element.40.sums, bf16[1024,512]{1,0:T(8,128)(2,1)S(1)} %collective-permute-done.1.other, bf16[3,1024,256]{2,1,0:T(8,128)(2,1)S(1)} %get-tuple-element.42.cots), custom_call_target="tpu_custom_call" | custom-call | flops 268435456 | bytes 2097152 | tf_op jit(solution)/shard_map/contract_near/pallas_call | solution.py:194
  11.3 1.0 %contract_far.1 = bf16[16,48,256]{2,1,0:T(8,128)(2,1)} custom-call(f32[3,256,256]{2,1,0:T(8,128)S(1)} %get-tuple-element.40.sums, bf16[1024,256]{1,0:T(8,128)(2,1)S(1)} %collective-permute-done.other, bf16[3,1024,256]{2,1,0:T(8,128)(2,1)S(1)} %get-tuple-element.42.cots, bf16[16,48,256]{2,1,0:T(8,128)(2,1)} %contract_near.1._), custom_call_target="tpu_custom_call", output_to_operand_aliasing={{}: (3, {})} | custom-call | flops 134217728 | bytes 1048576 | tf_op jit(solution)/shard_map/contract_far/pallas_call | solution.py:220
  12.3 7.9 %all-to-all-start = ((bf16[16,48,256]{2,1,0:T(8,128)(2,1)}), bf16[16,48,256]{2,1,0:T(8,128)(2,1)S(1)}, u32[]{:S(2)}, u32[]{:S(2)}) async-start(bf16[16,48,256]{2,1,0:T(8,128)(2,1)} %contract_far.1), calls=%async_computation | async-start | bytes 786432 | tf_op jit(solution)/shard_map/all_to_all | solution.py:516
  20.2 2.9 %collective-permute-start.6 = (bf16[128,768]{1,0:T(8,128)(2,1)S(1)}, bf16[128,768]{1,0:T(8,128)(2,1)S(1)}, u32[]{:S(2)}, u32[]{:S(2)}) collective-permute-start(bf16[128,768]{1,0:T(8,128)(2,1)S(1)} %get-tuple-element.45.refs_0_), channel_id=1, source_target_pairs={{0,64},{8,72},{16,80},{24,88},{32,96},{40,104},{48,112},{56,120},{... | collective-permute-start | bytes 589832 | tf_op jit(solution)/shard_map/ppermute | solution.py:459
  23.1 2.7 %collective-permute-start.7 = (bf16[128,768]{1,0:T(8,128)(2,1)S(1)}, bf16[128,768]{1,0:T(8,128)(2,1)S(1)}, u32[]{:S(2)}, u32[]{:S(2)}) collective-permute-start(bf16[128,768]{1,0:T(8,128)(2,1)S(1)} %get-tuple-element.45.refs_0_), channel_id=1, source_target_pairs={{0,16},{8,24},{16,0},{24,8},{32,48},{40,56},{48,32},{56,40},{64,80... | collective-permute-start | bytes 589832 | tf_op jit(solution)/shard_map/ppermute | solution.py:459
  26.0 3.9 %all-to-all-done.arrived = bf16[16,48,256]{2,1,0:T(8,128)(2,1)S(1)} async-done(((bf16[16,48,256]{2,1,0:T(8,128)(2,1)}), bf16[16,48,256]{2,1,0:T(8,128)(2,1)S(1)}, u32[]{:S(2)}, u32[]{:S(2)}) %all-to-all-start) | async-done | bytes 393248 | tf_op jit(solution)/shard_map/all_to_all | solution.py:516
  29.9 1.0 %moments.1 = (f32[16,256]{1,0:T(8,128)}, f32[16,256]{1,0:T(8,128)}, f32[16,256]{1,0:T(8,128)}, f32[16,256]{1,0:T(8,128)}, f32[16,256]{1,0:T(8,128)}, /*index=5*/f32[16,256]{1,0:T(8,128)}, bf16[16,48,256]{2,1,0:T(8,128)(2,1)}) custom-call(bf16[16,48,256]{2,1,0:T(8,128)(2,1)S(1)} %all-to-all-done.arrived, f32[6,16,256]{2,1,0:T(8,128)S(1)} %get-tuple-element.43.held), custom_call_target="tpu_custom_call" | custom-call | flops 4194304 | bytes 1048576 | tf_op jit(solution)/shard_map/moments/pallas_call | solution.py:267
  30.9 3.6 %all-to-all-start.1 = ((bf16[16,48,256]{2,1,0:T(8,128)(2,1)}), bf16[16,48,256]{2,1,0:T(8,128)(2,1)S(1)}, u32[]{:S(2)}, u32[]{:S(2)}) async-start(bf16[16,48,256]{2,1,0:T(8,128)(2,1)} %get-tuple-element.44), calls=%async_computation.1 | async-start | bytes 786432 | tf_op jit(solution)/shard_map/all_to_all | solution.py:518
  34.5 4.2 %collective-permute-done.8.refs_3_ = bf16[128,768]{1,0:T(8,128)(2,1)S(1)} collective-permute-done((bf16[128,768]{1,0:T(8,128)(2,1)S(1)}, bf16[128,768]{1,0:T(8,128)(2,1)S(1)}, u32[]{:S(2)}, u32[]{:S(2)}) %collective-permute-start.8) | collective-permute-done | bytes 196640 | tf_op jit(solution)/shard_map/ppermute | solution.py:459
  38.7 0.9 %collected.1.four = bf16[4,128,768]{2,1,0:T(8,128)(2,1)} custom-call(bf16[128,768]{1,0:T(8,128)(2,1)S(1)} %get-tuple-element.45.refs_0_, bf16[128,768]{1,0:T(8,128)(2,1)S(1)} %collective-permute-done.6.refs_1_, bf16[128,768]{1,0:T(8,128)(2,1)S(1)} %collective-permute-done.7.refs_2_, bf16[128,768]{1,0:T(8,128)(2,1)S(1)} %collective-permute-done.8.refs_3_), custom_call_target="tpu_custom_call" | custom-call | flops 1048576 | bytes 2097152 | tf_op jit(solution)/shard_map/collected/pallas_call | solution.py:294
  39.7 0.9 %collective-permute-start.10 = (bf16[4,128,768]{2,1,0:T(8,128)(2,1)}, bf16[4,128,768]{2,1,0:T(8,128)(2,1)S(1)}, u32[]{:S(2)}, u32[]{:S(2)}) collective-permute-start(bf16[4,128,768]{2,1,0:T(8,128)(2,1)} %collected.1.four), channel_id=1, source_target_pairs={{0,24},{8,0},{16,8},{24,16},{32,56},{40,32},{48,40},{56,48},{64,88... | collective-permute-start | bytes 2359304 | tf_op jit(solution)/shard_map/ppermute | solution.py:459
  41.1 2.4 %collective-permute-start.9 = (bf16[4,128,768]{2,1,0:T(8,128)(2,1)}, bf16[4,128,768]{2,1,0:T(8,128)(2,1)S(1)}, u32[]{:S(2)}, u32[]{:S(2)}) collective-permute-start(bf16[4,128,768]{2,1,0:T(8,128)(2,1)} %collected.1.four), channel_id=1, source_target_pairs={{0,96},{8,104},{16,112},{24,120},{32,0},{40,8},{48,16},{56,24},{64... | collective-permute-start | bytes 2359304 | tf_op jit(solution)/shard_map/ppermute | solution.py:459
  43.8 7.3 %collective-permute-start.2 = (f32[8,128]{1,0:T(8,128)S(1)}, f32[8,128]{1,0:T(8,128)S(1)}, u32[]{:S(2)}, u32[]{:S(2)}) collective-permute-start(f32[8,128]{1,0:T(8,128)S(1)} %squares.1), channel_id=1, source_target_pairs={{0,1},{1,0},{2,3},{3,2},{4,5},{5,4},{6,7},{7,6},{8,9},{9,8},{10,11... | collective-permute-start | bytes 12296 | tf_op jit(solution)/shard_map/ppermute | solution.py:470
  51.1 0.8 %collective-permute-done.2 = f32[8,128]{1,0:T(8,128)S(1)} collective-permute-done((f32[8,128]{1,0:T(8,128)S(1)}, f32[8,128]{1,0:T(8,128)S(1)}, u32[]{:S(2)}, u32[]{:S(2)}) %collective-permute-start.2) | collective-permute-done | bytes 4128 | tf_op jit(solution)/shard_map/ppermute | solution.py:470
  51.9 1.2 %collective-permute-start.3 = (f32[8,128]{1,0:T(8,128)S(1)}, f32[8,128]{1,0:T(8,128)S(1)}, u32[]{:S(2)}, u32[]{:S(2)}) collective-permute-start(f32[8,128]{1,0:T(8,128)S(1)} %add.12), channel_id=1, source_target_pairs={{0,2},{2,4},{4,6},{6,0},{1,3},{3,5},{5,7},{7,1},{8,10},{10,12},{12... | collective-permute-start | bytes 12296 | tf_op jit(solution)/shard_map/ppermute | solution.py:472
  53.2 1.5 %collective-permute-start.4 = (f32[8,128]{1,0:T(8,128)S(1)}, f32[8,128]{1,0:T(8,128)S(1)}, u32[]{:S(2)}, u32[]{:S(2)}) collective-permute-start(f32[8,128]{1,0:T(8,128)S(1)} %add.12), channel_id=1, source_target_pairs={{0,6},{2,0},{4,2},{6,4},{1,7},{3,1},{5,3},{7,5},{8,14},{10,8},{12,... | collective-permute-start | bytes 12296 | tf_op jit(solution)/shard_map/ppermute | solution.py:472
  54.6 1.2 %collective-permute-done.3 = f32[8,128]{1,0:T(8,128)S(1)} collective-permute-done((f32[8,128]{1,0:T(8,128)S(1)}, f32[8,128]{1,0:T(8,128)S(1)}, u32[]{:S(2)}, u32[]{:S(2)}) %collective-permute-start.3) | collective-permute-done | bytes 4128 | tf_op jit(solution)/shard_map/ppermute | solution.py:472
  55.8 1.5 %collective-permute-start.5 = (f32[8,128]{1,0:T(8,128)S(1)}, f32[8,128]{1,0:T(8,128)S(1)}, u32[]{:S(2)}, u32[]{:S(2)}) collective-permute-start(f32[8,128]{1,0:T(8,128)S(1)} %add.12), channel_id=1, source_target_pairs={{0,4},{2,6},{4,0},{6,2},{1,5},{3,7},{5,1},{7,3},{8,12},{10,14},{12... | collective-permute-start | bytes 12296 | tf_op jit(solution)/shard_map/ppermute | solution.py:472
  57.4 4.0 %steps.1.stepped = f32[3,2048,256]{2,1,0:T(8,128)S(1)} custom-call(bf16[16,48,256]{2,1,0:T(8,128)(2,1)S(1)} %all-to-all-done.1.gathered, bf16[2048,256]{1,0:T(8,128)(2,1)} %qb.3, bf16[2048,256]{1,0:T(8,128)(2,1)} %fb.3, bf16[2048,256]{1,0:T(8,128)(2,1)} %ob.3), custom_call_target="tpu_custom_call" | custom-call | flops 805306368 | bytes 9437184 | tf_op jit(solution)/shard_map/steps/pallas_call | solution.py:345
  61.4 1.6 %apply_far.1 = (f32[128,256]{1,0:T(8,128)}, f32[128,256]{1,0:T(8,128)}, f32[128,256]{1,0:T(8,128)}, bf16[3,4,128,256]{3,2,1,0:T(8,128)(2,1)S(1)}, f32[3,2048,256]{2,1,0:T(8,128)S(1)}) custom-call(s32[2]{0:T(128)S(1)} %pad_add_fusion.me, f32[8,128]{1,0:T(8,128)S(1)} %add_add_fusion.totals, f32[3,2048,256]{2,1,0:T(8,128)S(1)} %steps.1.stepped, ...), custom_call_target="tpu_custom_call" | custom-call | flops 8388608 | bytes 3145728 | tf_op jit(solution)/shard_map/apply_far/pallas_call | solution.py:396
  63.1 2.4 %apply_near.1 = (bf16[2048,256]{1,0:T(8,128)(2,1)}, bf16[2048,256]{1,0:T(8,128)(2,1)}, bf16[2048,256]{1,0:T(8,128)(2,1)}) custom-call(s32[2]{0:T(128)S(1)} %pad_add_fusion.me, f32[3,2048,256]{2,1,0:T(8,128)S(1)} %get-tuple-element.55.change, bf16[3,4,128,256]{3,2,1,0:T(8,128)(2,1)S(1)} %get-tuple-element.56.pieces, ...), custom_call_target="tpu_custom_call" | custom-call | flops 16777216 | bytes 9437184 | tf_op jit(solution)/shard_map/apply_near/pallas_call | solution.py:438
  (19 shorter events, 1.9 us)
Async XLA Ops:
  5.9 3.7 %collective-permute-start.1 = (bf16[1024,512]{1,0:T(8,128)(2,1)S(1)}, bf16[1024,512]{1,0:T(8,128)(2,1)S(1)}, u32[]{:S(2)}, u32[]{:S(2)}) collective-permute-start(bf16[1024,512]{1,0:T(8,128)(2,1)S(1)} %get-tuple-element.36.own), channel_id=1, source_target_pairs={{0,1},{1,0},{2,3},{3,2},{4,5},{5,4},{6,7},{7,6},{8,9},{9,8},{10,11... | collective-permute-start | bytes 3145736 | tf_op jit(solution)/shard_map/ppermute | solution.py:508
  9.3 2.0 %collective-permute-start = (bf16[1024,256]{1,0:T(8,128)(2,1)S(1)}, bf16[1024,256]{1,0:T(8,128)(2,1)S(1)}, u32[]{:S(2)}, u32[]{:S(2)}) collective-permute-start(bf16[1024,256]{1,0:T(8,128)(2,1)S(1)} %get-tuple-element.41), channel_id=1, source_target_pairs={{0,1},{1,0},{2,3},{3,2},{4,5},{5,4},{6,7},{7,6},{8,9},{9,8},{10,11... | collective-permute-start | bytes 1572872 | tf_op jit(solution)/shard_map/ppermute | solution.py:510
  12.3 17.5 %all-to-all-start = ((bf16[16,48,256]{2,1,0:T(8,128)(2,1)}), bf16[16,48,256]{2,1,0:T(8,128)(2,1)S(1)}, u32[]{:S(2)}, u32[]{:S(2)}) async-start(bf16[16,48,256]{2,1,0:T(8,128)(2,1)} %contract_far.1), calls=%async_computation | async-start | bytes 786432 | tf_op jit(solution)/shard_map/all_to_all | solution.py:516
  20.2 14.2 %collective-permute-start.6 = (bf16[128,768]{1,0:T(8,128)(2,1)S(1)}, bf16[128,768]{1,0:T(8,128)(2,1)S(1)}, u32[]{:S(2)}, u32[]{:S(2)}) collective-permute-start(bf16[128,768]{1,0:T(8,128)(2,1)S(1)} %get-tuple-element.45.refs_0_), channel_id=1, source_target_pairs={{0,64},{8,72},{16,80},{24,88},{32,96},{40,104},{48,112},{56,120},{... | collective-permute-start | bytes 589832 | tf_op jit(solution)/shard_map/ppermute | solution.py:459
  23.1 11.4 %collective-permute-start.7 = (bf16[128,768]{1,0:T(8,128)(2,1)S(1)}, bf16[128,768]{1,0:T(8,128)(2,1)S(1)}, u32[]{:S(2)}, u32[]{:S(2)}) collective-permute-start(bf16[128,768]{1,0:T(8,128)(2,1)S(1)} %get-tuple-element.45.refs_0_), channel_id=1, source_target_pairs={{0,16},{8,24},{16,0},{24,8},{32,48},{40,56},{48,32},{56,40},{64,80... | collective-permute-start | bytes 589832 | tf_op jit(solution)/shard_map/ppermute | solution.py:459
  25.8 12.9 %collective-permute-start.8 = (bf16[128,768]{1,0:T(8,128)(2,1)S(1)}, bf16[128,768]{1,0:T(8,128)(2,1)S(1)}, u32[]{:S(2)}, u32[]{:S(2)}) collective-permute-start(bf16[128,768]{1,0:T(8,128)(2,1)S(1)} %get-tuple-element.45.refs_0_), channel_id=1, source_target_pairs={{0,80},{8,88},{16,64},{24,72},{32,112},{40,120},{48,96},{56,104},{... | collective-permute-start | bytes 589832 | tf_op jit(solution)/shard_map/ppermute | solution.py:459
  30.9 12.6 %all-to-all-start.1 = ((bf16[16,48,256]{2,1,0:T(8,128)(2,1)}), bf16[16,48,256]{2,1,0:T(8,128)(2,1)S(1)}, u32[]{:S(2)}, u32[]{:S(2)}) async-start(bf16[16,48,256]{2,1,0:T(8,128)(2,1)} %get-tuple-element.44), calls=%async_computation.1 | async-start | bytes 786432 | tf_op jit(solution)/shard_map/all_to_all | solution.py:518
  39.7 21.8 %copy-start = (bf16[4,128,768]{2,1,0:T(8,128)(2,1)S(1)}, bf16[4,128,768]{2,1,0:T(8,128)(2,1)}, u32[]{:S(2)}) copy-start(bf16[4,128,768]{2,1,0:T(8,128)(2,1)} %collected.1.four) | copy-start | bytes 2359300
  39.7 23.4 %collective-permute-start.10 = (bf16[4,128,768]{2,1,0:T(8,128)(2,1)}, bf16[4,128,768]{2,1,0:T(8,128)(2,1)S(1)}, u32[]{:S(2)}, u32[]{:S(2)}) collective-permute-start(bf16[4,128,768]{2,1,0:T(8,128)(2,1)} %collected.1.four), channel_id=1, source_target_pairs={{0,24},{8,0},{16,8},{24,16},{32,56},{40,32},{48,40},{56,48},{64,88... | collective-permute-start | bytes 2359304 | tf_op jit(solution)/shard_map/ppermute | solution.py:459
  40.6 22.5 %collective-permute-start.11 = (bf16[4,128,768]{2,1,0:T(8,128)(2,1)}, bf16[4,128,768]{2,1,0:T(8,128)(2,1)S(1)}, u32[]{:S(2)}, u32[]{:S(2)}) collective-permute-start(bf16[4,128,768]{2,1,0:T(8,128)(2,1)} %collected.1.four), channel_id=1, source_target_pairs={{0,40},{8,48},{16,56},{24,32},{32,72},{40,80},{48,88},{56,64},{64,... | collective-permute-start | bytes 2359304 | tf_op jit(solution)/shard_map/ppermute | solution.py:459
  41.1 21.9 %collective-permute-start.9 = (bf16[4,128,768]{2,1,0:T(8,128)(2,1)}, bf16[4,128,768]{2,1,0:T(8,128)(2,1)S(1)}, u32[]{:S(2)}, u32[]{:S(2)}) collective-permute-start(bf16[4,128,768]{2,1,0:T(8,128)(2,1)} %collected.1.four), channel_id=1, source_target_pairs={{0,96},{8,104},{16,112},{24,120},{32,0},{40,8},{48,16},{56,24},{64... | collective-permute-start | bytes 2359304 | tf_op jit(solution)/shard_map/ppermute | solution.py:459
  43.8 8.1 %collective-permute-start.2 = (f32[8,128]{1,0:T(8,128)S(1)}, f32[8,128]{1,0:T(8,128)S(1)}, u32[]{:S(2)}, u32[]{:S(2)}) collective-permute-start(f32[8,128]{1,0:T(8,128)S(1)} %squares.1), channel_id=1, source_target_pairs={{0,1},{1,0},{2,3},{3,2},{4,5},{5,4},{6,7},{7,6},{8,9},{9,8},{10,11... | collective-permute-start | bytes 12296 | tf_op jit(solution)/shard_map/ppermute | solution.py:470
  51.9 4.0 %collective-permute-start.3 = (f32[8,128]{1,0:T(8,128)S(1)}, f32[8,128]{1,0:T(8,128)S(1)}, u32[]{:S(2)}, u32[]{:S(2)}) collective-permute-start(f32[8,128]{1,0:T(8,128)S(1)} %add.12), channel_id=1, source_target_pairs={{0,2},{2,4},{4,6},{6,0},{1,3},{3,5},{5,7},{7,1},{8,10},{10,12},{12... | collective-permute-start | bytes 12296 | tf_op jit(solution)/shard_map/ppermute | solution.py:472
  53.2 8.2 %collective-permute-start.4 = (f32[8,128]{1,0:T(8,128)S(1)}, f32[8,128]{1,0:T(8,128)S(1)}, u32[]{:S(2)}, u32[]{:S(2)}) collective-permute-start(f32[8,128]{1,0:T(8,128)S(1)} %add.12), channel_id=1, source_target_pairs={{0,6},{2,0},{4,2},{6,4},{1,7},{3,1},{5,3},{7,5},{8,14},{10,8},{12,... | collective-permute-start | bytes 12296 | tf_op jit(solution)/shard_map/ppermute | solution.py:472
  55.8 5.5 %collective-permute-start.5 = (f32[8,128]{1,0:T(8,128)S(1)}, f32[8,128]{1,0:T(8,128)S(1)}, u32[]{:S(2)}, u32[]{:S(2)}) collective-permute-start(f32[8,128]{1,0:T(8,128)S(1)} %add.12), channel_id=1, source_target_pairs={{0,4},{2,6},{4,0},{6,2},{1,5},{3,7},{5,1},{7,3},{8,12},{10,14},{12... | collective-permute-start | bytes 12296 | tf_op jit(solution)/shard_map/ppermute | solution.py:472
